TPU v7x, 32 devices: a whole 2x2x4 slice. The times are simulated.
32 devices in a mesh: fs: 8 (over z, y), tp: 4 (over x, core).
Axes of the slice: x: 2, y: 2, z: 4, core: 2. Of those that a mesh axis runs over, the one named last changes fastest.
Arguments:
- saved_input: bfloat16 [6144, 2048], P('fs'), may hold values from -6 to 6
- cot_inproj: bfloat16 [6144, 1024], P('fs', 'tp'), may hold values from -0.076171875 to 0.076171875
- cot_outproj: bfloat16 [6144, 1024], P('fs', 'tp'), may hold values from -0.076171875 to 0.076171875
- factor_inproj: bfloat16 [2048, 256], P('fs')
- factor_outproj: bfloat16 [2048, 256], P('fs')
- weight_inproj: float32 [2048, 1024], P('fs', 'tp'), may hold values from -0.125 to 0.125
- weight_outproj: float32 [2048, 1024], P('fs', 'tp'), may hold values from -0.125 to 0.125
- first_inproj: float32 [256, 1024], P('fs', 'tp'), may hold values from -6 to 6
- first_outproj: float32 [256, 1024], P('fs', 'tp'), may hold values from -6 to 6
- second_inproj: float32 [256, 1024], P('fs', 'tp'), may hold values from 0.25 to 4
- second_outproj: float32 [256, 1024], P('fs', 'tp'), may hold values from 0.25 to 4
Outputs:
- update_inproj: float32 [2048, 1024], P('fs', 'tp')
- update_outproj: float32 [2048, 1024], P('fs', 'tp')
- new_inproj: float32 [2048, 1024], P('fs', 'tp')
- new_outproj: float32 [2048, 1024], P('fs', 'tp')
- copy_inproj: bfloat16 [2048, 1024], P(None, 'tp')
- copy_outproj: bfloat16 [2048, 1024], P(None, 'tp')
- first_inproj_new: float32 [256, 1024], P('fs', 'tp')
- first_outproj_new: float32 [256, 1024], P('fs', 'tp')
- second_inproj_new: float32 [256, 1024], P('fs', 'tp')
- second_outproj_new: float32 [256, 1024], P('fs', 'tp')
All inputs are finite; a program needn't handle non-finite values.
Results may differ from a plain program's by a relative error of at most 0.00045.
Values may be sent and summed in bfloat16 or wider, within the bound.
No kernel may reach another device: no remote copies, remote signals or barrier semaphores. Data moves between devices by JAX's collectives and lax.ppermute only.
A program may use at most 64 MiB of HBM per device.

v0:
```python
import jax
import jax.numpy as jnp
from jax import lax
from jax.sharding import PartitionSpec as P


def contract_rows(left, right, precision):
    return lax.dot_general(
        left,
        right,
        (((0,), (0,)), ((), ())),
        precision=precision,
        preferred_element_type=jnp.float32,
    )


def on_device(
    saved_input,
    cot_inproj,
    cot_outproj,
    factor_inproj,
    factor_outproj,
    weight_inproj,
    weight_outproj,
    first_inproj,
    first_outproj,
    second_inproj,
    second_outproj,
):
    highest = lax.Precision.HIGHEST
    pieces = (
        lax.all_gather(factor_inproj, "fs", axis=0, tiled=True),
        lax.all_gather(factor_outproj, "fs", axis=0, tiled=True),
    )
    mapped_in = jnp.dot(saved_input, pieces[0], preferred_element_type=jnp.float32)
    mapped_out = jnp.dot(saved_input, pieces[1], preferred_element_type=jnp.float32)
    term_in = contract_rows(mapped_in, cot_inproj.astype(jnp.float32), highest)
    term_out = contract_rows(mapped_out, cot_outproj.astype(jnp.float32), highest)
    projected_in, projected_out = (
        lax.psum_scatter(term_in, "fs", scatter_dimension=0, tiled=True),
        lax.psum_scatter(term_out, "fs", scatter_dimension=0, tiled=True),
    )
    first_in_new = 0.8 * first_inproj + 0.2 * projected_in
    first_out_new = 0.8 * first_outproj + 0.2 * projected_out
    second_in_new = 0.9 * second_inproj + 0.1 * projected_in * projected_in
    second_out_new = 0.9 * second_outproj + 0.1 * projected_out * projected_out
    small_in = first_in_new / (jnp.sqrt(second_in_new) + 1e-08)
    small_out = first_out_new / (jnp.sqrt(second_out_new) + 1e-08)
    wide_in = factor_inproj.astype(jnp.float32)
    wide_out = factor_outproj.astype(jnp.float32)
    pieces = (
        lax.all_gather(small_in, "fs", axis=0, tiled=True),
        lax.all_gather(small_out, "fs", axis=0, tiled=True),
    )
    full_in = jnp.dot(wide_in, pieces[0], precision=highest)
    full_out = jnp.dot(wide_out, pieces[1], precision=highest)
    square_in, square_out = lax.psum(
        (jnp.sum(full_in * full_in), jnp.sum(full_out * full_out)), ("fs", "tp")
    )
    entries = float(full_in.shape[0] * full_in.shape[1] * lax.axis_size("fs") * lax.axis_size("tp"))
    update_in = full_in / jnp.sqrt(square_in / entries + 1e-06)
    update_out = full_out / jnp.sqrt(square_out / entries + 1e-06)
    fresh_in = weight_inproj - 0.02 * update_in
    fresh_out = weight_outproj - 0.02 * update_out
    copy_in, copy_out = (
        lax.all_gather(fresh_in.astype(jnp.bfloat16), "fs", axis=0, tiled=True),
        lax.all_gather(fresh_out.astype(jnp.bfloat16), "fs", axis=0, tiled=True),
    )
    return (
        update_in,
        update_out,
        fresh_in,
        fresh_out,
        copy_in,
        copy_out,
        first_in_new,
        first_out_new,
        second_in_new,
        second_out_new,
    )


def solution(mesh):
    return jax.shard_map(
        on_device,
        mesh=mesh,
        in_specs=(
            P("fs", None),
            P("fs", "tp"),
            P("fs", "tp"),
            P("fs", None),
            P("fs", None),
            P("fs", "tp"),
            P("fs", "tp"),
            P("fs", "tp"),
            P("fs", "tp"),
            P("fs", "tp"),
            P("fs", "tp"),
        ),
        out_specs=(
            P("fs", "tp"),
            P("fs", "tp"),
            P("fs", "tp"),
            P("fs", "tp"),
            P(None, "tp"),
            P(None, "tp"),
            P("fs", "tp"),
            P("fs", "tp"),
            P("fs", "tp"),
            P("fs", "tp"),
        ),
        check_vma=False,
    )
```

profile of v0, /device:TPU:0, one launch (start us, length us, event | category | flops | bytes accessed | tf_op | source)
XLA Modules:
  0.0 389.0 jit_solution(17355608462318028329)
XLA Ops:
  7.2 0.7 all-gather.5.cloned.1.call-update
  8.0 0.7 all-gather.7.cloned.1.call-update
  8.7 1.1 copy.21
  9.8 43.4 %all-gather.5.cloned.1.call-done = bf16[2048,256]{1,0:T(8,128)(2,1)} async-done(((bf16[256,256]{1,0:T(8,128)(2,1)}), bf16[2048,256]{1,0:T(8,128)(2,1)}) %all-gather.5.cloned.1.call-update) | async-done | bytes 1048592 | tf_op jit(solution)/shard_map/all_gather | solution.py:32
  53.2 2.3 fusion.6
  55.4 1.5 fusion.7
  57.0 0.0 reduce-scatter.5.cloned.1.call-start
  57.0 37.3 %all-gather.7.cloned.1.call-done = bf16[2048,256]{1,0:T(8,128)(2,1)} async-done(((bf16[256,256]{1,0:T(8,128)(2,1)}), bf16[2048,256]{1,0:T(8,128)(2,1)}) %all-gather.7.cloned.1.call-update) | async-done | bytes 1048592 | tf_op jit(solution)/shard_map/all_gather | solution.py:33
  94.3 2.3 fusion.8
  96.6 1.5 fusion.9
  98.1 0.0 all-gather.9.cloned.1.call-start
  98.2 60.9 %reduce-scatter.3.cloned.1.call-done = f32[32,256]{1,0:T(8,128)} async-done(((f32[256,256]{1,0:T(8,128)}), f32[32,256]{1,0:T(8,128)}) %reduce-scatter.3.cloned.1.call-update) | async-done | bytes 32784 | tf_op jit(solution)/shard_map/reduce_scatter | solution.py:40
  159.0 1.4 add_divide_fusion.1
  160.5 30.9 %all_gather.19 = f32[256,256]{1,0:T(8,128)S(1)} all-gather(f32[32,256]{1,0:T(8,128)S(1)} %get-tuple-element.31), channel_id=1, replica_groups=mesh['fs'=8,'tp'=4] {'fs'}, dimensions={0}, use_global_device_ids=true | all-gather | bytes 294912 | tf_op jit(solution)/shard_map/all_gather | solution.py:52
  191.4 1.7 multiply_reduce_fusion.1
  193.1 30.8 %reduce-scatter.5.cloned.1.call-done = f32[32,256]{1,0:T(8,128)} async-done(((f32[256,256]{1,0:T(8,128)}), f32[32,256]{1,0:T(8,128)}) %reduce-scatter.5.cloned.1.call-update) | async-done | bytes 32784 | tf_op jit(solution)/shard_map/reduce_scatter | solution.py:41
  223.9 1.4 add_divide_fusion
  225.3 30.9 %all_gather.21 = f32[256,256]{1,0:T(8,128)S(1)} all-gather(f32[32,256]{1,0:T(8,128)S(1)} %get-tuple-element.28), channel_id=1, replica_groups=mesh['fs'=8,'tp'=4] {'fs'}, dimensions={0}, use_global_device_ids=true | all-gather | bytes 294912 | tf_op jit(solution)/shard_map/all_gather | solution.py:53
  256.2 2.6 multiply_reduce_fusion
  258.8 37.9 %all-reduce = (f32[]{:T(128)}, f32[]{:T(128)}) all-reduce(f32[]{:T(128)} %get-tuple-element.34, f32[]{:T(128)} %get-tuple-element.36), channel_id=1, replica_groups=mesh['fs'=8,'tp'=4] {'fs','tp'}, use_global_device_ids=true, to_apply=%region_2.0 | all-reduce | flops 2 | bytes 16 | tf_op jit(solution)/shard_map/psum | solution.py:57
  297.4 1.8 fusion.3
  299.3 0.0 all-gather.11.cloned.1.call-start
  299.3 1.8 copy.22
  301.8 1.8 fusion.2
  303.7 1.8 copy.25
  305.4 1.8 copy.23
  307.2 1.8 copy.26
  309.0 0.8 copy.24
  309.9 29.7 %all-gather.9.cloned.1.call-done = bf16[2048,256]{0,1:T(8,128)(2,1)} async-done(((bf16[256,256]{0,1:T(8,128)(2,1)}), bf16[2048,256]{0,1:T(8,128)(2,1)}) %all-gather.9.cloned.1.call-update) | async-done | bytes 1048592 | tf_op jit(solution)/shard_map/all_gather | solution.py:66
  339.6 2.3 copy.27
  341.8 38.1 %all-gather.11.cloned.1.call-done = bf16[2048,256]{0,1:T(8,128)(2,1)} async-done(((bf16[256,256]{0,1:T(8,128)(2,1)}), bf16[2048,256]{0,1:T(8,128)(2,1)}) %all-gather.11.cloned.1.call-update) | async-done | bytes 1048592 | tf_op jit(solution)/shard_map/all_gather | solution.py:67
  379.9 2.3 copy.28
  (15 shorter events, 0.2 us)
Async XLA Ops:
  7.2 46.0 %copy-start = (bf16[768,2048]{1,0:T(8,128)(2,1)S(1)}, bf16[768,2048]{1,0:T(8,128)(2,1)}, u32[]{:S(2)}) copy-start(bf16[768,2048]{1,0:T(8,128)(2,1)} %param.11) | copy-start | bytes 9437188
  7.2 46.0 %all-gather.5.cloned.1.call-start = ((), (), s32[]{:S(2)}) async-start(), calls=%async_computation.2 | async-start | bytes 1179648 | tf_op jit(solution)/shard_map/all_gather | solution.py:32
  7.9 86.4 %all-gather.7.cloned.1.call-start = ((), (), s32[]{:S(2)}) async-start(), calls=%async_computation.4 | async-start | bytes 1179648 | tf_op jit(solution)/shard_map/all_gather | solution.py:33
  8.7 150.4 %reduce-scatter.3.cloned.1.call-start = ((), (), s32[]{:S(2)}) async-start(), calls=%async_computation.3 | async-start | bytes 294912 | tf_op jit(solution)/shard_map/reduce_scatter | solution.py:40
  53.2 2.3 copy-start.2
  57.0 134.4 %copy-start.1 = (bf16[256,256]{1,0:T(8,128)(2,1)S(1)}, bf16[256,256]{1,0:T(8,128)(2,1)}, u32[]{:S(2)}) copy-start(bf16[256,256]{1,0:T(8,128)(2,1)} %param.14) | copy-start | bytes 393220
  57.0 166.9 %reduce-scatter.5.cloned.1.call-start = ((), (), s32[]{:S(2)}) async-start(), calls=%async_computation.5 | async-start | bytes 294912 | tf_op jit(solution)/shard_map/reduce_scatter | solution.py:41
  94.3 2.3 copy-start.3
  98.1 241.5 %all-gather.9.cloned.1.call-start = ((), (), s32[]{:S(2)}) async-start(), calls=%async_computation.6 | async-start | bytes 1179648 | tf_op jit(solution)/shard_map/all_gather | solution.py:66
  299.3 80.6 %all-gather.11.cloned.1.call-start = ((), (), s32[]{:S(2)}) async-start(), calls=%async_computation.7 | async-start | bytes 1179648 | tf_op jit(solution)/shard_map/all_gather | solution.py:67
Sparse Core Ops, SparseCore 0:
  10.1 42.9 all-gather.4
  55.3 38.9 all-gather.6
  98.2 60.7 reduce-scatter.2
  162.8 61.0 reduce-scatter.4
  299.4 40.1 all-gather.8
  341.5 38.3 all-gather.10
where the time goes:
time: 390 us; the launch traced here: 389 us
  waiting for transfers between devices  242 us (62%)
  blocking collectives  99.7 us (26%)
  between operations  15.6 us (4%)
  local copies, waits for them, and re-layouts  13.6 us (3%)
  matrix products  11.8 us (3%)
  other arithmetic  6.5 us (2%)
    reduce_scatter x1, waiting for transfers between devices, on_device(): lax.psum_scatter(term_in, 'fs', scatter_dimension=0, tiled=True)  60.9 us
    all_gather x1, waiting for transfers between devices, on_device(): lax.all_gather(factor_inproj, 'fs', axis=0, tiled=True)  43.4 us
    all_gather x1, waiting for transfers between devices, on_device(): lax.all_gather(fresh_out.astype(jnp.bfloat16), 'fs', axis=0, tiled=True)  38.1 us
    psum x1, blocking collectives, on_device(): lax.psum((jnp.sum(full_in * full_in), jnp.sum(full_out * full_out)), ('fs...  37.9 us
    all_gather x1, waiting for transfers between devices, on_device(): lax.all_gather(factor_outproj, 'fs', axis=0, tiled=True)  37.3 us
    all_gather x1, blocking collectives, on_device(): lax.all_gather(small_in, 'fs', axis=0, tiled=True)  30.9 us
    all_gather x1, blocking collectives, on_device(): lax.all_gather(small_out, 'fs', axis=0, tiled=True)  30.9 us
    reduce_scatter x1, waiting for transfers between devices, on_device(): lax.psum_scatter(term_out, 'fs', scatter_dimension=0, tiled=True)  30.8 us
  transfers between devices with their start and end apart: 6, of which 6 were waited for; matrix products, arithmetic and copies ran while one was open for 6% of the time, Pallas kernels for 0%

commit v1 on v0

v1 whole, which is shorter than its diff:
```python
import jax
import jax.numpy as jnp
from jax import lax
from jax.sharding import PartitionSpec as P

HIGHEST = lax.Precision.HIGHEST


def flip(x, axis, bit):
    size = lax.axis_size(axis)
    return lax.ppermute(x, axis, [(i, i ^ bit) for i in range(size)])


def gather_blocks(x):
    size = lax.axis_size("fs")
    if size != 8:
        everyone = lax.all_gather(x, "fs", axis=0, tiled=False)
        here = lax.axis_index("fs")
        return [
            (d, lax.dynamic_index_in_dim(everyone, here ^ d, 0, keepdims=False)) for d in range(size)
        ]
    far, middle, near = flip(x, "fs", 6), flip(x, "fs", 4), flip(x, "fs", 2)
    side = flip(x, "fs", 1)
    return [
        (0, x),
        (1, side),
        (2, near),
        (3, flip(near, "fs", 1)),
        (4, middle),
        (5, flip(middle, "fs", 1)),
        (6, far),
        (7, flip(far, "fs", 1)),
    ]


def in_order(blocks):
    here = lax.axis_index("fs")
    rows = blocks[0][1].shape[0]
    whole = jnp.zeros((rows * len(blocks),) + blocks[0][1].shape[1:], blocks[0][1].dtype)
    for d, block in blocks:
        whole = lax.dynamic_update_slice_in_dim(whole, block, (here ^ d) * rows, 0)
    return whole


def sum_scatter(x):
    size = lax.axis_size("fs")
    if size != 8:
        return lax.psum_scatter(x, "fs", scatter_dimension=0, tiled=True)
    here = lax.axis_index("fs")
    rows = x.shape[0] // size
    total = lax.dynamic_slice_in_dim(x, here * rows, rows, 0)
    for d in (7, 6, 5, 4, 3, 2, 1):
        total = total + flip(lax.dynamic_slice_in_dim(x, (here ^ d) * rows, rows, 0), "fs", d)
    return total


def on_device(
    saved_input,
    cot_inproj,
    cot_outproj,
    factor_inproj,
    factor_outproj,
    weight_inproj,
    weight_outproj,
    first_inproj,
    first_outproj,
    second_inproj,
    second_outproj,
):
    odd = lax.axis_index("tp") % 2 == 1

    def mine(a, b):
        return jnp.where(odd, b, a)

    def theirs(a, b):
        return jnp.where(odd, a, b)

    factor = mine(factor_inproj, factor_outproj)
    factors = in_order(gather_blocks(factor))
    cot = mine(cot_inproj, cot_outproj)
    cot_peer = flip(theirs(cot_inproj, cot_outproj), "tp", 1)
    moments = jnp.stack([mine(first_inproj, first_outproj), mine(second_inproj, second_outproj)])
    moments_peer = flip(
        jnp.stack([theirs(first_inproj, first_outproj), theirs(second_inproj, second_outproj)]), "tp", 1
    )
    mapped = jnp.dot(saved_input, factors, preferred_element_type=jnp.float32)
    both = jnp.concatenate([cot, cot_peer], axis=1).astype(jnp.float32)
    term = lax.dot_general(
        mapped, both, (((0,), (0,)), ((), ())), precision=HIGHEST, preferred_element_type=jnp.float32
    )
    square = lax.dot_general(
        factors, factors, (((0,), (0,)), ((), ())), preferred_element_type=jnp.float32
    )
    projected = sum_scatter(term)
    first = jnp.concatenate([moments[0], moments_peer[0]], axis=1)
    second = jnp.concatenate([moments[1], moments_peer[1]], axis=1)
    first_new = 0.8 * first + 0.2 * projected
    second_new = 0.9 * second + 0.1 * projected * projected
    small = first_new / (jnp.sqrt(second_new) + 1e-08)
    columns = cot.shape[1]
    moments_new = jnp.stack([first_new[:, :columns], second_new[:, :columns]])
    moments_other = flip(jnp.stack([first_new[:, columns:], second_new[:, columns:]]), "tp", 1)
    smalls = in_order(gather_blocks(small))
    full = jnp.dot(factor.astype(jnp.float32), smalls, precision=HIGHEST)
    total = jnp.sum(smalls * jnp.dot(square, smalls, precision=HIGHEST))
    full_other = flip(full[:, columns:], "tp", 1)
    full_mine = full[:, :columns]
    total = jnp.full((8, 128), total, jnp.float32)
    bit = 2
    while bit < lax.axis_size("tp"):
        total = total + flip(total, "tp", bit)
        bit *= 2
    total_other = flip(total, "tp", 1)
    entries = float(full.shape[0] * columns * lax.axis_size("fs") * lax.axis_size("tp"))
    norm_mine = jnp.sqrt(jnp.maximum(total[0, 0], 0.0) / entries + 1e-06)
    norm_other = jnp.sqrt(jnp.maximum(total_other[0, 0], 0.0) / entries + 1e-06)
    update_mine = full_mine / norm_mine
    update_other = full_other / norm_other
    update_in, update_out = mine(update_mine, update_other), mine(update_other, update_mine)
    fresh_in = weight_inproj - 0.02 * update_in
    fresh_out = weight_outproj - 0.02 * update_out
    copies = gather_blocks(jnp.stack([fresh_in.astype(jnp.bfloat16), fresh_out.astype(jnp.bfloat16)]))
    copy_in = in_order([(d, block[0]) for d, block in copies])
    copy_out = in_order([(d, block[1]) for d, block in copies])
    return (
        update_in,
        update_out,
        fresh_in,
        fresh_out,
        copy_in,
        copy_out,
        mine(moments_new[0], moments_other[0]),
        mine(moments_other[0], moments_new[0]),
        mine(moments_new[1], moments_other[1]),
        mine(moments_other[1], moments_new[1]),
    )


def solution(mesh):
    rows, split = P("fs", None), P("fs", "tp")
    return jax.shard_map(
        on_device,
        mesh=mesh,
        in_specs=(rows, split, split, rows, rows) + (split,) * 6,
        out_specs=(split,) * 4 + (P(None, "tp"),) * 2 + (split,) * 4,
        check_vma=False,
    )
```

time: 390 us -> 114 us (0.29)
  waiting for transfers between devices: 242 us -> 40.4 us
  blocking collectives: 99.7 us -> 0 us
  starting transfers between devices: 0.24 us -> 41 us
  between operations: 15.6 us -> 2.54 us
    all_gather x4 -> x0, waiting for transfers between devices: 148 us -> none  [the longest x1 43.4 us: on_device(): lax.all_gather(factor_inproj, 'fs', axis=0, tiled=True)]
    reduce_scatter x2 -> x0, waiting for transfers between devices: 91.7 us -> none  [the longest x1 60.9 us: on_device(): lax.psum_scatter(term_in, 'fs', scatter_dimension=0, tiled=True)]
    all_gather x2 -> x0, blocking collectives: 61.8 us -> none  [the longest x1 30.9 us: on_device(): lax.all_gather(small_in, 'fs', axis=0, tiled=True)]
    ppermute x0 -> x34, starting transfers between devices: none -> 41 us  [flip(): return lax.ppermute(x, axis, [(i, i ^ bit) for i in range(size)])]
    ppermute x0 -> x34, waiting for transfers between devices: none -> 40.4 us  [flip(): return lax.ppermute(x, axis, [(i, i ^ bit) for i in range(size)])]
    psum x1 -> x0, blocking collectives: 37.9 us -> none  [on_device(): lax.psum((jnp.sum(full_in * full_in), jnp.sum(full_out * full_out)), ('fs...]
    unnamed x16 -> x26, local copies, waits for them, and re-layouts: 13.6 us -> 1.35 us
    dynamic_update_slice x0 -> x21, local copies, waits for them, and re-layouts: none -> 8.5 us  [in_order(): whole = lax.dynamic_update_slice_in_dim(whole, block, (here ^ d) * rows, 0)]
  transfers between devices with their start and end apart: 6 -> 34, of which waited for: 6 -> 12; matrix products, arithmetic and copies ran while one was open for 6% -> 21% of each run, Pallas kernels for 0% -> 0%
where the time goes in v1:
time: 114 us
  starting transfers between devices  41 us (36%)
  waiting for transfers between devices  40.4 us (35%)
  local copies, waits for them, and re-layouts  12.8 us (11%)
  matrix products  8.71 us (8%)
  other arithmetic  8.28 us (7%)
  between operations  2.54 us (2%)
    ppermute x34, starting transfers between devices, flip(): return lax.ppermute(x, axis, [(i, i ^ bit) for i in range(size)])  41 us
    ppermute x34, waiting for transfers between devices, flip(): return lax.ppermute(x, axis, [(i, i ^ bit) for i in range(size)])  40.4 us
    dynamic_update_slice x21, local copies, waits for them, and re-layouts, in_order(): whole = lax.dynamic_update_slice_in_dim(whole, block, (here ^ d) * rows, 0)  8.5 us
    select_n x3, other arithmetic, mine(): return jnp.where(odd, b, a)  3.23 us
    dynamic_update_slice x4, other arithmetic, in_order(): whole = lax.dynamic_update_slice_in_dim(whole, block, (here ^ d) * rows, 0)  2.8 us
  transfers between devices with their start and end apart: 34, of which 12 were waited for; matrix products, arithmetic and copies ran while one was open for 21% of the time, Pallas kernels for 0%

profile of v1, /device:TPU:0, one launch (start us, length us, event | category | flops | bytes accessed | tf_op | source)
XLA Modules:
  0.0 113.7 jit_solution(16386564493980381207)
XLA Ops:
  1.8 1.9 %constant_dynamic-update-slice_fusion.15 = (bf16[2048,256]{1,0:T(8,128)(2,1)}, bf16[256,256]{1,0:T(8,128)(2,1)}) fusion(bf16[2048,256]{1,0:T(8,128)(2,1)} %broadcast.7.clone, s32[]{:T(128)S(6)} %select_n.152, bf16[256,256]{1,0:T(8,128)(2,1)} %param.15, bf16[256,256]{1,0:T(8,128)(2,1)} %param.14, pred[]{:T(512)S(6)} %eq.5), kind=kLoop, calls=%fused_computation.93 | loop fusion | flops 65536 | bytes 524293 | tf_op jit(solution)/shard_map/dynamic_update_slice | solution.py:41
  3.7 3.0 %collective-permute-start.1 = (bf16[256,256]{1,0:T(8,128)(2,1)}, bf16[256,256]{1,0:T(8,128)(2,1)}, u32[]{:S(2)}, u32[]{:S(2)}) collective-permute-start(bf16[256,256]{1,0:T(8,128)(2,1)} %get-tuple-element.21), channel_id=1, source_target_pairs={{0,4},{4,0},{8,12},{12,8},{16,20},{20,16},{24,28},{28,24},{1,5},{5... | collective-permute-start | bytes 393224 | tf_op jit(solution)/shard_map/ppermute | solution.py:11
  6.7 1.6 %collective-permute-start.2 = (bf16[256,256]{1,0:T(8,128)(2,1)}, bf16[256,256]{1,0:T(8,128)(2,1)}, u32[]{:S(2)}, u32[]{:S(2)}) collective-permute-start(bf16[256,256]{1,0:T(8,128)(2,1)} %get-tuple-element.21), channel_id=1, source_target_pairs={{0,8},{4,12},{8,0},{12,4},{16,24},{20,28},{24,16},{28,20},{1,9},{5... | collective-permute-start | bytes 393224 | tf_op jit(solution)/shard_map/ppermute | solution.py:11
  8.2 2.6 %collective-permute-start.4 = (bf16[256,256]{1,0:T(8,128)(2,1)}, bf16[256,256]{1,0:T(8,128)(2,1)}, u32[]{:S(2)}, u32[]{:S(2)}) collective-permute-start(bf16[256,256]{1,0:T(8,128)(2,1)} %get-tuple-element.21), channel_id=1, source_target_pairs={{0,16},{4,20},{8,24},{12,28},{16,0},{20,4},{24,8},{28,12},{1,17},{... | collective-permute-start | bytes 393224 | tf_op jit(solution)/shard_map/ppermute | solution.py:11
  11.1 1.9 %broadcast_select_fusion.1 = (bf16[768,256]{1,0:T(8,128)(2,1)S(1)}, bf16[768,256]{1,0:T(8,128)(2,1)}) fusion(bf16[768,256]{1,0:T(8,128)(2,1)} %param.13, bf16[768,256]{1,0:T(8,128)(2,1)} %param.12, pred[]{:T(512)S(6)} %eq.5), kind=kLoop, calls=%fused_computation.7 | loop fusion | flops 393216 | bytes 1572865 | tf_op jit(solution)/shard_map/jit(_where)/select_n | solution.py:73
  15.3 5.9 %collective-permute-done.4 = bf16[256,256]{1,0:T(8,128)(2,1)} collective-permute-done((bf16[256,256]{1,0:T(8,128)(2,1)}, bf16[256,256]{1,0:T(8,128)(2,1)}, u32[]{:S(2)}, u32[]{:S(2)}) %collective-permute-start.4) | collective-permute-done | bytes 131104 | tf_op jit(solution)/shard_map/ppermute | solution.py:11
  21.7 1.5 %collective-permute-start.7 = (bf16[256,256]{1,0:T(8,128)(2,1)}, bf16[256,256]{1,0:T(8,128)(2,1)S(1)}, u32[]{:S(2)}, u32[]{:S(2)}) collective-permute-start(bf16[256,256]{1,0:T(8,128)(2,1)} %collective-permute-done.6), channel_id=1, source_target_pairs={{0,4},{4,0},{8,12},{12,8},{16,20},{20,16},{24,28},{28,24},{1,5},{5... | collective-permute-start | bytes 393224 | tf_op jit(solution)/shard_map/ppermute | solution.py:11
  23.2 1.6 %constant_dynamic-update-slice_fusion.14 = bf16[2048,256]{1,0:T(8,128)(2,1)} fusion(bf16[2048,256]{1,0:T(8,128)(2,1)} %get-tuple-element.20, bf16[256,256]{1,0:T(8,128)(2,1)} %collective-permute-done.1, s32[]{:T(128)S(6)} %select_n.153), kind=kLoop, calls=%fused_computation.92 | loop fusion | bytes 262148 | tf_op jit(solution)/shard_map/dynamic_update_slice | solution.py:41
  24.8 1.6 %constant_dynamic-update-slice_fusion.13 = bf16[2048,256]{1,0:T(8,128)(2,1)} fusion(bf16[2048,256]{1,0:T(8,128)(2,1)} %constant_dynamic-update-slice_fusion.14, bf16[256,256]{1,0:T(8,128)(2,1)} %collective-permute-done.2, s32[]{:T(128)S(6)} %select_n.154), kind=kLoop, calls=%fused_computation.91 | loop fusion | bytes 262148 | tf_op jit(solution)/shard_map/dynamic_update_slice | solution.py:41
  27.0 1.6 %constant_dynamic-update-slice_fusion.11 = bf16[2048,256]{1,0:T(8,128)(2,1)} fusion(bf16[2048,256]{1,0:T(8,128)(2,1)} %constant_dynamic-update-slice_fusion.12, bf16[256,256]{1,0:T(8,128)(2,1)} %collective-permute-done.4, s32[]{:T(128)S(6)} %select_n.156), kind=kLoop, calls=%fused_computation.89 | loop fusion | bytes 262148 | tf_op jit(solution)/shard_map/dynamic_update_slice | solution.py:41
  29.3 1.6 %constant_dynamic-update-slice_fusion.9 = bf16[2048,256]{1,0:T(8,128)(2,1)} fusion(bf16[2048,256]{1,0:T(8,128)(2,1)} %constant_dynamic-update-slice_fusion.10, bf16[256,256]{1,0:T(8,128)(2,1)} %collective-permute-done.6, s32[]{:T(128)S(6)} %select_n.158), kind=kLoop, calls=%fused_computation.87 | loop fusion | bytes 262148 | tf_op jit(solution)/shard_map/dynamic_update_slice | solution.py:41
  31.5 2.2 %fusion.28 = f32[256,768]{1,0:T(8,128)S(1)} fusion(bf16[2048,256]{1,0:T(8,128)(2,1)} %constant_dynamic-update-slice_fusion.8, bf16[768,2048]{1,0:T(8,128)(2,1)S(1)} %copy-done), kind=kOutput, calls=%fused_computation.96 | convolution fusion | flops 805306368 | bytes 4980736 | tf_op jit(solution)/shard_map/dot_general | solution.py:86
  33.8 1.8 %fusion = f32[256,512]{1,0:T(8,128)S(1)} fusion(f32[256,768]{1,0:T(8,128)S(1)} %fusion.28, bf16[768,256]{1,0:T(8,128)(2,1)} %collective-permute-done.8, bf16[768,256]{1,0:T(8,128)(2,1)S(1)} %get-tuple-element.22), kind=kOutput, calls=%fused_computation.1 | convolution fusion | flops 1209532416 | bytes 2097152 | tf_op jit(solution)/shard_map/dot_general | solution.py:88
  35.7 2.4 %collective-permute-start.10 = (f32[32,512]{1,0:T(8,128)S(1)}, f32[32,512]{1,0:T(8,128)S(1)}, u32[]{:S(2)}, u32[]{:S(2)}) collective-permute-start(f32[32,512]{1,0:T(8,128)S(1)} %get-tuple-element.30), channel_id=1, source_target_pairs={{0,24},{4,28},{8,16},{12,20},{16,8},{20,12},{24,0},{28,4},{1,25},{... | collective-permute-start | bytes 196616 | tf_op jit(solution)/shard_map/ppermute | solution.py:11
  38.6 2.4 %collective-permute-start.12 = (f32[32,512]{1,0:T(8,128)S(1)}, f32[32,512]{1,0:T(8,128)S(1)}, u32[]{:S(2)}, u32[]{:S(2)}) collective-permute-start(f32[32,512]{1,0:T(8,128)S(1)} %get-tuple-element.28), channel_id=1, source_target_pairs={{0,16},{4,20},{8,24},{12,28},{16,0},{20,4},{24,8},{28,12},{1,17},{... | collective-permute-start | bytes 196616 | tf_op jit(solution)/shard_map/ppermute | solution.py:11
  41.6 2.4 %collective-permute-start.14 = (f32[32,512]{1,0:T(8,128)S(1)}, f32[32,512]{1,0:T(8,128)S(1)}, u32[]{:S(2)}, u32[]{:S(2)}) collective-permute-start(f32[32,512]{1,0:T(8,128)S(1)} %get-tuple-element.26), channel_id=1, source_target_pairs={{0,8},{4,12},{8,0},{12,4},{16,24},{20,28},{24,16},{28,20},{1,9},{5... | collective-permute-start | bytes 196616 | tf_op jit(solution)/shard_map/ppermute | solution.py:11
  44.7 4.1 %collective-permute-start.9 = (f32[32,512]{1,0:T(8,128)S(1)}, f32[32,512]{1,0:T(8,128)S(1)}, u32[]{:S(2)}, u32[]{:S(2)}) collective-permute-start(f32[32,512]{1,0:T(8,128)S(1)} %get-tuple-element.24), channel_id=1, source_target_pairs={{0,28},{4,24},{8,20},{12,16},{16,12},{20,8},{24,4},{28,0},{1,29},{... | collective-permute-start | bytes 196616 | tf_op jit(solution)/shard_map/ppermute | solution.py:11
  48.8 2.0 %fusion.30 = f32[256,256]{1,0:T(8,128)S(1)} fusion(bf16[2048,256]{1,0:T(8,128)(2,1)} %constant_dynamic-update-slice_fusion.8), kind=kOutput, calls=%fused_computation.98 | convolution fusion | flops 268435456 | bytes 1310720 | tf_op jit(solution)/shard_map/dot_general | solution.py:91
  52.0 2.4 %collective-permute-start.16 = (f32[32,512]{1,0:T(8,128)S(1)}, f32[32,512]{1,0:T(8,128)S(1)}, u32[]{:S(2)}, u32[]{:S(2)}) collective-permute-start(f32[32,512]{1,0:T(8,128)S(1)} %get-tuple-element.17), channel_id=1, source_target_pairs={{0,4},{4,0},{8,12},{12,8},{16,20},{20,16},{24,28},{28,24},{1,5},{5... | collective-permute-start | bytes 196616 | tf_op jit(solution)/shard_map/ppermute | solution.py:11
  54.4 3.2 %collective-permute-start.19 = (f32[32,512]{1,0:T(8,128)S(1)}, f32[32,512]{1,0:T(8,128)S(1)}, u32[]{:S(2)}, u32[]{:S(2)}) collective-permute-start(f32[32,512]{1,0:T(8,128)S(1)} %get-tuple-element.17), channel_id=1, source_target_pairs={{0,16},{4,20},{8,24},{12,28},{16,0},{20,4},{24,8},{28,12},{1,17},{... | collective-permute-start | bytes 196616 | tf_op jit(solution)/shard_map/ppermute | solution.py:11
  60.9 2.8 %collective-permute-done.21 = f32[32,512]{1,0:T(8,128)S(1)} collective-permute-done((f32[32,512]{1,0:T(8,128)S(1)}, f32[32,512]{1,0:T(8,128)S(1)}, u32[]{:S(2)}, u32[]{:S(2)}) %collective-permute-start.21) | collective-permute-done | bytes 65568 | tf_op jit(solution)/shard_map/ppermute | solution.py:11
  64.2 3.8 %collective-permute-done.22 = f32[32,512]{1,0:T(8,128)S(1)} collective-permute-done((f32[32,512]{1,0:T(8,128)S(1)}, f32[32,512]{1,0:T(8,128)S(1)}, u32[]{:S(2)}, u32[]{:S(2)}) %collective-permute-start.22) | collective-permute-done | bytes 65568 | tf_op jit(solution)/shard_map/ppermute | solution.py:11
  68.0 1.3 %fusion.4 = f32[]{:T(128)} fusion(f32[256,512]{1,0:T(8,128)S(1)} %constant_dynamic-update-slice_fusion, f32[256,256]{1,0:T(8,128)S(1)} %fusion.30), kind=kOutput, calls=%fused_computation.5 | convolution fusion | flops 402915328 | bytes 786436 | tf_op jit(solution)/shard_map/dot_general | solution.py:105
  69.9 1.6 %collective-permute-start.24 = (f32[8,128]{1,0:T(8,128)S(1)}, f32[8,128]{1,0:T(8,128)S(1)}, u32[]{:S(2)}, u32[]{:S(2)}) collective-permute-start(f32[8,128]{1,0:T(8,128)S(1)} %broadcast_in_dim.7), channel_id=1, source_target_pairs={{0,2},{1,3},{2,0},{3,1},{4,6},{5,7},{6,4},{7,5},{8,10},{9,11},{10,... | collective-permute-start | bytes 12296 | tf_op jit(solution)/shard_map/ppermute | solution.py:11
  71.5 1.4 %fusion.29 = f32[256,512]{1,0:T(8,128)S(1)} fusion(bf16[256,256]{1,0:T(8,128)(2,1)} %get-tuple-element.21, f32[256,512]{1,0:T(8,128)S(1)} %constant_dynamic-update-slice_fusion), kind=kOutput, calls=%fused_computation.97 | convolution fusion | flops 402653184 | bytes 1179648 | tf_op jit(solution)/shard_map/dot_general | solution.py:104
  79.1 1.7 %collective-permute-start.29 = (bf16[2,256,256]{2,1,0:T(8,128)(2,1)S(1)}, bf16[2,256,256]{2,1,0:T(8,128)(2,1)S(1)}, u32[]{:S(2)}, u32[]{:S(2)}) collective-permute-start(bf16[2,256,256]{2,1,0:T(8,128)(2,1)S(1)} %pad_maximum_fusion), channel_id=1, source_target_pairs={{0,16},{4,20},{8,24},{12,28},{16,0},{20,4},{24,8},{28,12},{1,17},{... | collective-permute-start | bytes 786440 | tf_op jit(solution)/shard_map/ppermute | solution.py:11
  80.8 2.7 %collective-permute-start.31 = (bf16[2,256,256]{2,1,0:T(8,128)(2,1)S(1)}, bf16[2,256,256]{2,1,0:T(8,128)(2,1)S(1)}, u32[]{:S(2)}, u32[]{:S(2)}) collective-permute-start(bf16[2,256,256]{2,1,0:T(8,128)(2,1)S(1)} %pad_maximum_fusion), channel_id=1, source_target_pairs={{0,24},{4,28},{8,16},{12,20},{16,8},{20,12},{24,0},{28,4},{1,25},{... | collective-permute-start | bytes 786440 | tf_op jit(solution)/shard_map/ppermute | solution.py:11
  84.3 8.0 %collective-permute-done.27 = bf16[2,256,256]{2,1,0:T(8,128)(2,1)S(1)} collective-permute-done((bf16[2,256,256]{2,1,0:T(8,128)(2,1)S(1)}, bf16[2,256,256]{2,1,0:T(8,128)(2,1)S(1)}, u32[]{:S(2)}, u32[]{:S(2)}) %collective-permute-start.27) | collective-permute-done | bytes 262176 | tf_op jit(solution)/shard_map/ppermute | solution.py:11
  93.3 7.3 %collective-permute-done.29 = bf16[2,256,256]{2,1,0:T(8,128)(2,1)S(1)} collective-permute-done((bf16[2,256,256]{2,1,0:T(8,128)(2,1)S(1)}, bf16[2,256,256]{2,1,0:T(8,128)(2,1)S(1)}, u32[]{:S(2)}, u32[]{:S(2)}) %collective-permute-start.29) | collective-permute-done | bytes 262176 | tf_op jit(solution)/shard_map/ppermute | solution.py:11
  100.6 1.8 %collective-permute-start.30 = (bf16[2,256,256]{2,1,0:T(8,128)(2,1)S(1)}, bf16[2,256,256]{2,1,0:T(8,128)(2,1)S(1)}, u32[]{:S(2)}, u32[]{:S(2)}) collective-permute-start(bf16[2,256,256]{2,1,0:T(8,128)(2,1)S(1)} %collective-permute-done.29), channel_id=1, source_target_pairs={{0,4},{4,0},{8,12},{12,8},{16,20},{20,16},{24,28},{28,24},{1,5},{5... | collective-permute-start | bytes 786440 | tf_op jit(solution)/shard_map/ppermute | solution.py:11
  102.7 6.8 %collective-permute-done.30 = bf16[2,256,256]{2,1,0:T(8,128)(2,1)S(1)} collective-permute-done((bf16[2,256,256]{2,1,0:T(8,128)(2,1)S(1)}, bf16[2,256,256]{2,1,0:T(8,128)(2,1)S(1)}, u32[]{:S(2)}, u32[]{:S(2)}) %collective-permute-start.30) | collective-permute-done | bytes 262176 | tf_op jit(solution)/shard_map/ppermute | solution.py:11
  109.6 2.7 %collective-permute-done.32 = bf16[2,256,256]{2,1,0:T(8,128)(2,1)S(1)} collective-permute-done((bf16[2,256,256]{2,1,0:T(8,128)(2,1)S(1)}, bf16[2,256,256]{2,1,0:T(8,128)(2,1)S(1)}, u32[]{:S(2)}, u32[]{:S(2)}) %collective-permute-start.32) | collective-permute-done | bytes 262176 | tf_op jit(solution)/shard_map/ppermute | solution.py:11
  (113 shorter events, 21.6 us)
Async XLA Ops:
  3.7 10.8 %collective-permute-start.1 = (bf16[256,256]{1,0:T(8,128)(2,1)}, bf16[256,256]{1,0:T(8,128)(2,1)}, u32[]{:S(2)}, u32[]{:S(2)}) collective-permute-start(bf16[256,256]{1,0:T(8,128)(2,1)} %get-tuple-element.21), channel_id=1, source_target_pairs={{0,4},{4,0},{8,12},{12,8},{16,20},{20,16},{24,28},{28,24},{1,5},{5... | collective-permute-start | bytes 393224 | tf_op jit(solution)/shard_map/ppermute | solution.py:11
  6.7 8.3 %collective-permute-start.2 = (bf16[256,256]{1,0:T(8,128)(2,1)}, bf16[256,256]{1,0:T(8,128)(2,1)}, u32[]{:S(2)}, u32[]{:S(2)}) collective-permute-start(bf16[256,256]{1,0:T(8,128)(2,1)} %get-tuple-element.21), channel_id=1, source_target_pairs={{0,8},{4,12},{8,0},{12,4},{16,24},{20,28},{24,16},{28,20},{1,9},{5... | collective-permute-start | bytes 393224 | tf_op jit(solution)/shard_map/ppermute | solution.py:11
  8.2 13.0 %collective-permute-start.4 = (bf16[256,256]{1,0:T(8,128)(2,1)}, bf16[256,256]{1,0:T(8,128)(2,1)}, u32[]{:S(2)}, u32[]{:S(2)}) collective-permute-start(bf16[256,256]{1,0:T(8,128)(2,1)} %get-tuple-element.21), channel_id=1, source_target_pairs={{0,16},{4,20},{8,24},{12,28},{16,0},{20,4},{24,8},{28,12},{1,17},{... | collective-permute-start | bytes 393224 | tf_op jit(solution)/shard_map/ppermute | solution.py:11
  10.8 10.9 %collective-permute-start.6 = (bf16[256,256]{1,0:T(8,128)(2,1)}, bf16[256,256]{1,0:T(8,128)(2,1)}, u32[]{:S(2)}, u32[]{:S(2)}) collective-permute-start(bf16[256,256]{1,0:T(8,128)(2,1)} %get-tuple-element.21), channel_id=1, source_target_pairs={{0,24},{4,28},{8,16},{12,20},{16,8},{20,12},{24,0},{28,4},{1,25},{... | collective-permute-start | bytes 393224 | tf_op jit(solution)/shard_map/ppermute | solution.py:11
  13.0 20.8 %collective-permute-start.8 = (bf16[768,256]{1,0:T(8,128)(2,1)}, bf16[768,256]{1,0:T(8,128)(2,1)}, u32[]{:S(2)}, u32[]{:S(2)}) collective-permute-start(bf16[768,256]{1,0:T(8,128)(2,1)} %get-tuple-element.23), channel_id=1, source_target_pairs={{0,1},{1,0},{2,3},{3,2},{4,5},{5,4},{6,7},{7,6},{8,9},{9,8},{10,11... | collective-permute-start | bytes 1179656 | tf_op jit(solution)/shard_map/ppermute | solution.py:11
  14.4 24.1 %collective-permute-start = (f32[2,32,256]{2,1,0:T(8,128)S(1)}, f32[2,32,256]{2,1,0:T(8,128)S(1)}, u32[]{:S(2)}, u32[]{:S(2)}) collective-permute-start(f32[2,32,256]{2,1,0:T(8,128)S(1)} %pad_maximum_fusion.1), channel_id=1, source_target_pairs={{0,1},{1,0},{2,3},{3,2},{4,5},{5,4},{6,7},{7,6},{8,9},{9,8},{10,11... | collective-permute-start | bytes 196616 | tf_op jit(solution)/shard_map/ppermute | solution.py:11
  15.0 11.4 %collective-permute-start.3 = (bf16[256,256]{1,0:T(8,128)(2,1)}, bf16[256,256]{1,0:T(8,128)(2,1)S(1)}, u32[]{:S(2)}, u32[]{:S(2)}) collective-permute-start(bf16[256,256]{1,0:T(8,128)(2,1)} %collective-permute-done.2), channel_id=1, source_target_pairs={{0,4},{4,0},{8,12},{12,8},{16,20},{20,16},{24,28},{28,24},{1,5},{5... | collective-permute-start | bytes 393224 | tf_op jit(solution)/shard_map/ppermute | solution.py:11
  21.2 7.4 %collective-permute-start.5 = (bf16[256,256]{1,0:T(8,128)(2,1)}, bf16[256,256]{1,0:T(8,128)(2,1)S(1)}, u32[]{:S(2)}, u32[]{:S(2)}) collective-permute-start(bf16[256,256]{1,0:T(8,128)(2,1)} %collective-permute-done.4), channel_id=1, source_target_pairs={{0,4},{4,0},{8,12},{12,8},{16,20},{20,16},{24,28},{28,24},{1,5},{5... | collective-permute-start | bytes 393224 | tf_op jit(solution)/shard_map/ppermute | solution.py:11
  21.7 9.1 %collective-permute-start.7 = (bf16[256,256]{1,0:T(8,128)(2,1)}, bf16[256,256]{1,0:T(8,128)(2,1)S(1)}, u32[]{:S(2)}, u32[]{:S(2)}) collective-permute-start(bf16[256,256]{1,0:T(8,128)(2,1)} %collective-permute-done.6), channel_id=1, source_target_pairs={{0,4},{4,0},{8,12},{12,8},{16,20},{20,16},{24,28},{28,24},{1,5},{5... | collective-permute-start | bytes 393224 | tf_op jit(solution)/shard_map/ppermute | solution.py:11
  35.7 8.4 %collective-permute-start.10 = (f32[32,512]{1,0:T(8,128)S(1)}, f32[32,512]{1,0:T(8,128)S(1)}, u32[]{:S(2)}, u32[]{:S(2)}) collective-permute-start(f32[32,512]{1,0:T(8,128)S(1)} %get-tuple-element.30), channel_id=1, source_target_pairs={{0,24},{4,28},{8,16},{12,20},{16,8},{20,12},{24,0},{28,4},{1,25},{... | collective-permute-start | bytes 196616 | tf_op jit(solution)/shard_map/ppermute | solution.py:11
  38.1 6.6 %collective-permute-start.11 = (f32[32,512]{1,0:T(8,128)S(1)}, f32[32,512]{1,0:T(8,128)S(1)}, u32[]{:S(2)}, u32[]{:S(2)}) collective-permute-start(f32[32,512]{1,0:T(8,128)S(1)} %get-tuple-element.29), channel_id=1, source_target_pairs={{0,20},{4,16},{8,28},{12,24},{16,4},{20,0},{24,12},{28,8},{1,21},{... | collective-permute-start | bytes 196616 | tf_op jit(solution)/shard_map/ppermute | solution.py:11
  38.6 12.2 %collective-permute-start.12 = (f32[32,512]{1,0:T(8,128)S(1)}, f32[32,512]{1,0:T(8,128)S(1)}, u32[]{:S(2)}, u32[]{:S(2)}) collective-permute-start(f32[32,512]{1,0:T(8,128)S(1)} %get-tuple-element.28), channel_id=1, source_target_pairs={{0,16},{4,20},{8,24},{12,28},{16,0},{20,4},{24,8},{28,12},{1,17},{... | collective-permute-start | bytes 196616 | tf_op jit(solution)/shard_map/ppermute | solution.py:11
  41.0 9.8 %collective-permute-start.13 = (f32[32,512]{1,0:T(8,128)S(1)}, f32[32,512]{1,0:T(8,128)S(1)}, u32[]{:S(2)}, u32[]{:S(2)}) collective-permute-start(f32[32,512]{1,0:T(8,128)S(1)} %get-tuple-element.27), channel_id=1, source_target_pairs={{0,12},{4,8},{8,4},{12,0},{16,28},{20,24},{24,20},{28,16},{1,13},{... | collective-permute-start | bytes 196616 | tf_op jit(solution)/shard_map/ppermute | solution.py:11
  41.6 9.2 %collective-permute-start.14 = (f32[32,512]{1,0:T(8,128)S(1)}, f32[32,512]{1,0:T(8,128)S(1)}, u32[]{:S(2)}, u32[]{:S(2)}) collective-permute-start(f32[32,512]{1,0:T(8,128)S(1)} %get-tuple-element.26), channel_id=1, source_target_pairs={{0,8},{4,12},{8,0},{12,4},{16,24},{20,28},{24,16},{28,20},{1,9},{5... | collective-permute-start | bytes 196616 | tf_op jit(solution)/shard_map/ppermute | solution.py:11
  44.0 6.8 %collective-permute-start.15 = (f32[32,512]{1,0:T(8,128)S(1)}, f32[32,512]{1,0:T(8,128)S(1)}, u32[]{:S(2)}, u32[]{:S(2)}) collective-permute-start(f32[32,512]{1,0:T(8,128)S(1)} %get-tuple-element.25), channel_id=1, source_target_pairs={{0,4},{4,0},{8,12},{12,8},{16,20},{20,16},{24,28},{28,24},{1,5},{5... | collective-permute-start | bytes 196616 | tf_op jit(solution)/shard_map/ppermute | solution.py:11
  44.7 7.1 %collective-permute-start.9 = (f32[32,512]{1,0:T(8,128)S(1)}, f32[32,512]{1,0:T(8,128)S(1)}, u32[]{:S(2)}, u32[]{:S(2)}) collective-permute-start(f32[32,512]{1,0:T(8,128)S(1)} %get-tuple-element.24), channel_id=1, source_target_pairs={{0,28},{4,24},{8,20},{12,16},{16,12},{20,8},{24,4},{28,0},{1,29},{... | collective-permute-start | bytes 196616 | tf_op jit(solution)/shard_map/ppermute | solution.py:11
  52.0 11.8 %collective-permute-start.16 = (f32[32,512]{1,0:T(8,128)S(1)}, f32[32,512]{1,0:T(8,128)S(1)}, u32[]{:S(2)}, u32[]{:S(2)}) collective-permute-start(f32[32,512]{1,0:T(8,128)S(1)} %get-tuple-element.17), channel_id=1, source_target_pairs={{0,4},{4,0},{8,12},{12,8},{16,20},{20,16},{24,28},{28,24},{1,5},{5... | collective-permute-start | bytes 196616 | tf_op jit(solution)/shard_map/ppermute | solution.py:11
  54.4 4.4 %collective-permute-start.17 = (f32[32,512]{1,0:T(8,128)S(1)}, f32[32,512]{1,0:T(8,128)S(1)}, u32[]{:S(2)}, u32[]{:S(2)}) collective-permute-start(f32[32,512]{1,0:T(8,128)S(1)} %get-tuple-element.17), channel_id=1, source_target_pairs={{0,8},{4,12},{8,0},{12,4},{16,24},{20,28},{24,16},{28,20},{1,9},{5... | collective-permute-start | bytes 196616 | tf_op jit(solution)/shard_map/ppermute | solution.py:11
  54.4 5.5 %collective-permute-start.19 = (f32[32,512]{1,0:T(8,128)S(1)}, f32[32,512]{1,0:T(8,128)S(1)}, u32[]{:S(2)}, u32[]{:S(2)}) collective-permute-start(f32[32,512]{1,0:T(8,128)S(1)} %get-tuple-element.17), channel_id=1, source_target_pairs={{0,16},{4,20},{8,24},{12,28},{16,0},{20,4},{24,8},{28,12},{1,17},{... | collective-permute-start | bytes 196616 | tf_op jit(solution)/shard_map/ppermute | solution.py:11
  57.6 6.1 %collective-permute-start.21 = (f32[32,512]{1,0:T(8,128)S(1)}, f32[32,512]{1,0:T(8,128)S(1)}, u32[]{:S(2)}, u32[]{:S(2)}) collective-permute-start(f32[32,512]{1,0:T(8,128)S(1)} %get-tuple-element.17), channel_id=1, source_target_pairs={{0,24},{4,28},{8,16},{12,20},{16,8},{20,12},{24,0},{28,4},{1,25},{... | collective-permute-start | bytes 196616 | tf_op jit(solution)/shard_map/ppermute | solution.py:11
  58.8 5.0 %collective-permute-start.18 = (f32[32,512]{1,0:T(8,128)S(1)}, f32[32,512]{1,0:T(8,128)S(1)}, u32[]{:S(2)}, u32[]{:S(2)}) collective-permute-start(f32[32,512]{1,0:T(8,128)S(1)} %collective-permute-done.17), channel_id=1, source_target_pairs={{0,4},{4,0},{8,12},{12,8},{16,20},{20,16},{24,28},{28,24},{1,5},{5... | collective-permute-start | bytes 196616 | tf_op jit(solution)/shard_map/ppermute | solution.py:11
  59.9 4.3 %collective-permute-start.20 = (f32[32,512]{1,0:T(8,128)S(1)}, f32[32,512]{1,0:T(8,128)S(1)}, u32[]{:S(2)}, u32[]{:S(2)}) collective-permute-start(f32[32,512]{1,0:T(8,128)S(1)} %collective-permute-done.19), channel_id=1, source_target_pairs={{0,4},{4,0},{8,12},{12,8},{16,20},{20,16},{24,28},{28,24},{1,5},{5... | collective-permute-start | bytes 196616 | tf_op jit(solution)/shard_map/ppermute | solution.py:11
  63.7 4.3 %collective-permute-start.22 = (f32[32,512]{1,0:T(8,128)S(1)}, f32[32,512]{1,0:T(8,128)S(1)}, u32[]{:S(2)}, u32[]{:S(2)}) collective-permute-start(f32[32,512]{1,0:T(8,128)S(1)} %collective-permute-done.21), channel_id=1, source_target_pairs={{0,4},{4,0},{8,12},{12,8},{16,20},{20,16},{24,28},{28,24},{1,5},{5... | collective-permute-start | bytes 196616 | tf_op jit(solution)/shard_map/ppermute | solution.py:11
  72.9 4.4 %collective-permute-start.23 = (f32[256,256]{1,0:T(8,128)S(1)}, f32[256,256]{1,0:T(8,128)S(1)}, u32[]{:S(2)}, u32[]{:S(2)}) collective-permute-start(f32[256,256]{1,0:T(8,128)S(1)} %slice.108), channel_id=1, source_target_pairs={{0,1},{1,0},{2,3},{3,2},{4,5},{5,4},{6,7},{7,6},{8,9},{9,8},{10,11... | collective-permute-start | bytes 786440 | tf_op jit(solution)/shard_map/ppermute | solution.py:11
  74.3 9.2 %collective-permute-start.33 = (f32[2,32,256]{2,1,0:T(8,128)S(1)}, f32[2,32,256]{2,1,0:T(8,128)S(1)}, u32[]{:S(2)}, u32[]{:S(2)}) collective-permute-start(f32[2,32,256]{2,1,0:T(8,128)S(1)} %pad_maximum_fusion.2), channel_id=1, source_target_pairs={{0,1},{1,0},{2,3},{3,2},{4,5},{5,4},{6,7},{7,6},{8,9},{9,8},{10,11... | collective-permute-start | bytes 196616 | tf_op jit(solution)/shard_map/ppermute | solution.py:11
  79.0 23.6 %collective-permute-start.26 = (bf16[2,256,256]{2,1,0:T(8,128)(2,1)S(1)}, bf16[2,256,256]{2,1,0:T(8,128)(2,1)S(1)}, u32[]{:S(2)}, u32[]{:S(2)}) collective-permute-start(bf16[2,256,256]{2,1,0:T(8,128)(2,1)S(1)} %pad_maximum_fusion), channel_id=1, source_target_pairs={{0,4},{4,0},{8,12},{12,8},{16,20},{20,16},{24,28},{28,24},{1,5},{5... | collective-permute-start | bytes 786440 | tf_op jit(solution)/shard_map/ppermute | solution.py:11
  79.1 13.2 %collective-permute-start.27 = (bf16[2,256,256]{2,1,0:T(8,128)(2,1)S(1)}, bf16[2,256,256]{2,1,0:T(8,128)(2,1)S(1)}, u32[]{:S(2)}, u32[]{:S(2)}) collective-permute-start(bf16[2,256,256]{2,1,0:T(8,128)(2,1)S(1)} %pad_maximum_fusion), channel_id=1, source_target_pairs={{0,8},{4,12},{8,0},{12,4},{16,24},{20,28},{24,16},{28,20},{1,9},{5... | collective-permute-start | bytes 786440 | tf_op jit(solution)/shard_map/ppermute | solution.py:11
  79.1 21.4 %collective-permute-start.29 = (bf16[2,256,256]{2,1,0:T(8,128)(2,1)S(1)}, bf16[2,256,256]{2,1,0:T(8,128)(2,1)S(1)}, u32[]{:S(2)}, u32[]{:S(2)}) collective-permute-start(bf16[2,256,256]{2,1,0:T(8,128)(2,1)S(1)} %pad_maximum_fusion), channel_id=1, source_target_pairs={{0,16},{4,20},{8,24},{12,28},{16,0},{20,4},{24,8},{28,12},{1,17},{... | collective-permute-start | bytes 786440 | tf_op jit(solution)/shard_map/ppermute | solution.py:11
  80.8 21.6 %collective-permute-start.31 = (bf16[2,256,256]{2,1,0:T(8,128)(2,1)S(1)}, bf16[2,256,256]{2,1,0:T(8,128)(2,1)S(1)}, u32[]{:S(2)}, u32[]{:S(2)}) collective-permute-start(bf16[2,256,256]{2,1,0:T(8,128)(2,1)S(1)} %pad_maximum_fusion), channel_id=1, source_target_pairs={{0,24},{4,28},{8,16},{12,20},{16,8},{20,12},{24,0},{28,4},{1,25},{... | collective-permute-start | bytes 786440 | tf_op jit(solution)/shard_map/ppermute | solution.py:11
  92.3 10.4 %collective-permute-start.28 = (bf16[2,256,256]{2,1,0:T(8,128)(2,1)S(1)}, bf16[2,256,256]{2,1,0:T(8,128)(2,1)S(1)}, u32[]{:S(2)}, u32[]{:S(2)}) collective-permute-start(bf16[2,256,256]{2,1,0:T(8,128)(2,1)S(1)} %collective-permute-done.27), channel_id=1, source_target_pairs={{0,4},{4,0},{8,12},{12,8},{16,20},{20,16},{24,28},{28,24},{1,5},{5... | collective-permute-start | bytes 786440 | tf_op jit(solution)/shard_map/ppermute | solution.py:11
  100.6 9.0 %collective-permute-start.30 = (bf16[2,256,256]{2,1,0:T(8,128)(2,1)S(1)}, bf16[2,256,256]{2,1,0:T(8,128)(2,1)S(1)}, u32[]{:S(2)}, u32[]{:S(2)}) collective-permute-start(bf16[2,256,256]{2,1,0:T(8,128)(2,1)S(1)} %collective-permute-done.29), channel_id=1, source_target_pairs={{0,4},{4,0},{8,12},{12,8},{16,20},{20,16},{24,28},{28,24},{1,5},{5... | collective-permute-start | bytes 786440 | tf_op jit(solution)/shard_map/ppermute | solution.py:11
  102.4 10.0 %collective-permute-start.32 = (bf16[2,256,256]{2,1,0:T(8,128)(2,1)S(1)}, bf16[2,256,256]{2,1,0:T(8,128)(2,1)S(1)}, u32[]{:S(2)}, u32[]{:S(2)}) collective-permute-start(bf16[2,256,256]{2,1,0:T(8,128)(2,1)S(1)} %collective-permute-done.31), channel_id=1, source_target_pairs={{0,4},{4,0},{8,12},{12,8},{16,20},{20,16},{24,28},{28,24},{1,5},{5... | collective-permute-start | bytes 786440 | tf_op jit(solution)/shard_map/ppermute | solution.py:11
  (15 other events, 229.7 us)

commit v2 on v1

v2 whole, which is shorter than its diff:
```python
import functools

import jax
import jax.numpy as jnp
from jax import lax
from jax.experimental import pallas as pl
from jax.experimental.pallas import tpu as pltpu
from jax.sharding import PartitionSpec as P

HIGHEST = lax.Precision.HIGHEST
VMEM = pl.BlockSpec(memory_space=pltpu.VMEM)
SMEM = pl.BlockSpec(memory_space=pltpu.SMEM)
VMEM_BYTES = 16 * 2**20
ROWS = (((0,), (0,)), ((), ()))


def flip(x, axis, bit):
    size = lax.axis_size(axis)
    return lax.ppermute(x, axis, [(i, i ^ bit) for i in range(size)])


def pairwise():
    return lax.axis_size("fs") == 8


def gather_blocks(x):
    size = lax.axis_size("fs")
    if not pairwise():
        everyone = lax.all_gather(x, "fs", axis=0, tiled=False)
        here = lax.axis_index("fs")
        return [
            lax.dynamic_index_in_dim(everyone, here ^ d, 0, keepdims=False) for d in range(size)
        ]
    far, middle, near = flip(x, "fs", 6), flip(x, "fs", 4), flip(x, "fs", 2)
    side = flip(x, "fs", 1)
    return [
        x,
        side,
        near,
        flip(near, "fs", 1),
        middle,
        flip(middle, "fs", 1),
        far,
        flip(far, "fs", 1),
    ]


def in_order(blocks):
    here = lax.axis_index("fs")
    rows = blocks[0].shape[0]
    whole = jnp.zeros((rows * len(blocks),) + blocks[0].shape[1:], blocks[0].dtype)
    for d, block in enumerate(blocks):
        whole = lax.dynamic_update_slice_in_dim(whole, block, (here ^ d) * rows, 0)
    return whole


def thirds(x):
    high = x.astype(jnp.bfloat16)
    rest = x - high.astype(jnp.float32)
    middle = rest.astype(jnp.bfloat16)
    low = (rest - middle.astype(jnp.float32)).astype(jnp.bfloat16)
    return high, middle, low


def call(body, outs, *args, scratch=(), flops):
    size = sum(a.size * a.dtype.itemsize for a in args)
    return pl.pallas_call(
        body,
        out_shape=outs,
        in_specs=[SMEM if a.dtype == jnp.int32 else VMEM for a in args],
        out_specs=jax.tree.map(lambda _: VMEM, outs),
        scratch_shapes=list(scratch),
        compiler_params=pltpu.CompilerParams(vmem_limit_bytes=VMEM_BYTES),
        cost_estimate=pl.CostEstimate(flops=flops, bytes_accessed=size, transcendentals=0),
    )(*args)


def map_body(size, here_ref, saved_ref, *refs):
    factors, (cot_ref, peer_ref, term_ref) = refs[:size], refs[size:]
    here = here_ref[0]
    depth, rank = factors[0].shape
    mapped = jnp.zeros((saved_ref.shape[0], rank), jnp.float32)
    for d, factor in enumerate(factors):
        at = pl.multiple_of((here ^ d) * depth, depth)
        mapped += jnp.dot(
            saved_ref[:, pl.ds(at, depth)], factor[...], preferred_element_type=jnp.float32
        )
    parts = thirds(mapped)
    columns = cot_ref.shape[1]
    rows = rank // size
    for side, cot in enumerate((cot_ref, peer_ref)):
        term = sum(
            lax.dot_general(part, cot[...], ROWS, preferred_element_type=jnp.float32)
            for part in parts[::-1]
        )
        for k in range(size):
            term_ref[here ^ k, :, side * columns : (side + 1) * columns] = term[
                k * rows : (k + 1) * rows, :
            ]


def square_body(*refs):
    total = jnp.zeros(refs[-1].shape, jnp.float32)
    for factor in refs[:-1]:
        total += lax.dot_general(factor[...], factor[...], ROWS, preferred_element_type=jnp.float32)
    refs[-1][...] = total


def full_body(size, here_ref, factor_ref, square_ref, *refs):
    smalls, (full_ref, other_ref, sum_ref, held) = refs[:size], refs[size:]
    rows = smalls[0].shape[0]
    for d, small in enumerate(smalls):
        at = pl.multiple_of((here_ref[0] ^ d) * rows, rows)
        held[pl.ds(at, rows), :] = small[...]
    columns = full_ref.shape[1]
    small = held[...]
    full = sum(
        jnp.dot(factor_ref[...], part, preferred_element_type=jnp.float32)
        for part in thirds(small)[::-1]
    )
    full_ref[...] = full[:, :columns]
    other_ref[...] = full[:, columns:]
    product = small * jnp.dot(square_ref[...], small, precision=HIGHEST)
    sum_ref[...] = jnp.full(sum_ref.shape, jnp.sum(product), jnp.float32)


def finish_body(entries, odd_ref, sums_ref, others_ref, full_ref, other_ref, *refs):
    weights, (up_in, up_out, new_in, new_out, copy) = refs[:2], refs[2:]
    odd = odd_ref[0] == 1

    def norm(ref):
        mean = jnp.maximum(jnp.sum(ref[...], axis=0), 0.0) / entries
        return jnp.sqrt(mean + 1e-06)[0:1, 0:1]

    update = full_ref[...] / norm(sums_ref)
    update_other = other_ref[...] / norm(others_ref)
    for k, (up, new, weight) in enumerate(
        ((up_in, new_in, weights[0]), (up_out, new_out, weights[1]))
    ):
        chosen = jnp.where(odd, update, update_other) if k else jnp.where(odd, update_other, update)
        up[...] = chosen
        fresh = weight[...] - 0.02 * chosen
        new[...] = fresh
        copy[k] = fresh.astype(jnp.bfloat16)


def on_device(
    saved_input,
    cot_inproj,
    cot_outproj,
    factor_inproj,
    factor_outproj,
    weight_inproj,
    weight_outproj,
    first_inproj,
    first_outproj,
    second_inproj,
    second_outproj,
):
    odd = lax.axis_index("tp") % 2 == 1
    size, split = lax.axis_size("fs"), lax.axis_size("tp")
    here = lax.axis_index("fs").astype(jnp.int32).reshape(1)
    f32 = functools.partial(jax.ShapeDtypeStruct, dtype=jnp.float32)

    def mine(a, b):
        return jnp.where(odd, b, a)

    def theirs(a, b):
        return jnp.where(odd, a, b)

    factor = mine(factor_inproj, factor_outproj)
    depth, rank = factor.shape
    columns = cot_inproj.shape[1]
    factors = gather_blocks(factor)
    cot = mine(cot_inproj, cot_outproj)
    cot_peer = flip(theirs(cot_inproj, cot_outproj), "tp", 1)
    moments = jnp.stack([mine(first_inproj, first_outproj), mine(second_inproj, second_outproj)])
    moments_peer = flip(
        jnp.stack([theirs(first_inproj, first_outproj), theirs(second_inproj, second_outproj)]), "tp", 1
    )
    if pairwise():
        tokens = saved_input.shape[0]
        term = call(
            functools.partial(map_body, size),
            f32((size, rank // size, 2 * columns)),
            here,
            saved_input,
            *factors,
            cot,
            cot_peer,
            flops=2 * tokens * rank * (depth * size + 6 * columns),
        )
        square = call(square_body, f32((rank, rank)), *factors, flops=2 * rank * rank * depth * size)
        projected = term[0] + sum(flip(term[d], "fs", d) for d in (7, 6, 5, 4, 3, 2, 1))
    else:
        factors = in_order(factors)
        mapped = jnp.dot(saved_input, factors, preferred_element_type=jnp.float32)
        both = jnp.concatenate([cot, cot_peer], axis=1).astype(jnp.float32)
        term = lax.dot_general(mapped, both, ROWS, precision=HIGHEST)
        square = lax.dot_general(factors, factors, ROWS, preferred_element_type=jnp.float32)
        projected = lax.psum_scatter(term, "fs", scatter_dimension=0, tiled=True)
    first = jnp.concatenate([moments[0], moments_peer[0]], axis=1)
    second = jnp.concatenate([moments[1], moments_peer[1]], axis=1)
    first_new = 0.8 * first + 0.2 * projected
    second_new = 0.9 * second + 0.1 * projected * projected
    small = first_new / (jnp.sqrt(second_new) + 1e-08)
    moments_new = jnp.stack([first_new[:, :columns], second_new[:, :columns]])
    moments_other = flip(jnp.stack([first_new[:, columns:], second_new[:, columns:]]), "tp", 1)
    smalls = gather_blocks(small)
    if pairwise():
        full, full_other, total = call(
            functools.partial(full_body, size),
            (f32((depth, columns)), f32((depth, columns)), f32((8, 128))),
            here,
            factor,
            square,
            *smalls,
            scratch=[pltpu.VMEM((rank, 2 * columns), jnp.float32)],
            flops=2 * rank * 2 * columns * (3 * depth + 6 * rank),
        )
    else:
        smalls = in_order(smalls)
        full = jnp.dot(factor.astype(jnp.float32), smalls, precision=HIGHEST)
        total = jnp.sum(smalls * jnp.dot(square, smalls, precision=HIGHEST))
        total = jnp.full((8, 128), total, jnp.float32)
        full, full_other = full[:, :columns], full[:, columns:]
    full_other = flip(full_other, "tp", 1)
    totals = [total] + [flip(total, "tp", k) for k in range(1, split)]
    sums, sums_other = jnp.stack(totals[0::2]), jnp.stack(totals[1::2])
    entries = float(depth * size * columns * split)
    shard = f32((depth, columns))
    update_in, update_out, fresh_in, fresh_out, copies = call(
        functools.partial(finish_body, entries),
        (shard,) * 4 + (jax.ShapeDtypeStruct((2, depth, columns), jnp.bfloat16),),
        odd.astype(jnp.int32).reshape(1),
        sums,
        sums_other,
        full,
        full_other,
        weight_inproj,
        weight_outproj,
        flops=10 * depth * columns,
    )
    copies = gather_blocks(copies)
    copy_in = in_order([block[0] for block in copies])
    copy_out = in_order([block[1] for block in copies])
    return (
        update_in,
        update_out,
        fresh_in,
        fresh_out,
        copy_in,
        copy_out,
        mine(moments_new[0], moments_other[0]),
        mine(moments_other[0], moments_new[0]),
        mine(moments_new[1], moments_other[1]),
        mine(moments_other[1], moments_new[1]),
    )


def solution(mesh):
    rows, split = P("fs", None), P("fs", "tp")
    return jax.shard_map(
        on_device,
        mesh=mesh,
        in_specs=(rows, split, split, rows, rows) + (split,) * 6,
        out_specs=(split,) * 4 + (P(None, "tp"),) * 2 + (split,) * 4,
        check_vma=False,
    )
```

time: 114 us -> 100 us (0.88)
  local copies, waits for them, and re-layouts: 12.8 us -> 3.59 us
  matrix products: 8.71 us -> 0 us
  Pallas kernels: 0 us -> 5.4 us
  waiting for transfers between devices: 40.4 us -> 45.2 us
  other arithmetic: 8.28 us -> 3.67 us
  between operations: 2.54 us -> 0.93 us
    dot_general x5 -> x0, matrix products: 8.71 us -> none  [the longest x1 2.25 us: on_device(): mapped = jnp.dot(saved_input, factors, preferred_element_type=jnp.float32)]
    dynamic_update_slice x21 -> x9, local copies, waits for them, and re-layouts: 8.5 us -> 0.2 us  [in_order(): whole = lax.dynamic_update_slice_in_dim(whole, block, (here ^ d) * rows, 0)]
    pallas_call x0 -> x4, Pallas kernels: none -> 5.4 us  [call(): pl.pallas_call(body, out_shape=outs, in_specs=[SMEM if a.dtype == jnp.int...]
    ppermute x34 -> x35, waiting for transfers between devices: 40.4 us -> 45.2 us  [flip(): return lax.ppermute(x, axis, [(i, i ^ bit) for i in range(size)])]
    dynamic_update_slice x4 -> x0, other arithmetic: 2.8 us -> none  [in_order(): whole = lax.dynamic_update_slice_in_dim(whole, block, (here ^ d) * rows, 0)]
    unnamed x26 -> x10, local copies, waits for them, and re-layouts: 1.35 us -> 3.2 us
    select_n x0 -> x1, other arithmetic: none -> 1.17 us  [theirs(): return jnp.where(odd, a, b)]
    ppermute x34 -> x35, starting transfers between devices: 41 us -> 41.3 us  [flip(): return lax.ppermute(x, axis, [(i, i ^ bit) for i in range(size)])]
  transfers between devices with their start and end apart: 34 -> 35, of which waited for: 12 -> 16; matrix products, arithmetic and copies ran while one was open for 21% -> 3% of each run, Pallas kernels for 0% -> 4%
where the time goes in v2:
time: 100 us
  waiting for transfers between devices  45.2 us (45%)
  starting transfers between devices  41.3 us (41%)
  Pallas kernels  5.4 us (5%)
  other arithmetic  3.67 us (4%)
  local copies, waits for them, and re-layouts  3.59 us (4%)
    ppermute x35, waiting for transfers between devices, flip(): return lax.ppermute(x, axis, [(i, i ^ bit) for i in range(size)])  45.2 us
    ppermute x35, starting transfers between devices, flip(): return lax.ppermute(x, axis, [(i, i ^ bit) for i in range(size)])  41.3 us
    pallas_call x4, Pallas kernels, call(): pl.pallas_call(body, out_shape=outs, in_specs=[SMEM if a.dtype == jnp.int...  5.4 us
    unnamed x10, local copies, waits for them, and re-layouts  3.2 us
    select_n x3, other arithmetic, mine(): return jnp.where(odd, b, a)  2.41 us
  transfers between devices with their start and end apart: 35, of which 16 were waited for; matrix products, arithmetic and copies ran while one was open for 3% of the time, Pallas kernels for 4%

profile of v2, /device:TPU:0, one launch (start us, length us, event | category | flops | bytes accessed | tf_op | source)
XLA Modules:
  0.0 100.0 jit_solution(16295399590761497339)
XLA Ops:
  1.6 3.1 %collective-permute-start.1 = (bf16[256,256]{1,0:T(8,128)(2,1)S(1)}, bf16[256,256]{1,0:T(8,128)(2,1)S(1)}, u32[]{:S(2)}, u32[]{:S(2)}) collective-permute-start(bf16[256,256]{1,0:T(8,128)(2,1)S(1)} %broadcast_select_fusion.2.refs_0_.factor_ref), channel_id=1, source_target_pairs={{0,8},{4,12},{8,0},{12,4},{16,24},{20,28},{24,16},{28,20},{1,9},{5... | collective-permute-start | bytes 393224 | tf_op jit(solution)/shard_map/ppermute | solution.py:19
  4.7 2.6 %collective-permute-start.3 = (bf16[256,256]{1,0:T(8,128)(2,1)S(1)}, bf16[256,256]{1,0:T(8,128)(2,1)S(1)}, u32[]{:S(2)}, u32[]{:S(2)}) collective-permute-start(bf16[256,256]{1,0:T(8,128)(2,1)S(1)} %broadcast_select_fusion.2.refs_0_.factor_ref), channel_id=1, source_target_pairs={{0,16},{4,20},{8,24},{12,28},{16,0},{20,4},{24,8},{28,12},{1,17},{... | collective-permute-start | bytes 393224 | tf_op jit(solution)/shard_map/ppermute | solution.py:19
  7.3 1.2 %broadcast_select_fusion = (bf16[768,256]{1,0:T(8,128)(2,1)S(1)}, bf16[768,256]{1,0:T(8,128)(2,1)S(1)}) fusion(bf16[768,256]{1,0:T(8,128)(2,1)} %param.12, bf16[768,256]{1,0:T(8,128)(2,1)} %param.13, pred[]{:T(512)S(6)} %eq.5), kind=kLoop, calls=%fused_computation | loop fusion | flops 393216 | bytes 1572865 | tf_op jit(solution)/shard_map/jit(_where)/select_n | solution.py:169
  8.6 1.8 %collective-permute-start = (bf16[256,256]{1,0:T(8,128)(2,1)S(1)}, bf16[256,256]{1,0:T(8,128)(2,1)S(1)}, u32[]{:S(2)}, u32[]{:S(2)}) collective-permute-start(bf16[256,256]{1,0:T(8,128)(2,1)S(1)} %broadcast_select_fusion.2.refs_0_.factor_ref), channel_id=1, source_target_pairs={{0,4},{4,0},{8,12},{12,8},{16,20},{20,16},{24,28},{28,24},{1,5},{5... | collective-permute-start | bytes 393224 | tf_op jit(solution)/shard_map/ppermute | solution.py:19
  11.5 6.1 %collective-permute-done.3.refs_4_ = bf16[256,256]{1,0:T(8,128)(2,1)S(1)} collective-permute-done((bf16[256,256]{1,0:T(8,128)(2,1)S(1)}, bf16[256,256]{1,0:T(8,128)(2,1)S(1)}, u32[]{:S(2)}, u32[]{:S(2)}) %collective-permute-start.3) | collective-permute-done | bytes 131104 | tf_op jit(solution)/shard_map/ppermute | solution.py:19
  17.6 1.5 %collective-permute-start.4 = (bf16[256,256]{1,0:T(8,128)(2,1)S(1)}, bf16[256,256]{1,0:T(8,128)(2,1)S(1)}, u32[]{:S(2)}, u32[]{:S(2)}) collective-permute-start(bf16[256,256]{1,0:T(8,128)(2,1)S(1)} %collective-permute-done.3.refs_4_), channel_id=1, source_target_pairs={{0,4},{4,0},{8,12},{12,8},{16,20},{20,16},{24,28},{28,24},{1,5},{5... | collective-permute-start | bytes 393224 | tf_op jit(solution)/shard_map/ppermute | solution.py:19
  20.6 2.0 %collective-permute-done.4.refs_5_ = bf16[256,256]{1,0:T(8,128)(2,1)S(1)} collective-permute-done((bf16[256,256]{1,0:T(8,128)(2,1)S(1)}, bf16[256,256]{1,0:T(8,128)(2,1)S(1)}, u32[]{:S(2)}, u32[]{:S(2)}) %collective-permute-start.4) | collective-permute-done | bytes 131104 | tf_op jit(solution)/shard_map/ppermute | solution.py:19
  22.6 1.5 %collective-permute-done.6.refs_7_ = bf16[256,256]{1,0:T(8,128)(2,1)S(1)} collective-permute-done((bf16[256,256]{1,0:T(8,128)(2,1)S(1)}, bf16[256,256]{1,0:T(8,128)(2,1)S(1)}, u32[]{:S(2)}, u32[]{:S(2)}) %collective-permute-start.6) | collective-permute-done | bytes 131104 | tf_op jit(solution)/shard_map/ppermute | solution.py:19
  24.1 1.9 %copy-done = bf16[768,2048]{1,0:T(8,128)(2,1)S(1)} copy-done((bf16[768,2048]{1,0:T(8,128)(2,1)S(1)}, bf16[768,2048]{1,0:T(8,128)(2,1)}, u32[]{:S(2)}) %copy-start) | copy-done | bytes 3145752
  26.0 2.8 %shard_map.187 = f32[8,32,512]{2,1,0:T(8,128)S(1)} custom-call(s32[1]{0:T(128)} %bitcast.1.here_ref, bf16[768,2048]{1,0:T(8,128)(2,1)S(1)} %copy-done, bf16[256,256]{1,0:T(8,128)(2,1)S(1)} %broadcast_select_fusion.2.refs_0_.factor_ref, bf16[256,256]{1,0:T(8,128)(2,1)S(1)} %collective-permute-done.refs_1_, ...), custom_call_target="tpu_custom_call" | custom-call | flops 1409286144 | bytes 4980740 | tf_op jit(solution)/shard_map/pallas_call | solution.py:67
  28.8 1.5 %collective-permute-start.15 = (f32[32,512]{1,0:T(8,128)S(1)}, f32[32,512]{1,0:T(8,128)S(1)}, u32[]{:S(2)}, u32[]{:S(2)}) collective-permute-start(f32[32,512]{1,0:T(8,128)S(1)} %get-tuple-element.32), channel_id=1, source_target_pairs={{0,4},{4,0},{8,12},{12,8},{16,20},{20,16},{24,28},{28,24},{1,5},{5... | collective-permute-start | bytes 196616 | tf_op jit(solution)/shard_map/ppermute | solution.py:19
  31.2 1.2 %collective-permute-start.13 = (f32[32,512]{1,0:T(8,128)S(1)}, f32[32,512]{1,0:T(8,128)S(1)}, u32[]{:S(2)}, u32[]{:S(2)}) collective-permute-start(f32[32,512]{1,0:T(8,128)S(1)} %get-tuple-element.34), channel_id=1, source_target_pairs={{0,12},{4,8},{8,4},{12,0},{16,28},{20,24},{24,20},{28,16},{1,13},{... | collective-permute-start | bytes 196616 | tf_op jit(solution)/shard_map/ppermute | solution.py:19
  32.4 1.5 %collective-permute-start.12 = (f32[32,512]{1,0:T(8,128)S(1)}, f32[32,512]{1,0:T(8,128)S(1)}, u32[]{:S(2)}, u32[]{:S(2)}) collective-permute-start(f32[32,512]{1,0:T(8,128)S(1)} %get-tuple-element.35), channel_id=1, source_target_pairs={{0,16},{4,20},{8,24},{12,28},{16,0},{20,4},{24,8},{28,12},{1,17},{... | collective-permute-start | bytes 196616 | tf_op jit(solution)/shard_map/ppermute | solution.py:19
  33.9 2.3 %collective-permute-start.11 = (f32[32,512]{1,0:T(8,128)S(1)}, f32[32,512]{1,0:T(8,128)S(1)}, u32[]{:S(2)}, u32[]{:S(2)}) collective-permute-start(f32[32,512]{1,0:T(8,128)S(1)} %get-tuple-element.36), channel_id=1, source_target_pairs={{0,20},{4,16},{8,28},{12,24},{16,4},{20,0},{24,12},{28,8},{1,21},{... | collective-permute-start | bytes 196616 | tf_op jit(solution)/shard_map/ppermute | solution.py:19
  36.2 2.7 %collective-permute-start.9 = (f32[32,512]{1,0:T(8,128)S(1)}, f32[32,512]{1,0:T(8,128)S(1)}, u32[]{:S(2)}, u32[]{:S(2)}) collective-permute-start(f32[32,512]{1,0:T(8,128)S(1)} %get-tuple-element.37), channel_id=1, source_target_pairs={{0,28},{4,24},{8,20},{12,16},{16,12},{20,8},{24,4},{28,0},{1,29},{... | collective-permute-start | bytes 196616 | tf_op jit(solution)/shard_map/ppermute | solution.py:19
  38.9 1.2 %collective-permute-start.10 = (f32[32,512]{1,0:T(8,128)S(1)}, f32[32,512]{1,0:T(8,128)S(1)}, u32[]{:S(2)}, u32[]{:S(2)}) collective-permute-start(f32[32,512]{1,0:T(8,128)S(1)} %get-tuple-element.31), channel_id=1, source_target_pairs={{0,24},{4,28},{8,16},{12,20},{16,8},{20,12},{24,0},{28,4},{1,25},{... | collective-permute-start | bytes 196616 | tf_op jit(solution)/shard_map/ppermute | solution.py:19
  41.2 2.7 %collective-permute-done.11 = f32[32,512]{1,0:T(8,128)S(1)} collective-permute-done((f32[32,512]{1,0:T(8,128)S(1)}, f32[32,512]{1,0:T(8,128)S(1)}, u32[]{:S(2)}, u32[]{:S(2)}) %collective-permute-start.11) | collective-permute-done | bytes 65568 | tf_op jit(solution)/shard_map/ppermute | solution.py:19
  43.9 1.2 %collective-permute-done.10 = f32[32,512]{1,0:T(8,128)S(1)} collective-permute-done((f32[32,512]{1,0:T(8,128)S(1)}, f32[32,512]{1,0:T(8,128)S(1)}, u32[]{:S(2)}, u32[]{:S(2)}) %collective-permute-start.10) | collective-permute-done | bytes 65568 | tf_op jit(solution)/shard_map/ppermute | solution.py:19
  45.1 1.6 %collective-permute-start.16 = (f32[32,512]{1,0:T(8,128)S(1)}, f32[32,512]{1,0:T(8,128)S(1)}, u32[]{:S(2)}, u32[]{:S(2)}) collective-permute-start(f32[32,512]{1,0:T(8,128)S(1)} %get-tuple-element.26.refs_0_), channel_id=1, source_target_pairs={{0,4},{4,0},{8,12},{12,8},{16,20},{20,16},{24,28},{28,24},{1,5},{5... | collective-permute-start | bytes 196616 | tf_op jit(solution)/shard_map/ppermute | solution.py:19
  46.7 1.6 %collective-permute-start.19 = (f32[32,512]{1,0:T(8,128)S(1)}, f32[32,512]{1,0:T(8,128)S(1)}, u32[]{:S(2)}, u32[]{:S(2)}) collective-permute-start(f32[32,512]{1,0:T(8,128)S(1)} %get-tuple-element.26.refs_0_), channel_id=1, source_target_pairs={{0,16},{4,20},{8,24},{12,28},{16,0},{20,4},{24,8},{28,12},{1,17},{... | collective-permute-start | bytes 196616 | tf_op jit(solution)/shard_map/ppermute | solution.py:19
  48.3 2.8 %collective-permute-start.21 = (f32[32,512]{1,0:T(8,128)S(1)}, f32[32,512]{1,0:T(8,128)S(1)}, u32[]{:S(2)}, u32[]{:S(2)}) collective-permute-start(f32[32,512]{1,0:T(8,128)S(1)} %get-tuple-element.26.refs_0_), channel_id=1, source_target_pairs={{0,24},{4,28},{8,16},{12,20},{16,8},{20,12},{24,0},{28,4},{1,25},{... | collective-permute-start | bytes 196616 | tf_op jit(solution)/shard_map/ppermute | solution.py:19
  51.9 1.3 %collective-permute-start.20 = (f32[32,512]{1,0:T(8,128)S(1)}, f32[32,512]{1,0:T(8,128)S(1)}, u32[]{:S(2)}, u32[]{:S(2)}) collective-permute-start(f32[32,512]{1,0:T(8,128)S(1)} %collective-permute-done.19.refs_4_), channel_id=1, source_target_pairs={{0,4},{4,0},{8,12},{12,8},{16,20},{20,16},{24,28},{28,24},{1,5},{5... | collective-permute-start | bytes 196616 | tf_op jit(solution)/shard_map/ppermute | solution.py:19
  56.1 2.5 %collective-permute-done.22.refs_7_ = f32[32,512]{1,0:T(8,128)S(1)} collective-permute-done((f32[32,512]{1,0:T(8,128)S(1)}, f32[32,512]{1,0:T(8,128)S(1)}, u32[]{:S(2)}, u32[]{:S(2)}) %collective-permute-start.22) | collective-permute-done | bytes 65568 | tf_op jit(solution)/shard_map/ppermute | solution.py:19
  59.6 1.6 %collective-permute-start.23 = (f32[8,128]{1,0:T(8,128)S(1)}, f32[8,128]{1,0:T(8,128)S(1)}, u32[]{:S(2)}, u32[]{:S(2)}) collective-permute-start(f32[8,128]{1,0:T(8,128)S(1)} %get-tuple-element.18), channel_id=1, source_target_pairs={{0,2},{1,3},{2,0},{3,1},{4,6},{5,7},{6,4},{7,5},{8,10},{9,11},{10,... | collective-permute-start | bytes 12296 | tf_op jit(solution)/shard_map/ppermute | solution.py:19
  63.3 1.6 %collective-permute-done.25 = f32[8,128]{1,0:T(8,128)S(1)} collective-permute-done((f32[8,128]{1,0:T(8,128)S(1)}, f32[8,128]{1,0:T(8,128)S(1)}, u32[]{:S(2)}, u32[]{:S(2)}) %collective-permute-start.25) | collective-permute-done | bytes 4128 | tf_op jit(solution)/shard_map/ppermute | solution.py:19
  67.7 2.2 %collective-permute-start.30 = (bf16[2,256,256]{2,1,0:T(8,128)(2,1)S(1)}, bf16[2,256,256]{2,1,0:T(8,128)(2,1)S(1)}, u32[]{:S(2)}, u32[]{:S(2)}) collective-permute-start(bf16[2,256,256]{2,1,0:T(8,128)(2,1)S(1)} %get-tuple-element.25), channel_id=1, source_target_pairs={{0,16},{4,20},{8,24},{12,28},{16,0},{20,4},{24,8},{28,12},{1,17},{... | collective-permute-start | bytes 786440 | tf_op jit(solution)/shard_map/ppermute | solution.py:19
  71.2 8.7 %collective-permute-done.28 = bf16[2,256,256]{2,1,0:T(8,128)(2,1)S(1)} collective-permute-done((bf16[2,256,256]{2,1,0:T(8,128)(2,1)S(1)}, bf16[2,256,256]{2,1,0:T(8,128)(2,1)S(1)}, u32[]{:S(2)}, u32[]{:S(2)}) %collective-permute-start.28) | collective-permute-done | bytes 262176 | tf_op jit(solution)/shard_map/ppermute | solution.py:19
  79.9 1.5 %collective-permute-start.29 = (bf16[2,256,256]{2,1,0:T(8,128)(2,1)S(1)}, bf16[2,256,256]{2,1,0:T(8,128)(2,1)S(1)}, u32[]{:S(2)}, u32[]{:S(2)}) collective-permute-start(bf16[2,256,256]{2,1,0:T(8,128)(2,1)S(1)} %collective-permute-done.28), channel_id=1, source_target_pairs={{0,4},{4,0},{8,12},{12,8},{16,20},{20,16},{24,28},{28,24},{1,5},{5... | collective-permute-start | bytes 786440 | tf_op jit(solution)/shard_map/ppermute | solution.py:19
  81.4 7.6 %collective-permute-done.30 = bf16[2,256,256]{2,1,0:T(8,128)(2,1)S(1)} collective-permute-done((bf16[2,256,256]{2,1,0:T(8,128)(2,1)S(1)}, bf16[2,256,256]{2,1,0:T(8,128)(2,1)S(1)}, u32[]{:S(2)}, u32[]{:S(2)}) %collective-permute-start.30) | collective-permute-done | bytes 262176 | tf_op jit(solution)/shard_map/ppermute | solution.py:19
  89.0 1.3 %collective-permute-start.31 = (bf16[2,256,256]{2,1,0:T(8,128)(2,1)S(1)}, bf16[2,256,256]{2,1,0:T(8,128)(2,1)S(1)}, u32[]{:S(2)}, u32[]{:S(2)}) collective-permute-start(bf16[2,256,256]{2,1,0:T(8,128)(2,1)S(1)} %collective-permute-done.30), channel_id=1, source_target_pairs={{0,4},{4,0},{8,12},{12,8},{16,20},{20,16},{24,28},{28,24},{1,5},{5... | collective-permute-start | bytes 786440 | tf_op jit(solution)/shard_map/ppermute | solution.py:19
  91.2 4.7 %collective-permute-done.31 = bf16[2,256,256]{2,1,0:T(8,128)(2,1)S(1)} collective-permute-done((bf16[2,256,256]{2,1,0:T(8,128)(2,1)S(1)}, bf16[2,256,256]{2,1,0:T(8,128)(2,1)S(1)}, u32[]{:S(2)}, u32[]{:S(2)}) %collective-permute-start.31) | collective-permute-done | bytes 262176 | tf_op jit(solution)/shard_map/ppermute | solution.py:19
  96.0 2.8 %collective-permute-done.33 = bf16[2,256,256]{2,1,0:T(8,128)(2,1)S(1)} collective-permute-done((bf16[2,256,256]{2,1,0:T(8,128)(2,1)S(1)}, bf16[2,256,256]{2,1,0:T(8,128)(2,1)S(1)}, u32[]{:S(2)}, u32[]{:S(2)}) %collective-permute-start.33) | collective-permute-done | bytes 262176 | tf_op jit(solution)/shard_map/ppermute | solution.py:19
  (76 shorter events, 18.7 us)
Async XLA Ops:
  1.6 8.8 %collective-permute-start.1 = (bf16[256,256]{1,0:T(8,128)(2,1)S(1)}, bf16[256,256]{1,0:T(8,128)(2,1)S(1)}, u32[]{:S(2)}, u32[]{:S(2)}) collective-permute-start(bf16[256,256]{1,0:T(8,128)(2,1)S(1)} %broadcast_select_fusion.2.refs_0_.factor_ref), channel_id=1, source_target_pairs={{0,8},{4,12},{8,0},{12,4},{16,24},{20,28},{24,16},{28,20},{1,9},{5... | collective-permute-start | bytes 393224 | tf_op jit(solution)/shard_map/ppermute | solution.py:19
  4.7 12.9 %collective-permute-start.3 = (bf16[256,256]{1,0:T(8,128)(2,1)S(1)}, bf16[256,256]{1,0:T(8,128)(2,1)S(1)}, u32[]{:S(2)}, u32[]{:S(2)}) collective-permute-start(bf16[256,256]{1,0:T(8,128)(2,1)S(1)} %broadcast_select_fusion.2.refs_0_.factor_ref), channel_id=1, source_target_pairs={{0,16},{4,20},{8,24},{12,28},{16,0},{20,4},{24,8},{28,12},{1,17},{... | collective-permute-start | bytes 393224 | tf_op jit(solution)/shard_map/ppermute | solution.py:19
  7.3 11.8 %collective-permute-start.5 = (bf16[256,256]{1,0:T(8,128)(2,1)S(1)}, bf16[256,256]{1,0:T(8,128)(2,1)S(1)}, u32[]{:S(2)}, u32[]{:S(2)}) collective-permute-start(bf16[256,256]{1,0:T(8,128)(2,1)S(1)} %broadcast_select_fusion.2.refs_0_.factor_ref), channel_id=1, source_target_pairs={{0,24},{4,28},{8,16},{12,20},{16,8},{20,12},{24,0},{28,4},{1,25},{... | collective-permute-start | bytes 393224 | tf_op jit(solution)/shard_map/ppermute | solution.py:19
  8.5 15.6 %collective-permute-start.8 = (bf16[768,256]{1,0:T(8,128)(2,1)S(1)}, bf16[768,256]{1,0:T(8,128)(2,1)S(1)}, u32[]{:S(2)}, u32[]{:S(2)}) collective-permute-start(bf16[768,256]{1,0:T(8,128)(2,1)S(1)} %get-tuple-element.29), channel_id=1, source_target_pairs={{0,1},{1,0},{2,3},{3,2},{4,5},{5,4},{6,7},{7,6},{8,9},{9,8},{10,11... | collective-permute-start | bytes 1179656 | tf_op jit(solution)/shard_map/ppermute | solution.py:19
  8.6 11.9 %collective-permute-start = (bf16[256,256]{1,0:T(8,128)(2,1)S(1)}, bf16[256,256]{1,0:T(8,128)(2,1)S(1)}, u32[]{:S(2)}, u32[]{:S(2)}) collective-permute-start(bf16[256,256]{1,0:T(8,128)(2,1)S(1)} %broadcast_select_fusion.2.refs_0_.factor_ref), channel_id=1, source_target_pairs={{0,4},{4,0},{8,12},{12,8},{16,20},{20,16},{24,28},{28,24},{1,5},{5... | collective-permute-start | bytes 393224 | tf_op jit(solution)/shard_map/ppermute | solution.py:19
  10.4 10.2 %collective-permute-start.2 = (bf16[256,256]{1,0:T(8,128)(2,1)S(1)}, bf16[256,256]{1,0:T(8,128)(2,1)S(1)}, u32[]{:S(2)}, u32[]{:S(2)}) collective-permute-start(bf16[256,256]{1,0:T(8,128)(2,1)S(1)} %collective-permute-done.1.refs_2_), channel_id=1, source_target_pairs={{0,4},{4,0},{8,12},{12,8},{16,20},{20,16},{24,28},{28,24},{1,5},{5... | collective-permute-start | bytes 393224 | tf_op jit(solution)/shard_map/ppermute | solution.py:19
  17.6 5.0 %collective-permute-start.4 = (bf16[256,256]{1,0:T(8,128)(2,1)S(1)}, bf16[256,256]{1,0:T(8,128)(2,1)S(1)}, u32[]{:S(2)}, u32[]{:S(2)}) collective-permute-start(bf16[256,256]{1,0:T(8,128)(2,1)S(1)} %collective-permute-done.3.refs_4_), channel_id=1, source_target_pairs={{0,4},{4,0},{8,12},{12,8},{16,20},{20,16},{24,28},{28,24},{1,5},{5... | collective-permute-start | bytes 393224 | tf_op jit(solution)/shard_map/ppermute | solution.py:19
  19.1 5.0 %collective-permute-start.6 = (bf16[256,256]{1,0:T(8,128)(2,1)S(1)}, bf16[256,256]{1,0:T(8,128)(2,1)S(1)}, u32[]{:S(2)}, u32[]{:S(2)}) collective-permute-start(bf16[256,256]{1,0:T(8,128)(2,1)S(1)} %collective-permute-done.5.refs_6_), channel_id=1, source_target_pairs={{0,4},{4,0},{8,12},{12,8},{16,20},{20,16},{24,28},{28,24},{1,5},{5... | collective-permute-start | bytes 393224 | tf_op jit(solution)/shard_map/ppermute | solution.py:19
  20.5 13.4 %collective-permute-start.7 = (f32[2,32,256]{2,1,0:T(8,128)S(1)}, f32[2,32,256]{2,1,0:T(8,128)S(1)}, u32[]{:S(2)}, u32[]{:S(2)}) collective-permute-start(f32[2,32,256]{2,1,0:T(8,128)S(1)} %pad_maximum_fusion), channel_id=1, source_target_pairs={{0,1},{1,0},{2,3},{3,2},{4,5},{5,4},{6,7},{7,6},{8,9},{9,8},{10,11... | collective-permute-start | bytes 196616 | tf_op jit(solution)/shard_map/ppermute | solution.py:19
  28.8 7.3 %collective-permute-start.15 = (f32[32,512]{1,0:T(8,128)S(1)}, f32[32,512]{1,0:T(8,128)S(1)}, u32[]{:S(2)}, u32[]{:S(2)}) collective-permute-start(f32[32,512]{1,0:T(8,128)S(1)} %get-tuple-element.32), channel_id=1, source_target_pairs={{0,4},{4,0},{8,12},{12,8},{16,20},{20,16},{24,28},{28,24},{1,5},{5... | collective-permute-start | bytes 196616 | tf_op jit(solution)/shard_map/ppermute | solution.py:19
  30.3 8.5 %collective-permute-start.14 = (f32[32,512]{1,0:T(8,128)S(1)}, f32[32,512]{1,0:T(8,128)S(1)}, u32[]{:S(2)}, u32[]{:S(2)}) collective-permute-start(f32[32,512]{1,0:T(8,128)S(1)} %get-tuple-element.33), channel_id=1, source_target_pairs={{0,8},{4,12},{8,0},{12,4},{16,24},{20,28},{24,16},{28,20},{1,9},{5... | collective-permute-start | bytes 196616 | tf_op jit(solution)/shard_map/ppermute | solution.py:19
  31.2 8.9 %collective-permute-start.13 = (f32[32,512]{1,0:T(8,128)S(1)}, f32[32,512]{1,0:T(8,128)S(1)}, u32[]{:S(2)}, u32[]{:S(2)}) collective-permute-start(f32[32,512]{1,0:T(8,128)S(1)} %get-tuple-element.34), channel_id=1, source_target_pairs={{0,12},{4,8},{8,4},{12,0},{16,28},{20,24},{24,20},{28,16},{1,13},{... | collective-permute-start | bytes 196616 | tf_op jit(solution)/shard_map/ppermute | solution.py:19
  32.4 8.8 %collective-permute-start.12 = (f32[32,512]{1,0:T(8,128)S(1)}, f32[32,512]{1,0:T(8,128)S(1)}, u32[]{:S(2)}, u32[]{:S(2)}) collective-permute-start(f32[32,512]{1,0:T(8,128)S(1)} %get-tuple-element.35), channel_id=1, source_target_pairs={{0,16},{4,20},{8,24},{12,28},{16,0},{20,4},{24,8},{28,12},{1,17},{... | collective-permute-start | bytes 196616 | tf_op jit(solution)/shard_map/ppermute | solution.py:19
  33.9 10.0 %collective-permute-start.11 = (f32[32,512]{1,0:T(8,128)S(1)}, f32[32,512]{1,0:T(8,128)S(1)}, u32[]{:S(2)}, u32[]{:S(2)}) collective-permute-start(f32[32,512]{1,0:T(8,128)S(1)} %get-tuple-element.36), channel_id=1, source_target_pairs={{0,20},{4,16},{8,28},{12,24},{16,4},{20,0},{24,12},{28,8},{1,21},{... | collective-permute-start | bytes 196616 | tf_op jit(solution)/shard_map/ppermute | solution.py:19
  36.2 7.7 %collective-permute-start.9 = (f32[32,512]{1,0:T(8,128)S(1)}, f32[32,512]{1,0:T(8,128)S(1)}, u32[]{:S(2)}, u32[]{:S(2)}) collective-permute-start(f32[32,512]{1,0:T(8,128)S(1)} %get-tuple-element.37), channel_id=1, source_target_pairs={{0,28},{4,24},{8,20},{12,16},{16,12},{20,8},{24,4},{28,0},{1,29},{... | collective-permute-start | bytes 196616 | tf_op jit(solution)/shard_map/ppermute | solution.py:19
  38.9 6.2 %collective-permute-start.10 = (f32[32,512]{1,0:T(8,128)S(1)}, f32[32,512]{1,0:T(8,128)S(1)}, u32[]{:S(2)}, u32[]{:S(2)}) collective-permute-start(f32[32,512]{1,0:T(8,128)S(1)} %get-tuple-element.31), channel_id=1, source_target_pairs={{0,24},{4,28},{8,16},{12,20},{16,8},{20,12},{24,0},{28,4},{1,25},{... | collective-permute-start | bytes 196616 | tf_op jit(solution)/shard_map/ppermute | solution.py:19
  45.1 10.3 %collective-permute-start.16 = (f32[32,512]{1,0:T(8,128)S(1)}, f32[32,512]{1,0:T(8,128)S(1)}, u32[]{:S(2)}, u32[]{:S(2)}) collective-permute-start(f32[32,512]{1,0:T(8,128)S(1)} %get-tuple-element.26.refs_0_), channel_id=1, source_target_pairs={{0,4},{4,0},{8,12},{12,8},{16,20},{20,16},{24,28},{28,24},{1,5},{5... | collective-permute-start | bytes 196616 | tf_op jit(solution)/shard_map/ppermute | solution.py:19
  46.7 4.4 %collective-permute-start.17 = (f32[32,512]{1,0:T(8,128)S(1)}, f32[32,512]{1,0:T(8,128)S(1)}, u32[]{:S(2)}, u32[]{:S(2)}) collective-permute-start(f32[32,512]{1,0:T(8,128)S(1)} %get-tuple-element.26.refs_0_), channel_id=1, source_target_pairs={{0,8},{4,12},{8,0},{12,4},{16,24},{20,28},{24,16},{28,20},{1,9},{5... | collective-permute-start | bytes 196616 | tf_op jit(solution)/shard_map/ppermute | solution.py:19
  46.7 5.2 %collective-permute-start.19 = (f32[32,512]{1,0:T(8,128)S(1)}, f32[32,512]{1,0:T(8,128)S(1)}, u32[]{:S(2)}, u32[]{:S(2)}) collective-permute-start(f32[32,512]{1,0:T(8,128)S(1)} %get-tuple-element.26.refs_0_), channel_id=1, source_target_pairs={{0,16},{4,20},{8,24},{12,28},{16,0},{20,4},{24,8},{28,12},{1,17},{... | collective-permute-start | bytes 196616 | tf_op jit(solution)/shard_map/ppermute | solution.py:19
  48.3 6.1 %collective-permute-start.21 = (f32[32,512]{1,0:T(8,128)S(1)}, f32[32,512]{1,0:T(8,128)S(1)}, u32[]{:S(2)}, u32[]{:S(2)}) collective-permute-start(f32[32,512]{1,0:T(8,128)S(1)} %get-tuple-element.26.refs_0_), channel_id=1, source_target_pairs={{0,24},{4,28},{8,16},{12,20},{16,8},{20,12},{24,0},{28,4},{1,25},{... | collective-permute-start | bytes 196616 | tf_op jit(solution)/shard_map/ppermute | solution.py:19
  51.1 4.4 %collective-permute-start.18 = (f32[32,512]{1,0:T(8,128)S(1)}, f32[32,512]{1,0:T(8,128)S(1)}, u32[]{:S(2)}, u32[]{:S(2)}) collective-permute-start(f32[32,512]{1,0:T(8,128)S(1)} %collective-permute-done.17.refs_2_), channel_id=1, source_target_pairs={{0,4},{4,0},{8,12},{12,8},{16,20},{20,16},{24,28},{28,24},{1,5},{5... | collective-permute-start | bytes 196616 | tf_op jit(solution)/shard_map/ppermute | solution.py:19
  51.9 4.3 %collective-permute-start.20 = (f32[32,512]{1,0:T(8,128)S(1)}, f32[32,512]{1,0:T(8,128)S(1)}, u32[]{:S(2)}, u32[]{:S(2)}) collective-permute-start(f32[32,512]{1,0:T(8,128)S(1)} %collective-permute-done.19.refs_4_), channel_id=1, source_target_pairs={{0,4},{4,0},{8,12},{12,8},{16,20},{20,16},{24,28},{28,24},{1,5},{5... | collective-permute-start | bytes 196616 | tf_op jit(solution)/shard_map/ppermute | solution.py:19
  54.3 4.3 %collective-permute-start.22 = (f32[32,512]{1,0:T(8,128)S(1)}, f32[32,512]{1,0:T(8,128)S(1)}, u32[]{:S(2)}, u32[]{:S(2)}) collective-permute-start(f32[32,512]{1,0:T(8,128)S(1)} %collective-permute-done.21.refs_6_), channel_id=1, source_target_pairs={{0,4},{4,0},{8,12},{12,8},{16,20},{20,16},{24,28},{28,24},{1,5},{5... | collective-permute-start | bytes 196616 | tf_op jit(solution)/shard_map/ppermute | solution.py:19
  55.0 6.3 %collective-permute-start.34 = (f32[2,32,256]{2,1,0:T(8,128)S(1)}, f32[2,32,256]{2,1,0:T(8,128)S(1)}, u32[]{:S(2)}, u32[]{:S(2)}) collective-permute-start(f32[2,32,256]{2,1,0:T(8,128)S(1)} %pad_maximum_fusion.1), channel_id=1, source_target_pairs={{0,1},{1,0},{2,3},{3,2},{4,5},{5,4},{6,7},{7,6},{8,9},{9,8},{10,11... | collective-permute-start | bytes 196616 | tf_op jit(solution)/shard_map/ppermute | solution.py:19
  61.2 3.7 %collective-permute-start.26 = (f32[256,256]{1,0:T(8,128)S(1)}, f32[256,256]{1,0:T(8,128)S(1)}, u32[]{:S(2)}, u32[]{:S(2)}) collective-permute-start(f32[256,256]{1,0:T(8,128)S(1)} %get-tuple-element.20), channel_id=1, source_target_pairs={{0,1},{1,0},{2,3},{3,2},{4,5},{5,4},{6,7},{7,6},{8,9},{9,8},{10,11... | collective-permute-start | bytes 786440 | tf_op jit(solution)/shard_map/ppermute | solution.py:19
  66.0 25.0 %collective-permute-start.27 = (bf16[2,256,256]{2,1,0:T(8,128)(2,1)S(1)}, bf16[2,256,256]{2,1,0:T(8,128)(2,1)S(1)}, u32[]{:S(2)}, u32[]{:S(2)}) collective-permute-start(bf16[2,256,256]{2,1,0:T(8,128)(2,1)S(1)} %get-tuple-element.25), channel_id=1, source_target_pairs={{0,4},{4,0},{8,12},{12,8},{16,20},{20,16},{24,28},{28,24},{1,5},{5... | collective-permute-start | bytes 786440 | tf_op jit(solution)/shard_map/ppermute | solution.py:19
  66.6 13.2 %collective-permute-start.28 = (bf16[2,256,256]{2,1,0:T(8,128)(2,1)S(1)}, bf16[2,256,256]{2,1,0:T(8,128)(2,1)S(1)}, u32[]{:S(2)}, u32[]{:S(2)}) collective-permute-start(bf16[2,256,256]{2,1,0:T(8,128)(2,1)S(1)} %get-tuple-element.25), channel_id=1, source_target_pairs={{0,8},{4,12},{8,0},{12,4},{16,24},{20,28},{24,16},{28,20},{1,9},{5... | collective-permute-start | bytes 786440 | tf_op jit(solution)/shard_map/ppermute | solution.py:19
  67.7 21.3 %collective-permute-start.30 = (bf16[2,256,256]{2,1,0:T(8,128)(2,1)S(1)}, bf16[2,256,256]{2,1,0:T(8,128)(2,1)S(1)}, u32[]{:S(2)}, u32[]{:S(2)}) collective-permute-start(bf16[2,256,256]{2,1,0:T(8,128)(2,1)S(1)} %get-tuple-element.25), channel_id=1, source_target_pairs={{0,16},{4,20},{8,24},{12,28},{16,0},{20,4},{24,8},{28,12},{1,17},{... | collective-permute-start | bytes 786440 | tf_op jit(solution)/shard_map/ppermute | solution.py:19
  69.9 20.4 %collective-permute-start.32 = (bf16[2,256,256]{2,1,0:T(8,128)(2,1)S(1)}, bf16[2,256,256]{2,1,0:T(8,128)(2,1)S(1)}, u32[]{:S(2)}, u32[]{:S(2)}) collective-permute-start(bf16[2,256,256]{2,1,0:T(8,128)(2,1)S(1)} %get-tuple-element.25), channel_id=1, source_target_pairs={{0,24},{4,28},{8,16},{12,20},{16,8},{20,12},{24,0},{28,4},{1,25},{... | collective-permute-start | bytes 786440 | tf_op jit(solution)/shard_map/ppermute | solution.py:19
  79.9 11.2 %collective-permute-start.29 = (bf16[2,256,256]{2,1,0:T(8,128)(2,1)S(1)}, bf16[2,256,256]{2,1,0:T(8,128)(2,1)S(1)}, u32[]{:S(2)}, u32[]{:S(2)}) collective-permute-start(bf16[2,256,256]{2,1,0:T(8,128)(2,1)S(1)} %collective-permute-done.28), channel_id=1, source_target_pairs={{0,4},{4,0},{8,12},{12,8},{16,20},{20,16},{24,28},{28,24},{1,5},{5... | collective-permute-start | bytes 786440 | tf_op jit(solution)/shard_map/ppermute | solution.py:19
  89.0 6.9 %collective-permute-start.31 = (bf16[2,256,256]{2,1,0:T(8,128)(2,1)S(1)}, bf16[2,256,256]{2,1,0:T(8,128)(2,1)S(1)}, u32[]{:S(2)}, u32[]{:S(2)}) collective-permute-start(bf16[2,256,256]{2,1,0:T(8,128)(2,1)S(1)} %collective-permute-done.30), channel_id=1, source_target_pairs={{0,4},{4,0},{8,12},{12,8},{16,20},{20,16},{24,28},{28,24},{1,5},{5... | collective-permute-start | bytes 786440 | tf_op jit(solution)/shard_map/ppermute | solution.py:19
  90.3 8.4 %collective-permute-start.33 = (bf16[2,256,256]{2,1,0:T(8,128)(2,1)S(1)}, bf16[2,256,256]{2,1,0:T(8,128)(2,1)S(1)}, u32[]{:S(2)}, u32[]{:S(2)}) collective-permute-start(bf16[2,256,256]{2,1,0:T(8,128)(2,1)S(1)} %collective-permute-done.32), channel_id=1, source_target_pairs={{0,4},{4,0},{8,12},{12,8},{16,20},{20,16},{24,28},{28,24},{1,5},{5... | collective-permute-start | bytes 786440 | tf_op jit(solution)/shard_map/ppermute | solution.py:19
  (8 other events, 85.5 us)

commit v3 on v0

--- a/solution.py
+++ b/solution.py
@@ -1,7 +1,253 @@
+import functools
+
 import jax
 import jax.numpy as jnp
 from jax import lax
+from jax.experimental import pallas as pl
+from jax.experimental.pallas import tpu as pltpu
 from jax.sharding import PartitionSpec as P
+
+HIGHEST = lax.Precision.HIGHEST
+VMEM = pl.BlockSpec(memory_space=pltpu.VMEM)
+HBM = pl.BlockSpec(memory_space=pltpu.HBM)
+VMEM_BYTES = 16 * 2**20
+ROWS = (((0,), (0,)), ((), ()))
+
+
+def send(x, axis, bit):
+    size = lax.axis_size(axis)
+    return lax.ppermute(x, axis, [(i, i ^ bit) for i in range(size)])
+
+
+def thirds(x):
+    high = x.astype(jnp.bfloat16)
+    rest = x - high.astype(jnp.float32)
+    middle = rest.astype(jnp.bfloat16)
+    low = (rest - middle.astype(jnp.float32)).astype(jnp.bfloat16)
+    return high, middle, low
+
+
+def exact_dot(left, right, dims=(((1,), (0,)), ((), ()))):
+    wide = left.dtype == jnp.float32
+    total = None
+    for part in thirds(left if wide else right)[::-1]:
+        pair = (part, right) if wide else (left, part)
+        term = lax.dot_general(*pair, dims, preferred_element_type=jnp.float32)
+        total = term if total is None else total + term
+    return total
+
+
+def call(body, outs, *args, scratch=(), flops, hbm=(), out=VMEM, aliases={}):
+    size = sum(a.size * a.dtype.itemsize for a in args)
+    args = [
+        pltpu.with_memory_space_constraint(a, pltpu.HBM) if k in hbm else a
+        for k, a in enumerate(args)
+    ]
+    return pl.pallas_call(
+        body,
+        out_shape=outs,
+        in_specs=[HBM if k in hbm else VMEM for k in range(len(args))],
+        out_specs=jax.tree.map(lambda _: out, outs),
+        scratch_shapes=list(scratch),
+        input_output_aliases=aliases,
+        compiler_params=pltpu.CompilerParams(vmem_limit_bytes=VMEM_BYTES),
+        cost_estimate=pl.CostEstimate(flops=flops, bytes_accessed=size, transcendentals=0),
+    )(*args)
+
+
+def is_odd():
+    return lax.axis_index("tp") % 2 == 1
+
+
+def slot(d, rows):
+    return pl.ds(pl.multiple_of((lax.axis_index("fs") ^ d) * rows, rows), rows)
+
+
+def copy_all(copies):
+    for copy in copies:
+        copy.start()
+    for copy in copies:
+        copy.wait()
+
+
+def pick_body(even, odd, out, sem):
+    @pl.when(is_odd())
+    def _():
+        copy_all([pltpu.make_async_copy(odd, out, sem)])
+
+    @pl.when(jnp.logical_not(is_odd()))
+    def _():
+        copy_all([pltpu.make_async_copy(even, out, sem)])
+
+
+def picked_body(cots, firsts, seconds, factors, weights, cot, moments, factor, both, w4a, w4b, sems):
+    depth = factor.shape[0]
+    half = w4b.shape[0]
+
+    def copies(k):
+        pairs = (
+            (cots[k], cot),
+            (firsts[k], moments.at[0]),
+            (seconds[k], moments.at[1]),
+            (factors[k], factor),
+            (weights[0], both.at[0]),
+            (weights[1], both.at[1]),
+            (weights[0], w4a.at[pl.ds(0, depth), :]),
+            (weights[1].at[pl.ds(0, depth - half), :], w4a.at[pl.ds(depth, depth - half), :]),
+            (weights[1].at[pl.ds(depth - half, half), :], w4b),
+        )
+        return [pltpu.make_async_copy(*pair, sems.at[i]) for i, pair in enumerate(pairs)]
+
+    @pl.when(is_odd())
+    def _():
+        copy_all(copies(0))
+
+    @pl.when(jnp.logical_not(is_odd()))
+    def _():
+        copy_all(copies(1))
+
+
+def fetch(saved_ref, held, sems, numbers):
+    copies = [
+        pltpu.make_async_copy(saved_ref.at[:, slot(d, held.shape[2])], held.at[k], sems.at[k])
+        for k, d in enumerate(numbers)
+    ]
+    for copy in copies:
+        copy.start()
+    return copies
+
+
+def add_blocks(total, copies, held, factors):
+    for k, (copy, factor) in enumerate(zip(copies, factors, strict=True)):
+        copy.wait()
+        total = total + jnp.dot(held[k], factor[...], preferred_element_type=jnp.float32)
+    return total
+
+
+def map_body(numbers, saved_ref, *refs):
+    factors, (mapped_ref, held, sems) = refs[:-3], refs[-3:]
+    copies = fetch(saved_ref, held, sems, numbers)
+    mapped_ref[...] = add_blocks(jnp.zeros(mapped_ref.shape, jnp.float32), copies, held, factors)
+
+
+def term_body(size, numbers, saved_ref, mapped_ref, *refs):
+    factors, refs = refs[: len(numbers)], refs[len(numbers) :]
+    cot_in, cot_out, peer, far, near, own, held, cot, sems, cot_sem = refs
+    copies = fetch(saved_ref, held, sems, numbers)
+
+    @pl.when(is_odd())
+    def _():
+        pltpu.make_async_copy(cot_out, cot, cot_sem).start()
+
+    @pl.when(jnp.logical_not(is_odd()))
+    def _():
+        pltpu.make_async_copy(cot_in, cot, cot_sem).start()
+
+    mapped = add_blocks(mapped_ref[...], copies, held, factors)
+    columns = cot.shape[1]
+    rows = mapped.shape[1] // size
+    here = lax.axis_index("fs")
+    pltpu.make_async_copy(cot_in, cot, cot_sem).wait()
+    for side, right in enumerate((cot, peer)):
+        term = exact_dot(mapped, right[...], ROWS)
+        at = slice(side * columns, (side + 1) * columns)
+        for k in range(size):
+            own[here ^ k, :, at] = term[k * rows : (k + 1) * rows, :]
+    for ref, first in ((far, 7), (near, 3)):
+        ref[0] = own[first]
+        ref[1] = own[first - 2]
+
+
+def add_body(own, far, a4, a6):
+    a4[...] = own[4] + far[1]
+    a6[...] = own[6] + far[0]
+
+
+def add_near_body(own, near, a2):
+    a2[...] = own[2] + near[0]
+
+
+def moments_body(own, near, r4, r6, r2, f_in, f_out, s_in, s_out, peer, small, mine, other):
+    odd = is_odd()
+    projected = own[0] + near[1] + r4[...] + r6[...] + r2[...]
+    columns = f_in.shape[1]
+    pairs = (
+        (jnp.where(odd, f_out[...], f_in[...]), jnp.where(odd, s_out[...], s_in[...]), mine),
+        (peer[0], peer[1], other),
+    )
+    for side, (first, second, new) in enumerate(pairs):
+        at = slice(side * columns, (side + 1) * columns)
+        x = projected[:, at]
+        first_new = 0.8 * first + 0.2 * x
+        second_new = 0.9 * second + 0.1 * x * x
+        new[0] = first_new
+        new[1] = second_new
+        small[:, at] = first_new / (jnp.sqrt(second_new) + 1e-08)
+
+
+def square_body(size, *refs):
+    factors, (square_ref, held) = refs[:size], refs[size:]
+    for d, factor in enumerate(factors):
+        held[slot(d, factor.shape[0]), :] = factor[...]
+    square_ref[...] = lax.dot_general(
+        held[...], held[...], ROWS, preferred_element_type=jnp.float32
+    )
+
+
+def sum_body(size, square_ref, *refs):
+    smalls, (sum_ref, mine_ref, other_ref) = refs[:size], refs[size:]
+    columns = mine_ref.shape[1]
+    for d, small in enumerate(smalls):
+        at = slot(d, small.shape[0])
+        mine_ref[at, :] = small[:, :columns]
+        other_ref[at, :] = small[:, columns:]
+    product = sum(
+        ref[...] * jnp.dot(square_ref[...], ref[...], precision=HIGHEST)
+        for ref in (mine_ref, other_ref)
+    )
+    sum_ref[...] = jnp.full(sum_ref.shape, jnp.sum(product), jnp.float32)
+
+
+def full_body(small_ref, *refs):
+    small, full_ref = thirds(small_ref[...])[::-1], refs[-1]
+    for k, factor in enumerate(refs[:-1]):
+        full_ref[k] = sum(
+            jnp.dot(factor[...], part, preferred_element_type=jnp.float32) for part in small
+        )
+
+
+def finish_body(entries, sums, full_ref, other_ref, weights, news, back, outs):
+    odd = is_odd()
+    up_in, up_out, new_in, new_out, copies, firsts, seconds = outs
+
+    def scale(pair):
+        mean = jnp.maximum(pair[0][...] + pair[1][...], 0.0) / entries
+        return (1.0 / jnp.sqrt(mean + 1e-06))[0:1, 0:1]
+
+    scales = scale(sums[:2]), scale(sums[2:])
+    for k, (copy, both) in enumerate(zip(copies, weights, strict=True)):
+        update = full_ref[k] * scales[0]
+        update_other = other_ref[k] * scales[1]
+        for p, weight in enumerate(both):
+            chosen = jnp.where(odd, update, update_other) if p else jnp.where(odd, update_other, update)
+            fresh = weight() - 0.02 * chosen
+            copy[p] = fresh.astype(jnp.bfloat16)
+            if k == 0:
+                (new_out if p else new_in)[...] = fresh
+                (up_out if p else up_in)[...] = chosen
+    for k, pair in enumerate((firsts, seconds)):
+        pair[0][...] = jnp.where(odd, back[k], news[k])
+        pair[1][...] = jnp.where(odd, news[k], back[k])
+
+
+def place_body(numbers, *refs):
+    blocks, (copy_in, copy_out, sems) = refs[: len(numbers)], refs[-3:]
+    copies = []
+    for k, (d, block) in enumerate(zip(numbers, blocks, strict=True)):
+        for p, whole in enumerate((copy_in, copy_out)):
+            rows = whole.at[slot(d, block.shape[1]), :]
+            copies.append(pltpu.make_async_copy(block.at[p], rows, sems.at[2 * k + p]))
+    copy_all(copies)
 
 
 def contract_rows(left, right, precision):
@@ -14,7 +260,7 @@
     )
 
 
-def on_device(
+def general(
     saved_input,
     cot_inproj,
     cot_outproj,
@@ -80,34 +326,209 @@
     )
 
 
+def pairwise(
+    saved_input,
+    cot_inproj,
+    cot_outproj,
+    factor_inproj,
+    factor_outproj,
+    weight_inproj,
+    weight_outproj,
+    first_inproj,
+    first_outproj,
+    second_inproj,
+    second_outproj,
+):
+    size, split = lax.axis_size("fs"), lax.axis_size("tp")
+    f32 = functools.partial(jax.ShapeDtypeStruct, dtype=jnp.float32)
+    depth, rank = factor_inproj.shape
+    tokens, columns = cot_inproj.shape
+    rows = rank // size
+    like = jax.ShapeDtypeStruct
+    dma = pltpu.SemaphoreType.DMA
+
+    factor = call(
+        pick_body,
+        like((depth, rank), factor_inproj.dtype),
+        factor_inproj,
+        factor_outproj,
+        scratch=[dma],
+        hbm=range(2),
+        flops=depth * rank,
+    )
+    f4 = send(factor, "fs", 4)
+    f2 = send(factor, "fs", 2)
+    f1 = send(factor, "fs", 1)
+    half = depth // 2
+
+    def picked(c0, c1, f0, f1, s0, s1, g0, g1, w0, w1, *rest):
+        picked_body((c0, c1), (f0, f1), (s0, s1), (g0, g1), (w0, w1), *rest)
+
+    cot_theirs, moments_theirs, factor_theirs, both, early4, late4 = call(
+        picked,
+        (
+            like((tokens, columns), cot_inproj.dtype),
+            f32((2, rows, columns)),
+            like((depth, rank), factor_inproj.dtype),
+            f32((2, depth, columns)),
+            f32((2 * depth - half, columns)),
+            f32((half, columns)),
+        ),
+        *(cot_inproj, cot_outproj, first_inproj, first_outproj, second_inproj, second_outproj),
+        *(factor_inproj, factor_outproj, weight_inproj, weight_outproj),
+        scratch=[dma((9,))],
+        hbm=range(10),
+        flops=tokens * columns,
+    )
+    cot_peer = send(cot_theirs, "tp", 1)
+    f3 = send(f2, "fs", 1)
+    f6 = send(f4, "fs", 2)
+    w4a = send(early4, "fs", 4)
+    f5 = send(f4, "fs", 1)
+    f7 = send(f6, "fs", 1)
+    w2in = send(weight_inproj, "fs", 2)
+    w2out = send(weight_outproj, "fs", 2)
+    early, late = (0, 1, 2, 4), (3, 5, 6, 7)
+    factors = (factor, f1, f2, f3, f4, f5, f6, f7)
+    mapped = call(
+        functools.partial(map_body, early),
+        f32((tokens, rank)),
+        saved_input,
+        *(factors[k] for k in early),
+        scratch=[pltpu.VMEM((len(early), tokens, depth), saved_input.dtype), dma((len(early),))],
+        hbm=(0,),
+        flops=2 * tokens * rank * depth * len(early),
+    )
+    pair = f32((2, rows, 2 * columns))
+    far, near, own = call(
+        functools.partial(term_body, size, late),
+        (pair, pair, f32((size, rows, 2 * columns))),
+        saved_input,
+        mapped,
+        *(factors[k] for k in late),
+        cot_inproj,
+        cot_outproj,
+        cot_peer,
+        scratch=[
+            pltpu.VMEM((len(late), tokens, depth), saved_input.dtype),
+            pltpu.VMEM((tokens, columns), cot_inproj.dtype),
+            dma((len(late),)),
+            dma,
+        ],
+        hbm=(0, 2 + len(late), 3 + len(late)),
+        flops=2 * tokens * rank * (depth * len(late) + 6 * columns),
+    )
+    square = call(
+        functools.partial(square_body, size),
+        f32((rank, rank)),
+        *factors,
+        scratch=[pltpu.VMEM((depth * size, rank), factor.dtype)],
+        flops=2 * rank * rank * depth * size,
+    )
+
+    rfar = send(far, "fs", 1)
+    rnear = send(near, "fs", 1)
+    w1 = send(both, "fs", 1)
+    block = f32((rows, 2 * columns))
+    a4, a6 = call(add_body, (block, block), own, rfar, flops=2 * rows * columns)
+    a2 = call(add_near_body, block, own, rnear, flops=rows * columns)
+    r4 = send(a4, "fs", 4)
+    r6 = send(a6, "fs", 6)
+    r2 = send(a2, "fs", 2)
+    peer = send(moments_theirs, "tp", 1)
+    g1, g2, g4 = send(f1, "tp", 1), send(f2, "tp", 1), send(f4, "tp", 1)
+    halves = f32((2, rows, columns))
+    small, news, others_news = call(
+        moments_body,
+        (block, halves, halves),
+        *(own, rnear, r4, r6, r2),
+        *(first_inproj, first_outproj, second_inproj, second_outproj, peer),
+        flops=30 * rows * columns,
+    )
+
+    s4 = send(small, "fs", 4)
+    s2 = send(small, "fs", 2)
+    s1 = send(small, "fs", 1)
+    s6 = send(s4, "fs", 2)
+    s3 = send(s2, "fs", 1)
+    s5 = send(s4, "fs", 1)
+    s7 = send(s6, "fs", 1)
+    w4b = send(late4, "fs", 4)
+    back = send(others_news, "tp", 1)
+    total, small_mine, small_other = call(
+        functools.partial(sum_body, size),
+        (f32((8, 128)), f32((rank, columns)), f32((rank, columns))),
+        square,
+        *(small, s1, s2, s3, s4, s5, s6, s7),
+        flops=2 * rank * 2 * columns * 6 * rank,
+    )
+    sums = [total] + [send(total, "tp", k) for k in (2, 3, 1)]
+    small_other = send(small_other, "tp", 1)
+    fours, flops = f32((4, depth, columns)), 2 * rank * columns * 12 * depth
+    full = call(full_body, fours, small_mine, *(factor, f1, f2, f4), flops=flops)
+    full_other = call(full_body, fours, small_other, *(factor_theirs, g1, g2, g4), flops=flops)
+    entries = float(depth * size * columns * split)
+
+    def finish(t, n2, n3, n1, full_ref, other_ref, w_in, w_out, w1, w2in, w2out, w4a, w4b, *refs):
+        weights = (
+            (lambda: w_in[...], lambda: w_out[...]),
+            (lambda: w1[0], lambda: w1[1]),
+            (lambda: w2in[...], lambda: w2out[...]),
+            (
+                lambda: w4a[:depth, :],
+                lambda: jnp.concatenate([w4a[depth:, :], w4b[...]], axis=0),
+            ),
+        )
+        news_ref, back_ref, *refs = refs
+        outs = (*refs[:4], refs[4:8], refs[8:10], refs[10:12])
+        sums = (t, n2, n1, n3)
+        finish_body(entries, sums, full_ref, other_ref, weights, news_ref, back_ref, outs)
+
+    shard, copy = f32((depth, columns)), like((2, depth, columns), jnp.bfloat16)
+    outs = call(
+        finish,
+        (shard,) * 4 + (copy,) * 4 + (f32((rows, columns)),) * 4,
+        *sums,
+        full,
+        full_other,
+        *(weight_inproj, weight_outproj, w1, w2in, w2out, w4a, w4b, news, back),
+        flops=40 * depth * columns,
+    )
+    c0, c1, c2, c4 = outs[4:8]
+    c6 = send(c4, "fs", 2)
+    c5 = send(c4, "fs", 1)
+    c7 = send(c6, "fs", 1)
+    c3 = send(c1, "fs", 2)
+    whole = like((depth * size, columns), jnp.bfloat16)
+    copies = (whole, whole)
+    for numbers, blocks in (((0, 1, 2, 4, 5, 6), (c0, c1, c2, c4, c5, c6)), ((3, 7), (c3, c7))):
+        count = len(numbers)
+        first = copies[0] is whole
+        copies = call(
+            functools.partial(place_body, numbers),
+            (whole, whole),
+            *blocks,
+            *(() if first else copies),
+            scratch=[dma((2 * count,))],
+            hbm=() if first else (count, count + 1),
+            out=HBM,
+            aliases={} if first else {count: 0, count + 1: 1},
+            flops=depth * columns,
+        )
+    return (*outs[:4], *copies, *outs[8:])
+
+
+def layer(*args):
+    return pairwise(*args)
+
+
 def solution(mesh):
+    rows, split = P("fs", None), P("fs", "tp")
+    paired = mesh.shape["fs"] == 8 and mesh.shape["tp"] == 4
     return jax.shard_map(
-        on_device,
+        layer if paired else general,
         mesh=mesh,
-        in_specs=(
-            P("fs", None),
-            P("fs", "tp"),
-            P("fs", "tp"),
-            P("fs", None),
-            P("fs", None),
-            P("fs", "tp"),
-            P("fs", "tp"),
-            P("fs", "tp"),
-            P("fs", "tp"),
-            P("fs", "tp"),
-            P("fs", "tp"),
-        ),
-        out_specs=(
-            P("fs", "tp"),
-            P("fs", "tp"),
-            P("fs", "tp"),
-            P("fs", "tp"),
-            P(None, "tp"),
-            P(None, "tp"),
-            P("fs", "tp"),
-            P("fs", "tp"),
-            P("fs", "tp"),
-            P("fs", "tp"),
-        ),
+        in_specs=(rows, split, split, rows, rows) + (split,) * 6,
+        out_specs=(split,) * 4 + (P(None, "tp"),) * 2 + (split,) * 4,
         check_vma=False,
     )

time: 390 us -> 110 us (0.28)
  waiting for transfers between devices: 242 us -> 52.4 us
  blocking collectives: 99.7 us -> 0 us
  starting transfers between devices: 0.24 us -> 42.3 us
  between operations: 15.6 us -> 0.89 us
  Pallas kernels: 0 us -> 14 us
  local copies, waits for them, and re-layouts: 13.6 us -> 0.04 us
  matrix products: 11.8 us -> 0 us
  other arithmetic: 6.5 us -> 0 us
    all_gather x4 -> x0, waiting for transfers between devices: 148 us -> none  [the longest x1 43.4 us: on_device(): lax.all_gather(factor_inproj, 'fs', axis=0, tiled=True)]
    reduce_scatter x2 -> x0, waiting for transfers between devices: 91.7 us -> none  [the longest x1 60.9 us: on_device(): lax.psum_scatter(term_in, 'fs', scatter_dimension=0, tiled=True)]
    all_gather x2 -> x0, blocking collectives: 61.8 us -> none  [the longest x1 30.9 us: on_device(): lax.all_gather(small_in, 'fs', axis=0, tiled=True)]
    ppermute x0 -> x38, waiting for transfers between devices: none -> 52.4 us  [send(): return lax.ppermute(x, axis, [(i, i ^ bit) for i in range(size)])]
    ppermute x0 -> x38, starting transfers between devices: none -> 42.3 us  [send(): return lax.ppermute(x, axis, [(i, i ^ bit) for i in range(size)])]
    psum x1 -> x0, blocking collectives: 37.9 us -> none  [on_device(): lax.psum((jnp.sum(full_in * full_in), jnp.sum(full_out * full_out)), ('fs...]
    pallas_call x0 -> x14, Pallas kernels: none -> 14 us  [call(): pl.pallas_call(body, out_shape=outs, in_specs=[HBM if k in hbm else VMEM...]
    unnamed x16 -> x12, local copies, waits for them, and re-layouts: 13.6 us -> 0.04 us
  transfers between devices with their start and end apart: 6 -> 38, of which waited for: 6 -> 20; matrix products, arithmetic and copies ran while one was open for 6% -> 0% of each run, Pallas kernels for 0% -> 7%
where the time goes in v3:
time: 110 us
  waiting for transfers between devices  52.4 us (48%)
  starting transfers between devices  42.3 us (38%)
  Pallas kernels  14 us (13%)
    ppermute x38, waiting for transfers between devices, send(): return lax.ppermute(x, axis, [(i, i ^ bit) for i in range(size)])  52.4 us
    ppermute x38, starting transfers between devices, send(): return lax.ppermute(x, axis, [(i, i ^ bit) for i in range(size)])  42.3 us
    pallas_call x14, Pallas kernels, call(): pl.pallas_call(body, out_shape=outs, in_specs=[HBM if k in hbm else VMEM...  14 us
  transfers between devices with their start and end apart: 38, of which 20 were waited for; matrix products, arithmetic and copies ran while one was open for 0% of the time, Pallas kernels for 7%

profile of v3, /device:TPU:0, one launch (start us, length us, event | category | flops | bytes accessed | tf_op | source)
XLA Modules:
  0.0 109.6 jit_solution(7921832748836915244)
XLA Ops:
  1.6 4.1 %collective-permute-start.3 = (bf16[256,256]{1,0:T(8,128)(2,1)S(1)}, bf16[256,256]{1,0:T(8,128)(2,1)S(1)}, u32[]{:S(2)}, u32[]{:S(2)}) collective-permute-start(bf16[256,256]{1,0:T(8,128)(2,1)S(1)} %shard_map.186.refs_0_), channel_id=1, source_target_pairs={{0,16},{4,20},{8,24},{12,28},{16,0},{20,4},{24,8},{28,12},{1,17},{... | collective-permute-start | bytes 393224 | tf_op jit(solution)/shard_map/ppermute | solution.py:19
  5.7 1.5 %shard_map.189 = (bf16[768,256]{1,0:T(8,128)(2,1)S(1)}, f32[2,32,256]{2,1,0:T(8,128)S(1)}, bf16[256,256]{1,0:T(8,128)(2,1)S(1)}, f32[2,256,256]{2,1,0:T(8,128)S(...) custom-call(bf16[768,256]{1,0:T(8,128)(2,1)} %refs_4_.1, bf16[768,256]{1,0:T(8,128)(2,1)} %refs_5_.1, f32[32,256]{1,0:T(8,128)} %f_in.1, ...), custom_call_target="tpu_custom_call" | custom-call | flops 196608 | bytes 1703936 | tf_op jit(solution)/shard_map/pallas_call | solution.py:46
  7.3 1.6 %collective-permute-start.1 = (bf16[256,256]{1,0:T(8,128)(2,1)S(1)}, bf16[256,256]{1,0:T(8,128)(2,1)S(1)}, u32[]{:S(2)}, u32[]{:S(2)}) collective-permute-start(bf16[256,256]{1,0:T(8,128)(2,1)S(1)} %shard_map.186.refs_0_), channel_id=1, source_target_pairs={{0,8},{4,12},{8,0},{12,4},{16,24},{20,28},{24,16},{28,20},{1,9},{5... | collective-permute-start | bytes 393224 | tf_op jit(solution)/shard_map/ppermute | solution.py:19
  8.9 3.2 %collective-permute-done.3.refs_4_.refs_3_ = bf16[256,256]{1,0:T(8,128)(2,1)S(1)} collective-permute-done((bf16[256,256]{1,0:T(8,128)(2,1)S(1)}, bf16[256,256]{1,0:T(8,128)(2,1)S(1)}, u32[]{:S(2)}, u32[]{:S(2)}) %collective-permute-start.3) | collective-permute-done | bytes 131104 | tf_op jit(solution)/shard_map/ppermute | solution.py:19
  12.8 1.5 %collective-permute-start = (bf16[256,256]{1,0:T(8,128)(2,1)S(1)}, bf16[256,256]{1,0:T(8,128)(2,1)S(1)}, u32[]{:S(2)}, u32[]{:S(2)}) collective-permute-start(bf16[256,256]{1,0:T(8,128)(2,1)S(1)} %shard_map.186.refs_0_), channel_id=1, source_target_pairs={{0,4},{4,0},{8,12},{12,8},{16,20},{20,16},{24,28},{28,24},{1,5},{5... | collective-permute-start | bytes 393224 | tf_op jit(solution)/shard_map/ppermute | solution.py:19
  14.9 1.6 %collective-permute-start.2 = (bf16[256,256]{1,0:T(8,128)(2,1)S(1)}, bf16[256,256]{1,0:T(8,128)(2,1)S(1)}, u32[]{:S(2)}, u32[]{:S(2)}) collective-permute-start(bf16[256,256]{1,0:T(8,128)(2,1)S(1)} %collective-permute-done.1.refs_2_), channel_id=1, source_target_pairs={{0,4},{4,0},{8,12},{12,8},{16,20},{20,16},{24,28},{28,24},{1,5},{5... | collective-permute-start | bytes 393224 | tf_op jit(solution)/shard_map/ppermute | solution.py:19
  17.5 1.7 %collective-permute-start.6 = (bf16[256,256]{1,0:T(8,128)(2,1)S(1)}, bf16[256,256]{1,0:T(8,128)(2,1)S(1)}, u32[]{:S(2)}, u32[]{:S(2)}) collective-permute-start(bf16[256,256]{1,0:T(8,128)(2,1)S(1)} %collective-permute-done.5.refs_6_.refs_2_), channel_id=1, source_target_pairs={{0,4},{4,0},{8,12},{12,8},{16,20},{20,16},{24,28},{28,24},{1,5},{5... | collective-permute-start | bytes 393224 | tf_op jit(solution)/shard_map/ppermute | solution.py:19
  19.1 2.3 %shard_map.188.mapped_ref = f32[768,256]{1,0:T(8,128)S(1)} custom-call(bf16[768,2048]{1,0:T(8,128)(2,1)} %saved_ref.3, bf16[256,256]{1,0:T(8,128)(2,1)S(1)} %shard_map.186.refs_0_, bf16[256,256]{1,0:T(8,128)(2,1)S(1)} %collective-permute-done.refs_1_, bf16[256,256]{1,0:T(8,128)(2,1)S(1)} %collective-permute-done.1.refs_2_, ...), custom_call_target="tpu_custom_call" | custom-call | flops 402653184 | bytes 3670016 | tf_op jit(solution)/shard_map/pallas_call | solution.py:46
  22.0 2.8 %collective-permute-done.2.refs_3_.refs_0_ = bf16[256,256]{1,0:T(8,128)(2,1)S(1)} collective-permute-done((bf16[256,256]{1,0:T(8,128)(2,1)S(1)}, bf16[256,256]{1,0:T(8,128)(2,1)S(1)}, u32[]{:S(2)}, u32[]{:S(2)}) %collective-permute-start.2) | collective-permute-done | bytes 131104 | tf_op jit(solution)/shard_map/ppermute | solution.py:19
  24.8 1.6 %collective-permute-done.6.refs_7_.refs_3_ = bf16[256,256]{1,0:T(8,128)(2,1)S(1)} collective-permute-done((bf16[256,256]{1,0:T(8,128)(2,1)S(1)}, bf16[256,256]{1,0:T(8,128)(2,1)S(1)}, u32[]{:S(2)}, u32[]{:S(2)}) %collective-permute-start.6) | collective-permute-done | bytes 131104 | tf_op jit(solution)/shard_map/ppermute | solution.py:19
  26.3 3.3 %shard_map.190 = (f32[2,32,512]{2,1,0:T(8,128)S(1)}, f32[2,32,512]{2,1,0:T(8,128)S(1)}, f32[8,32,512]{2,1,0:T(8,128)S(1)}) custom-call(bf16[768,2048]{1,0:T(8,128)(2,1)} %saved_ref.3, f32[768,256]{1,0:T(8,128)S(1)} %shard_map.188.mapped_ref, bf16[256,256]{1,0:T(8,128)(2,1)S(1)} %collective-permute-done.2.refs_3_.refs_0_, ...), custom_call_target="tpu_custom_call" | custom-call | flops 1006632960 | bytes 5636096 | tf_op jit(solution)/shard_map/pallas_call | solution.py:46
  29.7 1.6 %collective-permute-start.8 = (f32[2,32,512]{2,1,0:T(8,128)S(1)}, f32[2,32,512]{2,1,0:T(8,128)S(1)}, u32[]{:S(2)}, u32[]{:S(2)}) collective-permute-start(f32[2,32,512]{2,1,0:T(8,128)S(1)} %get-tuple-element.45), channel_id=1, source_target_pairs={{0,4},{4,0},{8,12},{12,8},{16,20},{20,16},{24,28},{28,24},{1,5},{5... | collective-permute-start | bytes 393224 | tf_op jit(solution)/shard_map/ppermute | solution.py:19
  31.8 3.7 %collective-permute-done.8.near = f32[2,32,512]{2,1,0:T(8,128)S(1)} collective-permute-done((f32[2,32,512]{2,1,0:T(8,128)S(1)}, f32[2,32,512]{2,1,0:T(8,128)S(1)}, u32[]{:S(2)}, u32[]{:S(2)}) %collective-permute-start.8) | collective-permute-done | bytes 131104 | tf_op jit(solution)/shard_map/ppermute | solution.py:19
  35.5 3.9 %collective-permute-start.32 = (f32[128,256]{1,0:T(8,128)S(1)}, f32[128,256]{1,0:T(8,128)S(1)}, u32[]{:S(2)}, u32[]{:S(2)}) collective-permute-start(f32[128,256]{1,0:T(8,128)S(1)} %get-tuple-element.57), channel_id=1, source_target_pairs={{0,16},{4,20},{8,24},{12,28},{16,0},{20,4},{24,8},{28,12},{1,17},{... | collective-permute-start | bytes 393224 | tf_op jit(solution)/shard_map/ppermute | solution.py:19
  40.3 3.1 %collective-permute-start.11 = (f32[32,512]{1,0:T(8,128)S(1)}, f32[32,512]{1,0:T(8,128)S(1)}, u32[]{:S(2)}, u32[]{:S(2)}) collective-permute-start(f32[32,512]{1,0:T(8,128)S(1)} %get-tuple-element.48), channel_id=1, source_target_pairs={{0,24},{4,28},{8,16},{12,20},{16,8},{20,12},{24,0},{28,4},{1,25},{... | collective-permute-start | bytes 196616 | tf_op jit(solution)/shard_map/ppermute | solution.py:19
  43.3 4.9 %collective-permute-done.10.r4 = f32[32,512]{1,0:T(8,128)S(1)} collective-permute-done((f32[32,512]{1,0:T(8,128)S(1)}, f32[32,512]{1,0:T(8,128)S(1)}, u32[]{:S(2)}, u32[]{:S(2)}) %collective-permute-start.10) | collective-permute-done | bytes 65568 | tf_op jit(solution)/shard_map/ppermute | solution.py:19
  48.3 4.1 %collective-permute-start.17 = (f32[32,512]{1,0:T(8,128)S(1)}, f32[32,512]{1,0:T(8,128)S(1)}, u32[]{:S(2)}, u32[]{:S(2)}) collective-permute-start(f32[32,512]{1,0:T(8,128)S(1)} %get-tuple-element.50.refs_0_), channel_id=1, source_target_pairs={{0,16},{4,20},{8,24},{12,28},{16,0},{20,4},{24,8},{28,12},{1,17},{... | collective-permute-start | bytes 196616 | tf_op jit(solution)/shard_map/ppermute | solution.py:19
  52.4 1.5 %collective-permute-start.28 = (f32[2,256,256]{2,1,0:T(8,128)S(1)}, f32[2,256,256]{2,1,0:T(8,128)S(1)}, u32[]{:S(2)}, u32[]{:S(2)}) collective-permute-start(f32[2,256,256]{2,1,0:T(8,128)S(1)} %get-tuple-element.55), channel_id=1, source_target_pairs={{0,4},{4,0},{8,12},{12,8},{16,20},{20,16},{24,28},{28,24},{1,5},{5... | collective-permute-start | bytes 1572872 | tf_op jit(solution)/shard_map/ppermute | solution.py:19
  56.4 1.5 %collective-permute-start.18 = (f32[32,512]{1,0:T(8,128)S(1)}, f32[32,512]{1,0:T(8,128)S(1)}, u32[]{:S(2)}, u32[]{:S(2)}) collective-permute-start(f32[32,512]{1,0:T(8,128)S(1)} %collective-permute-done.17.refs_4_), channel_id=1, source_target_pairs={{0,4},{4,0},{8,12},{12,8},{16,20},{20,16},{24,28},{28,24},{1,5},{5... | collective-permute-start | bytes 196616 | tf_op jit(solution)/shard_map/ppermute | solution.py:19
  58.2 1.8 %collective-permute-start.31 = (f32[384,256]{1,0:T(8,128)S(1)}, f32[384,256]{1,0:T(8,128)S(1)}, u32[]{:S(2)}, u32[]{:S(2)}) collective-permute-start(f32[384,256]{1,0:T(8,128)S(1)} %get-tuple-element.56), channel_id=1, source_target_pairs={{0,16},{4,20},{8,24},{12,28},{16,0},{20,4},{24,8},{28,12},{1,17},{... | collective-permute-start | bytes 1179656 | tf_op jit(solution)/shard_map/ppermute | solution.py:19
  59.9 6.4 %collective-permute-done.14.refs_1_ = f32[32,512]{1,0:T(8,128)S(1)} collective-permute-done((f32[32,512]{1,0:T(8,128)S(1)}, f32[32,512]{1,0:T(8,128)S(1)}, u32[]{:S(2)}, u32[]{:S(2)}) %collective-permute-start.14) | collective-permute-done | bytes 65568 | tf_op jit(solution)/shard_map/ppermute | solution.py:19
  66.4 1.5 %collective-permute-start.16 = (f32[32,512]{1,0:T(8,128)S(1)}, f32[32,512]{1,0:T(8,128)S(1)}, u32[]{:S(2)}, u32[]{:S(2)}) collective-permute-start(f32[32,512]{1,0:T(8,128)S(1)} %collective-permute-done.15.refs_2_), channel_id=1, source_target_pairs={{0,4},{4,0},{8,12},{12,8},{16,20},{20,16},{24,28},{28,24},{1,5},{5... | collective-permute-start | bytes 196616 | tf_op jit(solution)/shard_map/ppermute | solution.py:19
  68.6 2.4 %collective-permute-done.16.refs_3_ = f32[32,512]{1,0:T(8,128)S(1)} collective-permute-done((f32[32,512]{1,0:T(8,128)S(1)}, f32[32,512]{1,0:T(8,128)S(1)}, u32[]{:S(2)}, u32[]{:S(2)}) %collective-permute-start.16) | collective-permute-done | bytes 65568 | tf_op jit(solution)/shard_map/ppermute | solution.py:19
  72.3 1.4 %collective-permute-start.30 = (f32[256,256]{1,0:T(8,128)S(1)}, f32[256,256]{1,0:T(8,128)S(1)}, u32[]{:S(2)}, u32[]{:S(2)}) collective-permute-start(f32[256,256]{1,0:T(8,128)S(1)} %copy-done.1), channel_id=1, source_target_pairs={{0,8},{4,12},{8,0},{12,4},{16,24},{20,28},{24,16},{28,20},{1,9},{5... | collective-permute-start | bytes 786440 | tf_op jit(solution)/shard_map/ppermute | solution.py:19
  74.6 6.5 %collective-permute-done.29.w2in = f32[256,256]{1,0:T(8,128)S(1)} collective-permute-done((f32[256,256]{1,0:T(8,128)S(1)}, f32[256,256]{1,0:T(8,128)S(1)}, u32[]{:S(2)}, u32[]{:S(2)}) %collective-permute-start.29) | collective-permute-done | bytes 262176 | tf_op jit(solution)/shard_map/ppermute | solution.py:19
  81.7 4.9 %collective-permute-done.30.w2out = f32[256,256]{1,0:T(8,128)S(1)} collective-permute-done((f32[256,256]{1,0:T(8,128)S(1)}, f32[256,256]{1,0:T(8,128)S(1)}, u32[]{:S(2)}, u32[]{:S(2)}) %collective-permute-start.30) | collective-permute-done | bytes 262176 | tf_op jit(solution)/shard_map/ppermute | solution.py:19
  86.7 1.6 %collective-permute-start.22 = (f32[8,128]{1,0:T(8,128)S(1)}, f32[8,128]{1,0:T(8,128)S(1)}, u32[]{:S(2)}, u32[]{:S(2)}) collective-permute-start(f32[8,128]{1,0:T(8,128)S(1)} %get-tuple-element.51.t), channel_id=1, source_target_pairs={{0,3},{1,2},{2,1},{3,0},{4,7},{5,6},{6,5},{7,4},{8,11},{9,10},{10,... | collective-permute-start | bytes 12296 | tf_op jit(solution)/shard_map/ppermute | solution.py:19
  89.7 2.2 %collective-permute-done.21.n2 = f32[8,128]{1,0:T(8,128)S(1)} collective-permute-done((f32[8,128]{1,0:T(8,128)S(1)}, f32[8,128]{1,0:T(8,128)S(1)}, u32[]{:S(2)}, u32[]{:S(2)}) %collective-permute-start.21) | collective-permute-done | bytes 4128 | tf_op jit(solution)/shard_map/ppermute | solution.py:19
  93.7 2.0 %collective-permute-start.34 = (bf16[2,256,256]{2,1,0:T(8,128)(2,1)S(1)}, bf16[2,256,256]{2,1,0:T(8,128)(2,1)S(1)}, u32[]{:S(2)}, u32[]{:S(2)}) collective-permute-start(bf16[2,256,256]{2,1,0:T(8,128)(2,1)S(1)} %get-tuple-element.64.refs_1_), channel_id=1, source_target_pairs={{0,8},{4,12},{8,0},{12,4},{16,24},{20,28},{24,16},{28,20},{1,9},{5... | collective-permute-start | bytes 786440 | tf_op jit(solution)/shard_map/ppermute | solution.py:19
  95.7 6.6 %collective-permute-done.35.refs_5_ = bf16[2,256,256]{2,1,0:T(8,128)(2,1)S(1)} collective-permute-done((bf16[2,256,256]{2,1,0:T(8,128)(2,1)S(1)}, bf16[2,256,256]{2,1,0:T(8,128)(2,1)S(1)}, u32[]{:S(2)}, u32[]{:S(2)}) %collective-permute-start.35) | collective-permute-done | bytes 262176 | tf_op jit(solution)/shard_map/ppermute | solution.py:19
  104.1 1.8 %collective-permute-done.34.refs_0_ = bf16[2,256,256]{2,1,0:T(8,128)(2,1)S(1)} collective-permute-done((bf16[2,256,256]{2,1,0:T(8,128)(2,1)S(1)}, bf16[2,256,256]{2,1,0:T(8,128)(2,1)S(1)}, u32[]{:S(2)}, u32[]{:S(2)}) %collective-permute-start.34) | collective-permute-done | bytes 262176 | tf_op jit(solution)/shard_map/ppermute | solution.py:19
  105.9 2.9 %collective-permute-done.36.refs_1_ = bf16[2,256,256]{2,1,0:T(8,128)(2,1)S(1)} collective-permute-done((bf16[2,256,256]{2,1,0:T(8,128)(2,1)S(1)}, bf16[2,256,256]{2,1,0:T(8,128)(2,1)S(1)}, u32[]{:S(2)}, u32[]{:S(2)}) %collective-permute-start.36) | collective-permute-done | bytes 262176 | tf_op jit(solution)/shard_map/ppermute | solution.py:19
  (70 shorter events, 17.2 us)
Async XLA Ops:
  1.6 10.5 %collective-permute-start.3 = (bf16[256,256]{1,0:T(8,128)(2,1)S(1)}, bf16[256,256]{1,0:T(8,128)(2,1)S(1)}, u32[]{:S(2)}, u32[]{:S(2)}) collective-permute-start(bf16[256,256]{1,0:T(8,128)(2,1)S(1)} %shard_map.186.refs_0_), channel_id=1, source_target_pairs={{0,16},{4,20},{8,24},{12,28},{16,0},{20,4},{24,8},{28,12},{1,17},{... | collective-permute-start | bytes 393224 | tf_op jit(solution)/shard_map/ppermute | solution.py:19
  7.2 19.2 %collective-permute-start.7 = (bf16[768,256]{1,0:T(8,128)(2,1)S(1)}, bf16[768,256]{1,0:T(8,128)(2,1)S(1)}, u32[]{:S(2)}, u32[]{:S(2)}) collective-permute-start(bf16[768,256]{1,0:T(8,128)(2,1)S(1)} %get-tuple-element.43), channel_id=1, source_target_pairs={{0,1},{1,0},{2,3},{3,2},{4,5},{5,4},{6,7},{7,6},{8,9},{9,8},{10,11... | collective-permute-start | bytes 1179656 | tf_op jit(solution)/shard_map/ppermute | solution.py:19
  7.3 7.6 %collective-permute-start.1 = (bf16[256,256]{1,0:T(8,128)(2,1)S(1)}, bf16[256,256]{1,0:T(8,128)(2,1)S(1)}, u32[]{:S(2)}, u32[]{:S(2)}) collective-permute-start(bf16[256,256]{1,0:T(8,128)(2,1)S(1)} %shard_map.186.refs_0_), channel_id=1, source_target_pairs={{0,8},{4,12},{8,0},{12,4},{16,24},{20,28},{24,16},{28,20},{1,9},{5... | collective-permute-start | bytes 393224 | tf_op jit(solution)/shard_map/ppermute | solution.py:19
  12.1 5.4 %collective-permute-start.5 = (bf16[256,256]{1,0:T(8,128)(2,1)S(1)}, bf16[256,256]{1,0:T(8,128)(2,1)S(1)}, u32[]{:S(2)}, u32[]{:S(2)}) collective-permute-start(bf16[256,256]{1,0:T(8,128)(2,1)S(1)} %collective-permute-done.3.refs_4_.refs_3_), channel_id=1, source_target_pairs={{0,8},{4,12},{8,0},{12,4},{16,24},{20,28},{24,16},{28,20},{1,9},{5... | collective-permute-start | bytes 393224 | tf_op jit(solution)/shard_map/ppermute | solution.py:19
  12.8 6.4 %collective-permute-start = (bf16[256,256]{1,0:T(8,128)(2,1)S(1)}, bf16[256,256]{1,0:T(8,128)(2,1)S(1)}, u32[]{:S(2)}, u32[]{:S(2)}) collective-permute-start(bf16[256,256]{1,0:T(8,128)(2,1)S(1)} %shard_map.186.refs_0_), channel_id=1, source_target_pairs={{0,4},{4,0},{8,12},{12,8},{16,20},{20,16},{24,28},{28,24},{1,5},{5... | collective-permute-start | bytes 393224 | tf_op jit(solution)/shard_map/ppermute | solution.py:19
  14.3 7.7 %collective-permute-start.4 = (bf16[256,256]{1,0:T(8,128)(2,1)S(1)}, bf16[256,256]{1,0:T(8,128)(2,1)S(1)}, u32[]{:S(2)}, u32[]{:S(2)}) collective-permute-start(bf16[256,256]{1,0:T(8,128)(2,1)S(1)} %collective-permute-done.3.refs_4_.refs_3_), channel_id=1, source_target_pairs={{0,4},{4,0},{8,12},{12,8},{16,20},{20,16},{24,28},{28,24},{1,5},{5... | collective-permute-start | bytes 393224 | tf_op jit(solution)/shard_map/ppermute | solution.py:19
  14.9 9.8 %collective-permute-start.2 = (bf16[256,256]{1,0:T(8,128)(2,1)S(1)}, bf16[256,256]{1,0:T(8,128)(2,1)S(1)}, u32[]{:S(2)}, u32[]{:S(2)}) collective-permute-start(bf16[256,256]{1,0:T(8,128)(2,1)S(1)} %collective-permute-done.1.refs_2_), channel_id=1, source_target_pairs={{0,4},{4,0},{8,12},{12,8},{16,20},{20,16},{24,28},{28,24},{1,5},{5... | collective-permute-start | bytes 393224 | tf_op jit(solution)/shard_map/ppermute | solution.py:19
  17.5 8.9 %collective-permute-start.6 = (bf16[256,256]{1,0:T(8,128)(2,1)S(1)}, bf16[256,256]{1,0:T(8,128)(2,1)S(1)}, u32[]{:S(2)}, u32[]{:S(2)}) collective-permute-start(bf16[256,256]{1,0:T(8,128)(2,1)S(1)} %collective-permute-done.5.refs_6_.refs_2_), channel_id=1, source_target_pairs={{0,4},{4,0},{8,12},{12,8},{16,20},{20,16},{24,28},{28,24},{1,5},{5... | collective-permute-start | bytes 393224 | tf_op jit(solution)/shard_map/ppermute | solution.py:19
  29.7 5.8 %collective-permute-start.8 = (f32[2,32,512]{2,1,0:T(8,128)S(1)}, f32[2,32,512]{2,1,0:T(8,128)S(1)}, u32[]{:S(2)}, u32[]{:S(2)}) collective-permute-start(f32[2,32,512]{2,1,0:T(8,128)S(1)} %get-tuple-element.45), channel_id=1, source_target_pairs={{0,4},{4,0},{8,12},{12,8},{16,20},{20,16},{24,28},{28,24},{1,5},{5... | collective-permute-start | bytes 393224 | tf_op jit(solution)/shard_map/ppermute | solution.py:19
  31.3 8.1 %collective-permute-start.9 = (f32[2,32,512]{2,1,0:T(8,128)S(1)}, f32[2,32,512]{2,1,0:T(8,128)S(1)}, u32[]{:S(2)}, u32[]{:S(2)}) collective-permute-start(f32[2,32,512]{2,1,0:T(8,128)S(1)} %get-tuple-element.46), channel_id=1, source_target_pairs={{0,4},{4,0},{8,12},{12,8},{16,20},{20,16},{24,28},{28,24},{1,5},{5... | collective-permute-start | bytes 393224 | tf_op jit(solution)/shard_map/ppermute | solution.py:19
  31.8 8.5 %collective-permute-start.13 = (f32[2,32,256]{2,1,0:T(8,128)S(1)}, f32[2,32,256]{2,1,0:T(8,128)S(1)}, u32[]{:S(2)}, u32[]{:S(2)}) collective-permute-start(f32[2,32,256]{2,1,0:T(8,128)S(1)} %get-tuple-element.49), channel_id=1, source_target_pairs={{0,1},{1,0},{2,3},{3,2},{4,5},{5,4},{6,7},{7,6},{8,9},{9,8},{10,11... | collective-permute-start | bytes 196616 | tf_op jit(solution)/shard_map/ppermute | solution.py:19
  35.5 7.9 %collective-permute-start.12 = (f32[32,512]{1,0:T(8,128)S(1)}, f32[32,512]{1,0:T(8,128)S(1)}, u32[]{:S(2)}, u32[]{:S(2)}) collective-permute-start(f32[32,512]{1,0:T(8,128)S(1)} %shard_map.192), channel_id=1, source_target_pairs={{0,8},{4,12},{8,0},{12,4},{16,24},{20,28},{24,16},{28,20},{1,9},{5... | collective-permute-start | bytes 196616 | tf_op jit(solution)/shard_map/ppermute | solution.py:19
  35.5 18.4 %collective-permute-start.32 = (f32[128,256]{1,0:T(8,128)S(1)}, f32[128,256]{1,0:T(8,128)S(1)}, u32[]{:S(2)}, u32[]{:S(2)}) collective-permute-start(f32[128,256]{1,0:T(8,128)S(1)} %get-tuple-element.57), channel_id=1, source_target_pairs={{0,16},{4,20},{8,24},{12,28},{16,0},{20,4},{24,8},{28,12},{1,17},{... | collective-permute-start | bytes 393224 | tf_op jit(solution)/shard_map/ppermute | solution.py:19
  39.4 15.3 %collective-permute-start.27 = (bf16[256,256]{1,0:T(8,128)(2,1)S(1)}, bf16[256,256]{1,0:T(8,128)(2,1)S(1)}, u32[]{:S(2)}, u32[]{:S(2)}) collective-permute-start(bf16[256,256]{1,0:T(8,128)(2,1)S(1)} %collective-permute-done.3.refs_4_.refs_3_), channel_id=1, source_target_pairs={{0,1},{1,0},{2,3},{3,2},{4,5},{5,4},{6,7},{7,6},{8,9},{9,8},{10,11... | collective-permute-start | bytes 393224 | tf_op jit(solution)/shard_map/ppermute | solution.py:19
  39.4 8.8 %collective-permute-start.10 = (f32[32,512]{1,0:T(8,128)S(1)}, f32[32,512]{1,0:T(8,128)S(1)}, u32[]{:S(2)}, u32[]{:S(2)}) collective-permute-start(f32[32,512]{1,0:T(8,128)S(1)} %get-tuple-element.47), channel_id=1, source_target_pairs={{0,16},{4,20},{8,24},{12,28},{16,0},{20,4},{24,8},{28,12},{1,17},{... | collective-permute-start | bytes 196616 | tf_op jit(solution)/shard_map/ppermute | solution.py:19
  40.3 7.9 %collective-permute-start.11 = (f32[32,512]{1,0:T(8,128)S(1)}, f32[32,512]{1,0:T(8,128)S(1)}, u32[]{:S(2)}, u32[]{:S(2)}) collective-permute-start(f32[32,512]{1,0:T(8,128)S(1)} %get-tuple-element.48), channel_id=1, source_target_pairs={{0,24},{4,28},{8,16},{12,20},{16,8},{20,12},{24,0},{28,4},{1,25},{... | collective-permute-start | bytes 196616 | tf_op jit(solution)/shard_map/ppermute | solution.py:19
  43.3 13.1 %collective-permute-start.26 = (bf16[256,256]{1,0:T(8,128)(2,1)S(1)}, bf16[256,256]{1,0:T(8,128)(2,1)S(1)}, u32[]{:S(2)}, u32[]{:S(2)}) collective-permute-start(bf16[256,256]{1,0:T(8,128)(2,1)S(1)} %collective-permute-done.1.refs_2_), channel_id=1, source_target_pairs={{0,1},{1,0},{2,3},{3,2},{4,5},{5,4},{6,7},{7,6},{8,9},{9,8},{10,11... | collective-permute-start | bytes 393224 | tf_op jit(solution)/shard_map/ppermute | solution.py:19
  48.3 6.9 %collective-permute-start.17 = (f32[32,512]{1,0:T(8,128)S(1)}, f32[32,512]{1,0:T(8,128)S(1)}, u32[]{:S(2)}, u32[]{:S(2)}) collective-permute-start(f32[32,512]{1,0:T(8,128)S(1)} %get-tuple-element.50.refs_0_), channel_id=1, source_target_pairs={{0,16},{4,20},{8,24},{12,28},{16,0},{20,4},{24,8},{28,12},{1,17},{... | collective-permute-start | bytes 196616 | tf_op jit(solution)/shard_map/ppermute | solution.py:19
  52.4 37.0 %collective-permute-start.28 = (f32[2,256,256]{2,1,0:T(8,128)S(1)}, f32[2,256,256]{2,1,0:T(8,128)S(1)}, u32[]{:S(2)}, u32[]{:S(2)}) collective-permute-start(f32[2,256,256]{2,1,0:T(8,128)S(1)} %get-tuple-element.55), channel_id=1, source_target_pairs={{0,4},{4,0},{8,12},{12,8},{16,20},{20,16},{24,28},{28,24},{1,5},{5... | collective-permute-start | bytes 1572872 | tf_op jit(solution)/shard_map/ppermute | solution.py:19
  54.7 11.7 %collective-permute-start.14 = (f32[32,512]{1,0:T(8,128)S(1)}, f32[32,512]{1,0:T(8,128)S(1)}, u32[]{:S(2)}, u32[]{:S(2)}) collective-permute-start(f32[32,512]{1,0:T(8,128)S(1)} %get-tuple-element.50.refs_0_), channel_id=1, source_target_pairs={{0,4},{4,0},{8,12},{12,8},{16,20},{20,16},{24,28},{28,24},{1,5},{5... | collective-permute-start | bytes 196616 | tf_op jit(solution)/shard_map/ppermute | solution.py:19
  55.2 11.1 %collective-permute-start.19 = (f32[32,512]{1,0:T(8,128)S(1)}, f32[32,512]{1,0:T(8,128)S(1)}, u32[]{:S(2)}, u32[]{:S(2)}) collective-permute-start(f32[32,512]{1,0:T(8,128)S(1)} %collective-permute-done.17.refs_4_), channel_id=1, source_target_pairs={{0,8},{4,12},{8,0},{12,4},{16,24},{20,28},{24,16},{28,20},{1,9},{5... | collective-permute-start | bytes 196616 | tf_op jit(solution)/shard_map/ppermute | solution.py:19
  56.4 11.5 %collective-permute-start.18 = (f32[32,512]{1,0:T(8,128)S(1)}, f32[32,512]{1,0:T(8,128)S(1)}, u32[]{:S(2)}, u32[]{:S(2)}) collective-permute-start(f32[32,512]{1,0:T(8,128)S(1)} %collective-permute-done.17.refs_4_), channel_id=1, source_target_pairs={{0,4},{4,0},{8,12},{12,8},{16,20},{20,16},{24,28},{28,24},{1,5},{5... | collective-permute-start | bytes 196616 | tf_op jit(solution)/shard_map/ppermute | solution.py:19
  58.2 28.5 %collective-permute-start.31 = (f32[384,256]{1,0:T(8,128)S(1)}, f32[384,256]{1,0:T(8,128)S(1)}, u32[]{:S(2)}, u32[]{:S(2)}) collective-permute-start(f32[384,256]{1,0:T(8,128)S(1)} %get-tuple-element.56), channel_id=1, source_target_pairs={{0,16},{4,20},{8,24},{12,28},{16,0},{20,4},{24,8},{28,12},{1,17},{... | collective-permute-start | bytes 1179656 | tf_op jit(solution)/shard_map/ppermute | solution.py:19
  66.4 8.1 %collective-permute-start.25 = (bf16[256,256]{1,0:T(8,128)(2,1)S(1)}, bf16[256,256]{1,0:T(8,128)(2,1)S(1)}, u32[]{:S(2)}, u32[]{:S(2)}) collective-permute-start(bf16[256,256]{1,0:T(8,128)(2,1)S(1)} %collective-permute-done.refs_1_), channel_id=1, source_target_pairs={{0,1},{1,0},{2,3},{3,2},{4,5},{5,4},{6,7},{7,6},{8,9},{9,8},{10,11... | collective-permute-start | bytes 393224 | tf_op jit(solution)/shard_map/ppermute | solution.py:19
  71.1 10.1 %collective-permute-start.29 = (f32[256,256]{1,0:T(8,128)S(1)}, f32[256,256]{1,0:T(8,128)S(1)}, u32[]{:S(2)}, u32[]{:S(2)}) collective-permute-start(f32[256,256]{1,0:T(8,128)S(1)} %copy-done), channel_id=1, source_target_pairs={{0,8},{4,12},{8,0},{12,4},{16,24},{20,28},{24,16},{28,20},{1,9},{5... | collective-permute-start | bytes 786440 | tf_op jit(solution)/shard_map/ppermute | solution.py:19
  72.3 14.4 %collective-permute-start.30 = (f32[256,256]{1,0:T(8,128)S(1)}, f32[256,256]{1,0:T(8,128)S(1)}, u32[]{:S(2)}, u32[]{:S(2)}) collective-permute-start(f32[256,256]{1,0:T(8,128)S(1)} %copy-done.1), channel_id=1, source_target_pairs={{0,8},{4,12},{8,0},{12,4},{16,24},{20,28},{24,16},{28,20},{1,9},{5... | collective-permute-start | bytes 786440 | tf_op jit(solution)/shard_map/ppermute | solution.py:19
  74.5 13.8 %collective-permute-start.24 = (f32[256,256]{1,0:T(8,128)S(1)}, f32[256,256]{1,0:T(8,128)S(1)}, u32[]{:S(2)}, u32[]{:S(2)}) collective-permute-start(f32[256,256]{1,0:T(8,128)S(1)} %get-tuple-element.53), channel_id=1, source_target_pairs={{0,1},{1,0},{2,3},{3,2},{4,5},{5,4},{6,7},{7,6},{8,9},{9,8},{10,11... | collective-permute-start | bytes 786440 | tf_op jit(solution)/shard_map/ppermute | solution.py:19
  81.1 8.3 %collective-permute-start.33 = (f32[2,32,256]{2,1,0:T(8,128)S(1)}, f32[2,32,256]{2,1,0:T(8,128)S(1)}, u32[]{:S(2)}, u32[]{:S(2)}) collective-permute-start(f32[2,32,256]{2,1,0:T(8,128)S(1)} %get-tuple-element.59), channel_id=1, source_target_pairs={{0,1},{1,0},{2,3},{3,2},{4,5},{5,4},{6,7},{7,6},{8,9},{9,8},{10,11... | collective-permute-start | bytes 196616 | tf_op jit(solution)/shard_map/ppermute | solution.py:19
  93.2 9.2 %collective-permute-start.35 = (bf16[2,256,256]{2,1,0:T(8,128)(2,1)S(1)}, bf16[2,256,256]{2,1,0:T(8,128)(2,1)S(1)}, u32[]{:S(2)}, u32[]{:S(2)}) collective-permute-start(bf16[2,256,256]{2,1,0:T(8,128)(2,1)S(1)} %get-tuple-element.65.refs_3_), channel_id=1, source_target_pairs={{0,8},{4,12},{8,0},{12,4},{16,24},{20,28},{24,16},{28,20},{1,9},{5... | collective-permute-start | bytes 786440 | tf_op jit(solution)/shard_map/ppermute | solution.py:19
  93.2 9.7 %collective-permute-start.37 = (bf16[2,256,256]{2,1,0:T(8,128)(2,1)S(1)}, bf16[2,256,256]{2,1,0:T(8,128)(2,1)S(1)}, u32[]{:S(2)}, u32[]{:S(2)}) collective-permute-start(bf16[2,256,256]{2,1,0:T(8,128)(2,1)S(1)} %get-tuple-element.65.refs_3_), channel_id=1, source_target_pairs={{0,4},{4,0},{8,12},{12,8},{16,20},{20,16},{24,28},{28,24},{1,5},{5... | collective-permute-start | bytes 786440 | tf_op jit(solution)/shard_map/ppermute | solution.py:19
  93.7 12.2 %collective-permute-start.34 = (bf16[2,256,256]{2,1,0:T(8,128)(2,1)S(1)}, bf16[2,256,256]{2,1,0:T(8,128)(2,1)S(1)}, u32[]{:S(2)}, u32[]{:S(2)}) collective-permute-start(bf16[2,256,256]{2,1,0:T(8,128)(2,1)S(1)} %get-tuple-element.64.refs_1_), channel_id=1, source_target_pairs={{0,8},{4,12},{8,0},{12,4},{16,24},{20,28},{24,16},{28,20},{1,9},{5... | collective-permute-start | bytes 786440 | tf_op jit(solution)/shard_map/ppermute | solution.py:19
  102.4 6.4 %collective-permute-start.36 = (bf16[2,256,256]{2,1,0:T(8,128)(2,1)S(1)}, bf16[2,256,256]{2,1,0:T(8,128)(2,1)S(1)}, u32[]{:S(2)}, u32[]{:S(2)}) collective-permute-start(bf16[2,256,256]{2,1,0:T(8,128)(2,1)S(1)} %collective-permute-done.35.refs_5_), channel_id=1, source_target_pairs={{0,4},{4,0},{8,12},{12,8},{16,20},{20,16},{24,28},{28,24},{1,5},{5... | collective-permute-start | bytes 786440 | tf_op jit(solution)/shard_map/ppermute | solution.py:19
  (12 other events, 221.9 us)

commit v4 on v3

--- a/solution.py
+++ b/solution.py
@@ -80,21 +80,19 @@
         copy_all([pltpu.make_async_copy(even, out, sem)])
 
 
-def picked_body(cots, firsts, seconds, factors, weights, cot, moments, factor, both, w4a, w4b, sems):
-    depth = factor.shape[0]
-    half = w4b.shape[0]
+def picked_body(saved, cots, firsts, seconds, factors, weights, outs, sems):
+    held, own, cot, moments, factor, both = outs
 
     def copies(k):
         pairs = (
             (cots[k], cot),
+            (cots[1 - k], own),
+            (saved, held),
             (firsts[k], moments.at[0]),
             (seconds[k], moments.at[1]),
             (factors[k], factor),
             (weights[0], both.at[0]),
             (weights[1], both.at[1]),
-            (weights[0], w4a.at[pl.ds(0, depth), :]),
-            (weights[1].at[pl.ds(0, depth - half), :], w4a.at[pl.ds(depth, depth - half), :]),
-            (weights[1].at[pl.ds(depth - half, half), :], w4b),
         )
         return [pltpu.make_async_copy(*pair, sems.at[i]) for i, pair in enumerate(pairs)]
 
@@ -107,47 +105,25 @@
         copy_all(copies(1))
 
 
-def fetch(saved_ref, held, sems, numbers):
-    copies = [
-        pltpu.make_async_copy(saved_ref.at[:, slot(d, held.shape[2])], held.at[k], sems.at[k])
-        for k, d in enumerate(numbers)
-    ]
-    for copy in copies:
-        copy.start()
-    return copies
-
-
-def add_blocks(total, copies, held, factors):
-    for k, (copy, factor) in enumerate(zip(copies, factors, strict=True)):
-        copy.wait()
-        total = total + jnp.dot(held[k], factor[...], preferred_element_type=jnp.float32)
+def add_blocks(total, saved_ref, factors, numbers):
+    for d, factor in zip(numbers, factors, strict=True):
+        total = total + jnp.dot(
+            saved_ref[:, slot(d, factor.shape[0])], factor[...], preferred_element_type=jnp.float32
+        )
     return total
 
 
 def map_body(numbers, saved_ref, *refs):
-    factors, (mapped_ref, held, sems) = refs[:-3], refs[-3:]
-    copies = fetch(saved_ref, held, sems, numbers)
-    mapped_ref[...] = add_blocks(jnp.zeros(mapped_ref.shape, jnp.float32), copies, held, factors)
+    mapped = jnp.zeros(refs[-1].shape, jnp.float32)
+    refs[-1][...] = add_blocks(mapped, saved_ref, refs[:-1], numbers)
 
 
 def term_body(size, numbers, saved_ref, mapped_ref, *refs):
-    factors, refs = refs[: len(numbers)], refs[len(numbers) :]
-    cot_in, cot_out, peer, far, near, own, held, cot, sems, cot_sem = refs
-    copies = fetch(saved_ref, held, sems, numbers)
-
-    @pl.when(is_odd())
-    def _():
-        pltpu.make_async_copy(cot_out, cot, cot_sem).start()
-
-    @pl.when(jnp.logical_not(is_odd()))
-    def _():
-        pltpu.make_async_copy(cot_in, cot, cot_sem).start()
-
-    mapped = add_blocks(mapped_ref[...], copies, held, factors)
+    cot, peer, far, near, own = refs[len(numbers) :]
+    mapped = add_blocks(mapped_ref[...], saved_ref, refs[: len(numbers)], numbers)
     columns = cot.shape[1]
     rows = mapped.shape[1] // size
     here = lax.axis_index("fs")
-    pltpu.make_async_copy(cot_in, cot, cot_sem).wait()
     for side, right in enumerate((cot, peer)):
         term = exact_dot(mapped, right[...], ROWS)
         at = slice(side * columns, (side + 1) * columns)
@@ -216,37 +192,59 @@
         )
 
 
-def finish_body(entries, sums, full_ref, other_ref, weights, news, back, outs):
+def scales(entries, sums):
+    t, n2, n3, n1 = sums
+    for pair in ((t, n2), (n1, n3)):
+        mean = jnp.maximum(pair[0][...] + pair[1][...], 0.0) / entries
+        yield (1.0 / jnp.sqrt(mean + 1e-06))[0:1, 0:1]
+
+
+def updates(k, scaled, full_ref, other_ref):
     odd = is_odd()
-    up_in, up_out, new_in, new_out, copies, firsts, seconds = outs
-
-    def scale(pair):
-        mean = jnp.maximum(pair[0][...] + pair[1][...], 0.0) / entries
-        return (1.0 / jnp.sqrt(mean + 1e-06))[0:1, 0:1]
-
-    scales = scale(sums[:2]), scale(sums[2:])
-    for k, (copy, both) in enumerate(zip(copies, weights, strict=True)):
-        update = full_ref[k] * scales[0]
-        update_other = other_ref[k] * scales[1]
-        for p, weight in enumerate(both):
-            chosen = jnp.where(odd, update, update_other) if p else jnp.where(odd, update_other, update)
-            fresh = weight() - 0.02 * chosen
-            copy[p] = fresh.astype(jnp.bfloat16)
+    mine, other = full_ref[k] * scaled[0], other_ref[k] * scaled[1]
+    return jnp.where(odd, other, mine), jnp.where(odd, mine, other)
+
+
+def ahead_body(entries, *refs):
+    full_ref, other_ref, *weights, both, c_in, c_out = refs[4:]
+    chosen = updates(3, tuple(scales(entries, refs[:4])), full_ref, other_ref)
+    for p, copy in enumerate((c_in, c_out)):
+        copy[...] = (weights[p][...] - 0.02 * chosen[p]).astype(jnp.bfloat16)
+        both[p] = copy[...]
+
+
+def finish_body(entries, *refs):
+    full_ref, other_ref, w_in, w_out, w1, w2in, w2out, news, back = refs[4:13]
+    ups, fresh, copies, firsts, seconds = (
+        refs[13:15],
+        refs[15:17],
+        refs[17:20],
+        refs[20:22],
+        refs[22:24],
+    )
+    scaled = tuple(scales(entries, refs[:4]))
+    weights = ((w_in, w_out), (w1.at[0], w1.at[1]), (w2in, w2out))
+    for k, (copy, pair) in enumerate(zip(copies, weights, strict=True)):
+        for p, chosen in enumerate(updates(k, scaled, full_ref, other_ref)):
+            new = pair[p][...] - 0.02 * chosen
+            copy[p] = new.astype(jnp.bfloat16)
             if k == 0:
-                (new_out if p else new_in)[...] = fresh
-                (up_out if p else up_in)[...] = chosen
+                fresh[p][...] = new
+                ups[p][...] = chosen
+    odd = is_odd()
     for k, pair in enumerate((firsts, seconds)):
         pair[0][...] = jnp.where(odd, back[k], news[k])
         pair[1][...] = jnp.where(odd, news[k], back[k])
 
 
-def place_body(numbers, *refs):
-    blocks, (copy_in, copy_out, sems) = refs[: len(numbers)], refs[-3:]
+def place_body(pieces, *refs):
+    blocks, (*whole, sems) = refs[: len(pieces)], refs[-3:]
     copies = []
-    for k, (d, block) in enumerate(zip(numbers, blocks, strict=True)):
-        for p, whole in enumerate((copy_in, copy_out)):
-            rows = whole.at[slot(d, block.shape[1]), :]
-            copies.append(pltpu.make_async_copy(block.at[p], rows, sems.at[2 * k + p]))
+    for (d, only), block in zip(pieces, blocks, strict=True):
+        for p in (0, 1) if only is None else (only,):
+            rows = whole[p].at[slot(d, block.shape[-2]), :]
+            source = block.at[p] if only is None else block
+            copies.append(pltpu.make_async_copy(source, rows, sems.at[len(copies)]))
     copy_all(copies)
 
 
@@ -359,31 +357,32 @@
     f4 = send(factor, "fs", 4)
     f2 = send(factor, "fs", 2)
     f1 = send(factor, "fs", 1)
-    half = depth // 2
-
-    def picked(c0, c1, f0, f1, s0, s1, g0, g1, w0, w1, *rest):
-        picked_body((c0, c1), (f0, f1), (s0, s1), (g0, g1), (w0, w1), *rest)
-
-    cot_theirs, moments_theirs, factor_theirs, both, early4, late4 = call(
+
+    def picked(saved, c0, c1, f0, f1, s0, s1, g0, g1, w0, w1, *rest):
+        outs, sems = rest[:-1], rest[-1]
+        picked_body(saved, (c0, c1), (f0, f1), (s0, s1), (g0, g1), (w0, w1), outs, sems)
+
+    saved, cot, cot_theirs, moments_theirs, factor_theirs, both = call(
         picked,
         (
+            like(saved_input.shape, saved_input.dtype),
+            like((tokens, columns), cot_inproj.dtype),
             like((tokens, columns), cot_inproj.dtype),
             f32((2, rows, columns)),
             like((depth, rank), factor_inproj.dtype),
             f32((2, depth, columns)),
-            f32((2 * depth - half, columns)),
-            f32((half, columns)),
         ),
-        *(cot_inproj, cot_outproj, first_inproj, first_outproj, second_inproj, second_outproj),
+        *(saved_input, cot_inproj, cot_outproj),
+        *(first_inproj, first_outproj, second_inproj, second_outproj),
         *(factor_inproj, factor_outproj, weight_inproj, weight_outproj),
-        scratch=[dma((9,))],
-        hbm=range(10),
+        scratch=[dma((8,))],
+        hbm=range(11),
         flops=tokens * columns,
     )
     cot_peer = send(cot_theirs, "tp", 1)
-    f3 = send(f2, "fs", 1)
+    f3 = send(f1, "fs", 2)
     f6 = send(f4, "fs", 2)
-    w4a = send(early4, "fs", 4)
+    w4in = send(weight_inproj, "fs", 4)
     f5 = send(f4, "fs", 1)
     f7 = send(f6, "fs", 1)
     w2in = send(weight_inproj, "fs", 2)
@@ -393,29 +392,19 @@
     mapped = call(
         functools.partial(map_body, early),
         f32((tokens, rank)),
-        saved_input,
+        saved,
         *(factors[k] for k in early),
-        scratch=[pltpu.VMEM((len(early), tokens, depth), saved_input.dtype), dma((len(early),))],
-        hbm=(0,),
         flops=2 * tokens * rank * depth * len(early),
     )
     pair = f32((2, rows, 2 * columns))
     far, near, own = call(
         functools.partial(term_body, size, late),
         (pair, pair, f32((size, rows, 2 * columns))),
-        saved_input,
+        saved,
         mapped,
         *(factors[k] for k in late),
-        cot_inproj,
-        cot_outproj,
+        cot,
         cot_peer,
-        scratch=[
-            pltpu.VMEM((len(late), tokens, depth), saved_input.dtype),
-            pltpu.VMEM((tokens, columns), cot_inproj.dtype),
-            dma((len(late),)),
-            dma,
-        ],
-        hbm=(0, 2 + len(late), 3 + len(late)),
         flops=2 * tokens * rank * (depth * len(late) + 6 * columns),
     )
     square = call(
@@ -449,11 +438,11 @@
     s4 = send(small, "fs", 4)
     s2 = send(small, "fs", 2)
     s1 = send(small, "fs", 1)
-    s6 = send(s4, "fs", 2)
+    s6 = send(small, "fs", 6)
     s3 = send(s2, "fs", 1)
     s5 = send(s4, "fs", 1)
     s7 = send(s6, "fs", 1)
-    w4b = send(late4, "fs", 4)
+    w4out = send(weight_outproj, "fs", 4)
     back = send(others_news, "tp", 1)
     total, small_mine, small_other = call(
         functools.partial(sum_body, size),
@@ -468,54 +457,45 @@
     full = call(full_body, fours, small_mine, *(factor, f1, f2, f4), flops=flops)
     full_other = call(full_body, fours, small_other, *(factor_theirs, g1, g2, g4), flops=flops)
     entries = float(depth * size * columns * split)
-
-    def finish(t, n2, n3, n1, full_ref, other_ref, w_in, w_out, w1, w2in, w2out, w4a, w4b, *refs):
-        weights = (
-            (lambda: w_in[...], lambda: w_out[...]),
-            (lambda: w1[0], lambda: w1[1]),
-            (lambda: w2in[...], lambda: w2out[...]),
-            (
-                lambda: w4a[:depth, :],
-                lambda: jnp.concatenate([w4a[depth:, :], w4b[...]], axis=0),
-            ),
-        )
-        news_ref, back_ref, *refs = refs
-        outs = (*refs[:4], refs[4:8], refs[8:10], refs[10:12])
-        sums = (t, n2, n1, n3)
-        finish_body(entries, sums, full_ref, other_ref, weights, news_ref, back_ref, outs)
-
-    shard, copy = f32((depth, columns)), like((2, depth, columns), jnp.bfloat16)
+    shard, one = f32((depth, columns)), like((depth, columns), jnp.bfloat16)
+    two = like((2, depth, columns), jnp.bfloat16)
+    c4, c4in, c4out = call(
+        functools.partial(ahead_body, entries),
+        (two, one, one),
+        *(*sums, full, full_other, w4in, w4out),
+        flops=10 * depth * columns,
+    )
+    c5 = send(c4, "fs", 1)
+    c6in, c6out = send(c4in, "fs", 2), send(c4out, "fs", 2)
     outs = call(
-        finish,
-        (shard,) * 4 + (copy,) * 4 + (f32((rows, columns)),) * 4,
-        *sums,
-        full,
-        full_other,
-        *(weight_inproj, weight_outproj, w1, w2in, w2out, w4a, w4b, news, back),
-        flops=40 * depth * columns,
-    )
-    c0, c1, c2, c4 = outs[4:8]
-    c6 = send(c4, "fs", 2)
-    c5 = send(c4, "fs", 1)
-    c7 = send(c6, "fs", 1)
+        functools.partial(finish_body, entries),
+        (shard,) * 4 + (two,) * 3 + (f32((rows, columns)),) * 4,
+        *(*sums, full, full_other, weight_inproj, weight_outproj, w1, w2in, w2out, news, back),
+        flops=30 * depth * columns,
+    )
+    c0, c1, c2 = outs[4:7]
     c3 = send(c1, "fs", 2)
+    c7in, c7out = send(c6in, "fs", 1), send(c6out, "fs", 1)
     whole = like((depth * size, columns), jnp.bfloat16)
-    copies = (whole, whole)
-    for numbers, blocks in (((0, 1, 2, 4, 5, 6), (c0, c1, c2, c4, c5, c6)), ((3, 7), (c3, c7))):
-        count = len(numbers)
-        first = copies[0] is whole
+    copies = ()
+    for pieces, blocks in (
+        (((0, None), (1, None), (2, None), (4, None)), (c0, c1, c2, c4)),
+        (((5, None), (6, 0), (6, 1)), (c5, c6in, c6out)),
+        (((3, None), (7, 0), (7, 1)), (c3, c7in, c7out)),
+    ):
+        count = len(pieces)
         copies = call(
-            functools.partial(place_body, numbers),
+            functools.partial(place_body, pieces),
             (whole, whole),
             *blocks,
-            *(() if first else copies),
+            *copies,
             scratch=[dma((2 * count,))],
-            hbm=() if first else (count, count + 1),
+            hbm=range(count, count + len(copies)),
             out=HBM,
-            aliases={} if first else {count: 0, count + 1: 1},
+            aliases={count + k: k for k in range(len(copies))},
             flops=depth * columns,
         )
-    return (*outs[:4], *copies, *outs[8:])
+    return (*outs[:4], *copies, *outs[7:])
 
 
 def layer(*args):

time: 110 us -> 104 us (0.945)
  waiting for transfers between devices: 52.4 us -> 48.3 us
  Pallas kernels: 14 us -> 12.6 us
    ppermute x38 -> x40, waiting for transfers between devices: 52.4 us -> 48.3 us  [send(): return lax.ppermute(x, axis, [(i, i ^ bit) for i in range(size)])]
    pallas_call x14 -> x16, Pallas kernels: 14 us -> 12.6 us  [call(): pl.pallas_call(body, out_shape=outs, in_specs=[HBM if k in hbm else VMEM...]
    ppermute x38 -> x40, starting transfers between devices: 42.3 us -> 41.6 us  [send(): return lax.ppermute(x, axis, [(i, i ^ bit) for i in range(size)])]
  transfers between devices with their start and end apart: 38 -> 40, of which waited for: 20 -> 21; matrix products, arithmetic and copies ran while one was open for 0% -> 0% of each run, Pallas kernels for 7% -> 9%
where the time goes in v4:
time: 104 us; the launch traced here: 103 us
  waiting for transfers between devices  48.3 us (46%)
  starting transfers between devices  41.6 us (40%)
  Pallas kernels  12.6 us (12%)
    ppermute x40, waiting for transfers between devices, send(): return lax.ppermute(x, axis, [(i, i ^ bit) for i in range(size)])  48.3 us
    ppermute x40, starting transfers between devices, send(): return lax.ppermute(x, axis, [(i, i ^ bit) for i in range(size)])  41.6 us
    pallas_call x16, Pallas kernels, call(): pl.pallas_call(body, out_shape=outs, in_specs=[HBM if k in hbm else VMEM...  12.6 us
  transfers between devices with their start and end apart: 40, of which 21 were waited for; matrix products, arithmetic and copies ran while one was open for 0% of the time, Pallas kernels for 9%

profile of v4, /device:TPU:0, one launch (start us, length us, event | category | flops | bytes accessed | tf_op | source)
XLA Modules:
  0.0 103.4 jit_solution(6265024597699521736)
XLA Ops:
  1.6 4.1 %collective-permute-start.3 = (bf16[256,256]{1,0:T(8,128)(2,1)S(1)}, bf16[256,256]{1,0:T(8,128)(2,1)S(1)}, u32[]{:S(2)}, u32[]{:S(2)}) collective-permute-start(bf16[256,256]{1,0:T(8,128)(2,1)S(1)} %shard_map.186.refs_0_), channel_id=1, source_target_pairs={{0,16},{4,20},{8,24},{12,28},{16,0},{20,4},{24,8},{28,12},{1,17},{... | collective-permute-start | bytes 393224 | tf_op jit(solution)/shard_map/ppermute | solution.py:19
  5.7 2.4 %shard_map.188 = (bf16[768,2048]{1,0:T(8,128)(2,1)S(1)}, bf16[768,256]{1,0:T(8,128)(2,1)S(1)}, bf16[768,256]{1,0:T(8,128)(2,1)S(1)}, f32[2,32,256]{2,1,0:T(8,128...) custom-call(bf16[768,2048]{1,0:T(8,128)(2,1)} %saved.1, bf16[768,256]{1,0:T(8,128)(2,1)} %c0.1, ...), custom_call_target="tpu_custom_call" | custom-call | flops 196608 | bytes 4849664 | tf_op jit(solution)/shard_map/pallas_call | solution.py:46
  8.1 1.6 %collective-permute-start = (bf16[256,256]{1,0:T(8,128)(2,1)S(1)}, bf16[256,256]{1,0:T(8,128)(2,1)S(1)}, u32[]{:S(2)}, u32[]{:S(2)}) collective-permute-start(bf16[256,256]{1,0:T(8,128)(2,1)S(1)} %shard_map.186.refs_0_), channel_id=1, source_target_pairs={{0,4},{4,0},{8,12},{12,8},{16,20},{20,16},{24,28},{28,24},{1,5},{5... | collective-permute-start | bytes 393224 | tf_op jit(solution)/shard_map/ppermute | solution.py:19
  9.7 2.3 %collective-permute-done.3.refs_4_.refs_3_ = bf16[256,256]{1,0:T(8,128)(2,1)S(1)} collective-permute-done((bf16[256,256]{1,0:T(8,128)(2,1)S(1)}, bf16[256,256]{1,0:T(8,128)(2,1)S(1)}, u32[]{:S(2)}, u32[]{:S(2)}) %collective-permute-start.3) | collective-permute-done | bytes 131104 | tf_op jit(solution)/shard_map/ppermute | solution.py:19
  14.0 1.6 %collective-permute-start.4 = (bf16[256,256]{1,0:T(8,128)(2,1)S(1)}, bf16[256,256]{1,0:T(8,128)(2,1)S(1)}, u32[]{:S(2)}, u32[]{:S(2)}) collective-permute-start(bf16[256,256]{1,0:T(8,128)(2,1)S(1)} %collective-permute-done.3.refs_4_.refs_3_), channel_id=1, source_target_pairs={{0,4},{4,0},{8,12},{12,8},{16,20},{20,16},{24,28},{28,24},{1,5},{5... | collective-permute-start | bytes 393224 | tf_op jit(solution)/shard_map/ppermute | solution.py:19
  16.3 2.1 %collective-permute-done.5.refs_6_.refs_2_ = bf16[256,256]{1,0:T(8,128)(2,1)S(1)} collective-permute-done((bf16[256,256]{1,0:T(8,128)(2,1)S(1)}, bf16[256,256]{1,0:T(8,128)(2,1)S(1)}, u32[]{:S(2)}, u32[]{:S(2)}) %collective-permute-start.5) | collective-permute-done | bytes 131104 | tf_op jit(solution)/shard_map/ppermute | solution.py:19
  18.4 1.6 %collective-permute-start.6 = (bf16[256,256]{1,0:T(8,128)(2,1)S(1)}, bf16[256,256]{1,0:T(8,128)(2,1)S(1)}, u32[]{:S(2)}, u32[]{:S(2)}) collective-permute-start(bf16[256,256]{1,0:T(8,128)(2,1)S(1)} %collective-permute-done.5.refs_6_.refs_2_), channel_id=1, source_target_pairs={{0,4},{4,0},{8,12},{12,8},{16,20},{20,16},{24,28},{28,24},{1,5},{5... | collective-permute-start | bytes 393224 | tf_op jit(solution)/shard_map/ppermute | solution.py:19
  23.4 2.0 %shard_map.190 = (f32[2,32,512]{2,1,0:T(8,128)S(1)}, f32[2,32,512]{2,1,0:T(8,128)S(1)}, f32[8,32,512]{2,1,0:T(8,128)S(1)}) custom-call(bf16[768,2048]{1,0:T(8,128)(2,1)S(1)} %get-tuple-element.47.saved_ref, f32[768,256]{1,0:T(8,128)S(1)} %shard_map.189.mapped_ref, bf16[256,256]{1,0:T(8,128)(2,1)S(1)} %collective-permute-done.2.refs_3_.refs_0_, ...), custom_call_target="tpu_custom_call" | custom-call | flops 1006632960 | bytes 5242880 | tf_op jit(solution)/shard_map/pallas_call | solution.py:46
  25.4 1.6 %collective-permute-start.8 = (f32[2,32,512]{2,1,0:T(8,128)S(1)}, f32[2,32,512]{2,1,0:T(8,128)S(1)}, u32[]{:S(2)}, u32[]{:S(2)}) collective-permute-start(f32[2,32,512]{2,1,0:T(8,128)S(1)} %get-tuple-element.51), channel_id=1, source_target_pairs={{0,4},{4,0},{8,12},{12,8},{16,20},{20,16},{24,28},{28,24},{1,5},{5... | collective-permute-start | bytes 393224 | tf_op jit(solution)/shard_map/ppermute | solution.py:19
  28.0 2.4 %collective-permute-done.8.near = f32[2,32,512]{2,1,0:T(8,128)S(1)} collective-permute-done((f32[2,32,512]{2,1,0:T(8,128)S(1)}, f32[2,32,512]{2,1,0:T(8,128)S(1)}, u32[]{:S(2)}, u32[]{:S(2)}) %collective-permute-start.8) | collective-permute-done | bytes 131104 | tf_op jit(solution)/shard_map/ppermute | solution.py:19
  30.5 1.5 %collective-permute-start.12 = (f32[32,512]{1,0:T(8,128)S(1)}, f32[32,512]{1,0:T(8,128)S(1)}, u32[]{:S(2)}, u32[]{:S(2)}) collective-permute-start(f32[32,512]{1,0:T(8,128)S(1)} %shard_map.192), channel_id=1, source_target_pairs={{0,8},{4,12},{8,0},{12,4},{16,24},{20,28},{24,16},{28,20},{1,9},{5... | collective-permute-start | bytes 196616 | tf_op jit(solution)/shard_map/ppermute | solution.py:19
  32.1 3.4 %collective-permute-start.10 = (f32[32,512]{1,0:T(8,128)S(1)}, f32[32,512]{1,0:T(8,128)S(1)}, u32[]{:S(2)}, u32[]{:S(2)}) collective-permute-start(f32[32,512]{1,0:T(8,128)S(1)} %get-tuple-element.53), channel_id=1, source_target_pairs={{0,16},{4,20},{8,24},{12,28},{16,0},{20,4},{24,8},{28,12},{1,17},{... | collective-permute-start | bytes 196616 | tf_op jit(solution)/shard_map/ppermute | solution.py:19
  36.3 3.1 %collective-permute-done.10.r4 = f32[32,512]{1,0:T(8,128)S(1)} collective-permute-done((f32[32,512]{1,0:T(8,128)S(1)}, f32[32,512]{1,0:T(8,128)S(1)}, u32[]{:S(2)}, u32[]{:S(2)}) %collective-permute-start.10) | collective-permute-done | bytes 65568 | tf_op jit(solution)/shard_map/ppermute | solution.py:19
  39.4 2.2 %collective-permute-done.11.r6 = f32[32,512]{1,0:T(8,128)S(1)} collective-permute-done((f32[32,512]{1,0:T(8,128)S(1)}, f32[32,512]{1,0:T(8,128)S(1)}, u32[]{:S(2)}, u32[]{:S(2)}) %collective-permute-start.11) | collective-permute-done | bytes 65568 | tf_op jit(solution)/shard_map/ppermute | solution.py:19
  41.7 1.9 %collective-permute-start.17 = (f32[32,512]{1,0:T(8,128)S(1)}, f32[32,512]{1,0:T(8,128)S(1)}, u32[]{:S(2)}, u32[]{:S(2)}) collective-permute-start(f32[32,512]{1,0:T(8,128)S(1)} %get-tuple-element.56.refs_0_), channel_id=1, source_target_pairs={{0,16},{4,20},{8,24},{12,28},{16,0},{20,4},{24,8},{28,12},{1,17},{... | collective-permute-start | bytes 196616 | tf_op jit(solution)/shard_map/ppermute | solution.py:19
  43.5 2.5 %collective-permute-start.19 = (f32[32,512]{1,0:T(8,128)S(1)}, f32[32,512]{1,0:T(8,128)S(1)}, u32[]{:S(2)}, u32[]{:S(2)}) collective-permute-start(f32[32,512]{1,0:T(8,128)S(1)} %get-tuple-element.56.refs_0_), channel_id=1, source_target_pairs={{0,24},{4,28},{8,16},{12,20},{16,8},{20,12},{24,0},{28,4},{1,25},{... | collective-permute-start | bytes 196616 | tf_op jit(solution)/shard_map/ppermute | solution.py:19
  46.2 1.5 %collective-permute-start.28 = (f32[2,256,256]{2,1,0:T(8,128)S(1)}, f32[2,256,256]{2,1,0:T(8,128)S(1)}, u32[]{:S(2)}, u32[]{:S(2)}) collective-permute-start(f32[2,256,256]{2,1,0:T(8,128)S(1)} %get-tuple-element.61), channel_id=1, source_target_pairs={{0,4},{4,0},{8,12},{12,8},{16,20},{20,16},{24,28},{28,24},{1,5},{5... | collective-permute-start | bytes 1572872 | tf_op jit(solution)/shard_map/ppermute | solution.py:19
  48.3 5.8 %collective-permute-done.17.refs_4_ = f32[32,512]{1,0:T(8,128)S(1)} collective-permute-done((f32[32,512]{1,0:T(8,128)S(1)}, f32[32,512]{1,0:T(8,128)S(1)}, u32[]{:S(2)}, u32[]{:S(2)}) %collective-permute-start.17) | collective-permute-done | bytes 65568 | tf_op jit(solution)/shard_map/ppermute | solution.py:19
  54.0 1.5 %collective-permute-start.16 = (f32[32,512]{1,0:T(8,128)S(1)}, f32[32,512]{1,0:T(8,128)S(1)}, u32[]{:S(2)}, u32[]{:S(2)}) collective-permute-start(f32[32,512]{1,0:T(8,128)S(1)} %collective-permute-done.15.refs_2_), channel_id=1, source_target_pairs={{0,4},{4,0},{8,12},{12,8},{16,20},{20,16},{24,28},{28,24},{1,5},{5... | collective-permute-start | bytes 196616 | tf_op jit(solution)/shard_map/ppermute | solution.py:19
  56.1 3.4 %collective-permute-done.14.refs_1_ = f32[32,512]{1,0:T(8,128)S(1)} collective-permute-done((f32[32,512]{1,0:T(8,128)S(1)}, f32[32,512]{1,0:T(8,128)S(1)}, u32[]{:S(2)}, u32[]{:S(2)}) %collective-permute-start.14) | collective-permute-done | bytes 65568 | tf_op jit(solution)/shard_map/ppermute | solution.py:19
  60.2 1.5 %collective-permute-start.20 = (f32[32,512]{1,0:T(8,128)S(1)}, f32[32,512]{1,0:T(8,128)S(1)}, u32[]{:S(2)}, u32[]{:S(2)}) collective-permute-start(f32[32,512]{1,0:T(8,128)S(1)} %collective-permute-done.19.refs_6_), channel_id=1, source_target_pairs={{0,4},{4,0},{8,12},{12,8},{16,20},{20,16},{24,28},{28,24},{1,5},{5... | collective-permute-start | bytes 196616 | tf_op jit(solution)/shard_map/ppermute | solution.py:19
  61.7 2.7 %collective-permute-done.20.refs_7_ = f32[32,512]{1,0:T(8,128)S(1)} collective-permute-done((f32[32,512]{1,0:T(8,128)S(1)}, f32[32,512]{1,0:T(8,128)S(1)}, u32[]{:S(2)}, u32[]{:S(2)}) %collective-permute-start.20) | collective-permute-done | bytes 65568 | tf_op jit(solution)/shard_map/ppermute | solution.py:19
  64.5 2.6 %collective-permute-start.34 = (f32[256,256]{1,0:T(8,128)S(1)}, f32[256,256]{1,0:T(8,128)S(1)}, u32[]{:S(2)}, u32[]{:S(2)}) collective-permute-start(f32[256,256]{1,0:T(8,128)S(1)} %copy-done.1), channel_id=1, source_target_pairs={{0,16},{4,20},{8,24},{12,28},{16,0},{20,4},{24,8},{28,12},{1,17},{... | collective-permute-start | bytes 786440 | tf_op jit(solution)/shard_map/ppermute | solution.py:19
  68.6 2.0 %collective-permute-start.30 = (f32[256,256]{1,0:T(8,128)S(1)}, f32[256,256]{1,0:T(8,128)S(1)}, u32[]{:S(2)}, u32[]{:S(2)}) collective-permute-start(f32[256,256]{1,0:T(8,128)S(1)} %copy-done.1), channel_id=1, source_target_pairs={{0,8},{4,12},{8,0},{12,4},{16,24},{20,28},{24,16},{28,20},{1,9},{5... | collective-permute-start | bytes 786440 | tf_op jit(solution)/shard_map/ppermute | solution.py:19
  70.6 7.4 %collective-permute-done.34.refs_7_ = f32[256,256]{1,0:T(8,128)S(1)} collective-permute-done((f32[256,256]{1,0:T(8,128)S(1)}, f32[256,256]{1,0:T(8,128)S(1)}, u32[]{:S(2)}, u32[]{:S(2)}) %collective-permute-start.34) | collective-permute-done | bytes 262176 | tf_op jit(solution)/shard_map/ppermute | solution.py:19
  79.5 2.1 %collective-permute-done.21.refs_1_ = f32[8,128]{1,0:T(8,128)S(1)} collective-permute-done((f32[8,128]{1,0:T(8,128)S(1)}, f32[8,128]{1,0:T(8,128)S(1)}, u32[]{:S(2)}, u32[]{:S(2)}) %collective-permute-start.21) | collective-permute-done | bytes 4128 | tf_op jit(solution)/shard_map/ppermute | solution.py:19
  81.6 3.0 %collective-permute-done.22.refs_2_ = f32[8,128]{1,0:T(8,128)S(1)} collective-permute-done((f32[8,128]{1,0:T(8,128)S(1)}, f32[8,128]{1,0:T(8,128)S(1)}, u32[]{:S(2)}, u32[]{:S(2)}) %collective-permute-start.22) | collective-permute-done | bytes 4128 | tf_op jit(solution)/shard_map/ppermute | solution.py:19
  86.8 1.6 %collective-permute-start.39 = (bf16[2,256,256]{2,1,0:T(8,128)(2,1)S(1)}, bf16[2,256,256]{2,1,0:T(8,128)(2,1)S(1)}, u32[]{:S(2)}, u32[]{:S(2)}) collective-permute-start(bf16[2,256,256]{2,1,0:T(8,128)(2,1)S(1)} %get-tuple-element.71.refs_3_), channel_id=1, source_target_pairs={{0,4},{4,0},{8,12},{12,8},{16,20},{20,16},{24,28},{28,24},{1,5},{5... | collective-permute-start | bytes 786440 | tf_op jit(solution)/shard_map/ppermute | solution.py:19
  88.4 2.0 %collective-permute-start.37 = (bf16[256,256]{1,0:T(8,128)(2,1)S(1)}, bf16[256,256]{1,0:T(8,128)(2,1)S(1)}, u32[]{:S(2)}, u32[]{:S(2)}) collective-permute-start(bf16[256,256]{1,0:T(8,128)(2,1)S(1)} %get-tuple-element.70), channel_id=1, source_target_pairs={{0,8},{4,12},{8,0},{12,4},{16,24},{20,28},{24,16},{28,20},{1,9},{5... | collective-permute-start | bytes 393224 | tf_op jit(solution)/shard_map/ppermute | solution.py:19
  91.7 3.1 %collective-permute-done.35.refs_1_ = bf16[256,256]{1,0:T(8,128)(2,1)S(1)} collective-permute-done((bf16[256,256]{1,0:T(8,128)(2,1)S(1)}, bf16[256,256]{1,0:T(8,128)(2,1)S(1)}, u32[]{:S(2)}, u32[]{:S(2)}) %collective-permute-start.35) | collective-permute-done | bytes 131104 | tf_op jit(solution)/shard_map/ppermute | solution.py:19
  95.3 2.3 %collective-permute-done.37.refs_2_ = bf16[256,256]{1,0:T(8,128)(2,1)S(1)} collective-permute-done((bf16[256,256]{1,0:T(8,128)(2,1)S(1)}, bf16[256,256]{1,0:T(8,128)(2,1)S(1)}, u32[]{:S(2)}, u32[]{:S(2)}) %collective-permute-start.37) | collective-permute-done | bytes 131104 | tf_op jit(solution)/shard_map/ppermute | solution.py:19
  101.0 1.5 %collective-permute-done.38.refs_2_ = bf16[256,256]{1,0:T(8,128)(2,1)S(1)} collective-permute-done((bf16[256,256]{1,0:T(8,128)(2,1)S(1)}, bf16[256,256]{1,0:T(8,128)(2,1)S(1)}, u32[]{:S(2)}, u32[]{:S(2)}) %collective-permute-start.38) | collective-permute-done | bytes 131104 | tf_op jit(solution)/shard_map/ppermute | solution.py:19
  (76 shorter events, 22.2 us)
Async XLA Ops:
  1.6 10.4 %collective-permute-start.3 = (bf16[256,256]{1,0:T(8,128)(2,1)S(1)}, bf16[256,256]{1,0:T(8,128)(2,1)S(1)}, u32[]{:S(2)}, u32[]{:S(2)}) collective-permute-start(bf16[256,256]{1,0:T(8,128)(2,1)S(1)} %shard_map.186.refs_0_), channel_id=1, source_target_pairs={{0,16},{4,20},{8,24},{12,28},{16,0},{20,4},{24,8},{28,12},{1,17},{... | collective-permute-start | bytes 393224 | tf_op jit(solution)/shard_map/ppermute | solution.py:19
  8.1 15.3 %collective-permute-start.7 = (bf16[768,256]{1,0:T(8,128)(2,1)S(1)}, bf16[768,256]{1,0:T(8,128)(2,1)S(1)}, u32[]{:S(2)}, u32[]{:S(2)}) collective-permute-start(bf16[768,256]{1,0:T(8,128)(2,1)S(1)} %get-tuple-element.49), channel_id=1, source_target_pairs={{0,1},{1,0},{2,3},{3,2},{4,5},{5,4},{6,7},{7,6},{8,9},{9,8},{10,11... | collective-permute-start | bytes 1179656 | tf_op jit(solution)/shard_map/ppermute | solution.py:19
  8.1 7.5 %collective-permute-start = (bf16[256,256]{1,0:T(8,128)(2,1)S(1)}, bf16[256,256]{1,0:T(8,128)(2,1)S(1)}, u32[]{:S(2)}, u32[]{:S(2)}) collective-permute-start(bf16[256,256]{1,0:T(8,128)(2,1)S(1)} %shard_map.186.refs_0_), channel_id=1, source_target_pairs={{0,4},{4,0},{8,12},{12,8},{16,20},{20,16},{24,28},{28,24},{1,5},{5... | collective-permute-start | bytes 393224 | tf_op jit(solution)/shard_map/ppermute | solution.py:19
  12.0 6.4 %collective-permute-start.5 = (bf16[256,256]{1,0:T(8,128)(2,1)S(1)}, bf16[256,256]{1,0:T(8,128)(2,1)S(1)}, u32[]{:S(2)}, u32[]{:S(2)}) collective-permute-start(bf16[256,256]{1,0:T(8,128)(2,1)S(1)} %collective-permute-done.3.refs_4_.refs_3_), channel_id=1, source_target_pairs={{0,8},{4,12},{8,0},{12,4},{16,24},{20,28},{24,16},{28,20},{1,9},{5... | collective-permute-start | bytes 393224 | tf_op jit(solution)/shard_map/ppermute | solution.py:19
  12.7 8.1 %collective-permute-start.1 = (bf16[256,256]{1,0:T(8,128)(2,1)S(1)}, bf16[256,256]{1,0:T(8,128)(2,1)S(1)}, u32[]{:S(2)}, u32[]{:S(2)}) collective-permute-start(bf16[256,256]{1,0:T(8,128)(2,1)S(1)} %shard_map.186.refs_0_), channel_id=1, source_target_pairs={{0,8},{4,12},{8,0},{12,4},{16,24},{20,28},{24,16},{28,20},{1,9},{5... | collective-permute-start | bytes 393224 | tf_op jit(solution)/shard_map/ppermute | solution.py:19
  14.0 7.4 %collective-permute-start.4 = (bf16[256,256]{1,0:T(8,128)(2,1)S(1)}, bf16[256,256]{1,0:T(8,128)(2,1)S(1)}, u32[]{:S(2)}, u32[]{:S(2)}) collective-permute-start(bf16[256,256]{1,0:T(8,128)(2,1)S(1)} %collective-permute-done.3.refs_4_.refs_3_), channel_id=1, source_target_pairs={{0,4},{4,0},{8,12},{12,8},{16,20},{20,16},{24,28},{28,24},{1,5},{5... | collective-permute-start | bytes 393224 | tf_op jit(solution)/shard_map/ppermute | solution.py:19
  15.6 6.7 %collective-permute-start.2 = (bf16[256,256]{1,0:T(8,128)(2,1)S(1)}, bf16[256,256]{1,0:T(8,128)(2,1)S(1)}, u32[]{:S(2)}, u32[]{:S(2)}) collective-permute-start(bf16[256,256]{1,0:T(8,128)(2,1)S(1)} %collective-permute-done.refs_1_), channel_id=1, source_target_pairs={{0,8},{4,12},{8,0},{12,4},{16,24},{20,28},{24,16},{28,20},{1,9},{5... | collective-permute-start | bytes 393224 | tf_op jit(solution)/shard_map/ppermute | solution.py:19
  27.5 18.7 %collective-permute-start.27 = (bf16[256,256]{1,0:T(8,128)(2,1)S(1)}, bf16[256,256]{1,0:T(8,128)(2,1)S(1)}, u32[]{:S(2)}, u32[]{:S(2)}) collective-permute-start(bf16[256,256]{1,0:T(8,128)(2,1)S(1)} %collective-permute-done.3.refs_4_.refs_3_), channel_id=1, source_target_pairs={{0,1},{1,0},{2,3},{3,2},{4,5},{5,4},{6,7},{7,6},{8,9},{9,8},{10,11... | collective-permute-start | bytes 393224 | tf_op jit(solution)/shard_map/ppermute | solution.py:19
  27.5 8.8 %collective-permute-start.13 = (f32[2,32,256]{2,1,0:T(8,128)S(1)}, f32[2,32,256]{2,1,0:T(8,128)S(1)}, u32[]{:S(2)}, u32[]{:S(2)}) collective-permute-start(f32[2,32,256]{2,1,0:T(8,128)S(1)} %get-tuple-element.55), channel_id=1, source_target_pairs={{0,1},{1,0},{2,3},{3,2},{4,5},{5,4},{6,7},{7,6},{8,9},{9,8},{10,11... | collective-permute-start | bytes 196616 | tf_op jit(solution)/shard_map/ppermute | solution.py:19
  30.5 5.8 %collective-permute-start.12 = (f32[32,512]{1,0:T(8,128)S(1)}, f32[32,512]{1,0:T(8,128)S(1)}, u32[]{:S(2)}, u32[]{:S(2)}) collective-permute-start(f32[32,512]{1,0:T(8,128)S(1)} %shard_map.192), channel_id=1, source_target_pairs={{0,8},{4,12},{8,0},{12,4},{16,24},{20,28},{24,16},{28,20},{1,9},{5... | collective-permute-start | bytes 196616 | tf_op jit(solution)/shard_map/ppermute | solution.py:19
  32.1 7.3 %collective-permute-start.10 = (f32[32,512]{1,0:T(8,128)S(1)}, f32[32,512]{1,0:T(8,128)S(1)}, u32[]{:S(2)}, u32[]{:S(2)}) collective-permute-start(f32[32,512]{1,0:T(8,128)S(1)} %get-tuple-element.53), channel_id=1, source_target_pairs={{0,16},{4,20},{8,24},{12,28},{16,0},{20,4},{24,8},{28,12},{1,17},{... | collective-permute-start | bytes 196616 | tf_op jit(solution)/shard_map/ppermute | solution.py:19
  35.5 6.1 %collective-permute-start.11 = (f32[32,512]{1,0:T(8,128)S(1)}, f32[32,512]{1,0:T(8,128)S(1)}, u32[]{:S(2)}, u32[]{:S(2)}) collective-permute-start(f32[32,512]{1,0:T(8,128)S(1)} %get-tuple-element.54), channel_id=1, source_target_pairs={{0,24},{4,28},{8,16},{12,20},{16,8},{20,12},{24,0},{28,4},{1,25},{... | collective-permute-start | bytes 196616 | tf_op jit(solution)/shard_map/ppermute | solution.py:19
  41.6 6.2 %collective-permute-start.15 = (f32[32,512]{1,0:T(8,128)S(1)}, f32[32,512]{1,0:T(8,128)S(1)}, u32[]{:S(2)}, u32[]{:S(2)}) collective-permute-start(f32[32,512]{1,0:T(8,128)S(1)} %get-tuple-element.56.refs_0_), channel_id=1, source_target_pairs={{0,8},{4,12},{8,0},{12,4},{16,24},{20,28},{24,16},{28,20},{1,9},{5... | collective-permute-start | bytes 196616 | tf_op jit(solution)/shard_map/ppermute | solution.py:19
  41.7 12.3 %collective-permute-start.17 = (f32[32,512]{1,0:T(8,128)S(1)}, f32[32,512]{1,0:T(8,128)S(1)}, u32[]{:S(2)}, u32[]{:S(2)}) collective-permute-start(f32[32,512]{1,0:T(8,128)S(1)} %get-tuple-element.56.refs_0_), channel_id=1, source_target_pairs={{0,16},{4,20},{8,24},{12,28},{16,0},{20,4},{24,8},{28,12},{1,17},{... | collective-permute-start | bytes 196616 | tf_op jit(solution)/shard_map/ppermute | solution.py:19
  43.5 12.0 %collective-permute-start.19 = (f32[32,512]{1,0:T(8,128)S(1)}, f32[32,512]{1,0:T(8,128)S(1)}, u32[]{:S(2)}, u32[]{:S(2)}) collective-permute-start(f32[32,512]{1,0:T(8,128)S(1)} %get-tuple-element.56.refs_0_), channel_id=1, source_target_pairs={{0,24},{4,28},{8,16},{12,20},{16,8},{20,12},{24,0},{28,4},{1,25},{... | collective-permute-start | bytes 196616 | tf_op jit(solution)/shard_map/ppermute | solution.py:19
  46.1 22.5 %collective-permute-start.33 = (f32[256,256]{1,0:T(8,128)S(1)}, f32[256,256]{1,0:T(8,128)S(1)}, u32[]{:S(2)}, u32[]{:S(2)}) collective-permute-start(f32[256,256]{1,0:T(8,128)S(1)} %copy-done), channel_id=1, source_target_pairs={{0,16},{4,20},{8,24},{12,28},{16,0},{20,4},{24,8},{28,12},{1,17},{... | collective-permute-start | bytes 786440 | tf_op jit(solution)/shard_map/ppermute | solution.py:19
  46.2 44.2 %collective-permute-start.28 = (f32[2,256,256]{2,1,0:T(8,128)S(1)}, f32[2,256,256]{2,1,0:T(8,128)S(1)}, u32[]{:S(2)}, u32[]{:S(2)}) collective-permute-start(f32[2,256,256]{2,1,0:T(8,128)S(1)} %get-tuple-element.61), channel_id=1, source_target_pairs={{0,4},{4,0},{8,12},{12,8},{16,20},{20,16},{24,28},{28,24},{1,5},{5... | collective-permute-start | bytes 1572872 | tf_op jit(solution)/shard_map/ppermute | solution.py:19
  47.8 11.7 %collective-permute-start.14 = (f32[32,512]{1,0:T(8,128)S(1)}, f32[32,512]{1,0:T(8,128)S(1)}, u32[]{:S(2)}, u32[]{:S(2)}) collective-permute-start(f32[32,512]{1,0:T(8,128)S(1)} %get-tuple-element.56.refs_0_), channel_id=1, source_target_pairs={{0,4},{4,0},{8,12},{12,8},{16,20},{20,16},{24,28},{28,24},{1,5},{5... | collective-permute-start | bytes 196616 | tf_op jit(solution)/shard_map/ppermute | solution.py:19
  54.0 6.2 %collective-permute-start.16 = (f32[32,512]{1,0:T(8,128)S(1)}, f32[32,512]{1,0:T(8,128)S(1)}, u32[]{:S(2)}, u32[]{:S(2)}) collective-permute-start(f32[32,512]{1,0:T(8,128)S(1)} %collective-permute-done.15.refs_2_), channel_id=1, source_target_pairs={{0,4},{4,0},{8,12},{12,8},{16,20},{20,16},{24,28},{28,24},{1,5},{5... | collective-permute-start | bytes 196616 | tf_op jit(solution)/shard_map/ppermute | solution.py:19
  55.5 6.2 %collective-permute-start.18 = (f32[32,512]{1,0:T(8,128)S(1)}, f32[32,512]{1,0:T(8,128)S(1)}, u32[]{:S(2)}, u32[]{:S(2)}) collective-permute-start(f32[32,512]{1,0:T(8,128)S(1)} %collective-permute-done.17.refs_4_), channel_id=1, source_target_pairs={{0,4},{4,0},{8,12},{12,8},{16,20},{20,16},{24,28},{28,24},{1,5},{5... | collective-permute-start | bytes 196616 | tf_op jit(solution)/shard_map/ppermute | solution.py:19
  59.5 8.9 %collective-permute-start.25 = (bf16[256,256]{1,0:T(8,128)(2,1)S(1)}, bf16[256,256]{1,0:T(8,128)(2,1)S(1)}, u32[]{:S(2)}, u32[]{:S(2)}) collective-permute-start(bf16[256,256]{1,0:T(8,128)(2,1)S(1)} %collective-permute-done.refs_1_), channel_id=1, source_target_pairs={{0,1},{1,0},{2,3},{3,2},{4,5},{5,4},{6,7},{7,6},{8,9},{9,8},{10,11... | collective-permute-start | bytes 393224 | tf_op jit(solution)/shard_map/ppermute | solution.py:19
  61.7 6.8 %collective-permute-start.26 = (bf16[256,256]{1,0:T(8,128)(2,1)S(1)}, bf16[256,256]{1,0:T(8,128)(2,1)S(1)}, u32[]{:S(2)}, u32[]{:S(2)}) collective-permute-start(bf16[256,256]{1,0:T(8,128)(2,1)S(1)} %collective-permute-done.1.refs_2_), channel_id=1, source_target_pairs={{0,1},{1,0},{2,3},{3,2},{4,5},{5,4},{6,7},{7,6},{8,9},{9,8},{10,11... | collective-permute-start | bytes 393224 | tf_op jit(solution)/shard_map/ppermute | solution.py:19
  64.5 13.5 %collective-permute-start.34 = (f32[256,256]{1,0:T(8,128)S(1)}, f32[256,256]{1,0:T(8,128)S(1)}, u32[]{:S(2)}, u32[]{:S(2)}) collective-permute-start(f32[256,256]{1,0:T(8,128)S(1)} %copy-done.1), channel_id=1, source_target_pairs={{0,16},{4,20},{8,24},{12,28},{16,0},{20,4},{24,8},{28,12},{1,17},{... | collective-permute-start | bytes 786440 | tf_op jit(solution)/shard_map/ppermute | solution.py:19
  68.4 16.9 %collective-permute-start.24 = (f32[256,256]{1,0:T(8,128)S(1)}, f32[256,256]{1,0:T(8,128)S(1)}, u32[]{:S(2)}, u32[]{:S(2)}) collective-permute-start(f32[256,256]{1,0:T(8,128)S(1)} %get-tuple-element.59), channel_id=1, source_target_pairs={{0,1},{1,0},{2,3},{3,2},{4,5},{5,4},{6,7},{7,6},{8,9},{9,8},{10,11... | collective-permute-start | bytes 786440 | tf_op jit(solution)/shard_map/ppermute | solution.py:19
  68.5 19.9 %collective-permute-start.29 = (f32[256,256]{1,0:T(8,128)S(1)}, f32[256,256]{1,0:T(8,128)S(1)}, u32[]{:S(2)}, u32[]{:S(2)}) collective-permute-start(f32[256,256]{1,0:T(8,128)S(1)} %copy-done), channel_id=1, source_target_pairs={{0,8},{4,12},{8,0},{12,4},{16,24},{20,28},{24,16},{28,20},{1,9},{5... | collective-permute-start | bytes 786440 | tf_op jit(solution)/shard_map/ppermute | solution.py:19
  68.6 19.8 %collective-permute-start.30 = (f32[256,256]{1,0:T(8,128)S(1)}, f32[256,256]{1,0:T(8,128)S(1)}, u32[]{:S(2)}, u32[]{:S(2)}) collective-permute-start(f32[256,256]{1,0:T(8,128)S(1)} %copy-done.1), channel_id=1, source_target_pairs={{0,8},{4,12},{8,0},{12,4},{16,24},{20,28},{24,16},{28,20},{1,9},{5... | collective-permute-start | bytes 786440 | tf_op jit(solution)/shard_map/ppermute | solution.py:19
  84.6 5.8 %collective-permute-start.31 = (f32[2,32,256]{2,1,0:T(8,128)S(1)}, f32[2,32,256]{2,1,0:T(8,128)S(1)}, u32[]{:S(2)}, u32[]{:S(2)}) collective-permute-start(f32[2,32,256]{2,1,0:T(8,128)S(1)} %get-tuple-element.63), channel_id=1, source_target_pairs={{0,1},{1,0},{2,3},{3,2},{4,5},{5,4},{6,7},{7,6},{8,9},{9,8},{10,11... | collective-permute-start | bytes 196616 | tf_op jit(solution)/shard_map/ppermute | solution.py:19
  86.8 12.3 %collective-permute-start.39 = (bf16[2,256,256]{2,1,0:T(8,128)(2,1)S(1)}, bf16[2,256,256]{2,1,0:T(8,128)(2,1)S(1)}, u32[]{:S(2)}, u32[]{:S(2)}) collective-permute-start(bf16[2,256,256]{2,1,0:T(8,128)(2,1)S(1)} %get-tuple-element.71.refs_3_), channel_id=1, source_target_pairs={{0,4},{4,0},{8,12},{12,8},{16,20},{20,16},{24,28},{28,24},{1,5},{5... | collective-permute-start | bytes 786440 | tf_op jit(solution)/shard_map/ppermute | solution.py:19
  88.4 6.4 %collective-permute-start.35 = (bf16[256,256]{1,0:T(8,128)(2,1)S(1)}, bf16[256,256]{1,0:T(8,128)(2,1)S(1)}, u32[]{:S(2)}, u32[]{:S(2)}) collective-permute-start(bf16[256,256]{1,0:T(8,128)(2,1)S(1)} %get-tuple-element.69), channel_id=1, source_target_pairs={{0,8},{4,12},{8,0},{12,4},{16,24},{20,28},{24,16},{28,20},{1,9},{5... | collective-permute-start | bytes 393224 | tf_op jit(solution)/shard_map/ppermute | solution.py:19
  88.4 9.2 %collective-permute-start.37 = (bf16[256,256]{1,0:T(8,128)(2,1)S(1)}, bf16[256,256]{1,0:T(8,128)(2,1)S(1)}, u32[]{:S(2)}, u32[]{:S(2)}) collective-permute-start(bf16[256,256]{1,0:T(8,128)(2,1)S(1)} %get-tuple-element.70), channel_id=1, source_target_pairs={{0,8},{4,12},{8,0},{12,4},{16,24},{20,28},{24,16},{28,20},{1,9},{5... | collective-permute-start | bytes 393224 | tf_op jit(solution)/shard_map/ppermute | solution.py:19
  91.6 10.9 %collective-permute-start.32 = (bf16[2,256,256]{2,1,0:T(8,128)(2,1)S(1)}, bf16[2,256,256]{2,1,0:T(8,128)(2,1)S(1)}, u32[]{:S(2)}, u32[]{:S(2)}) collective-permute-start(bf16[2,256,256]{2,1,0:T(8,128)(2,1)S(1)} %get-tuple-element.68.refs_1_), channel_id=1, source_target_pairs={{0,8},{4,12},{8,0},{12,4},{16,24},{20,28},{24,16},{28,20},{1,9},{5... | collective-permute-start | bytes 786440 | tf_op jit(solution)/shard_map/ppermute | solution.py:19
  94.8 6.2 %collective-permute-start.36 = (bf16[256,256]{1,0:T(8,128)(2,1)S(1)}, bf16[256,256]{1,0:T(8,128)(2,1)S(1)}, u32[]{:S(2)}, u32[]{:S(2)}) collective-permute-start(bf16[256,256]{1,0:T(8,128)(2,1)S(1)} %collective-permute-done.35.refs_1_), channel_id=1, source_target_pairs={{0,4},{4,0},{8,12},{12,8},{16,20},{20,16},{24,28},{28,24},{1,5},{5... | collective-permute-start | bytes 393224 | tf_op jit(solution)/shard_map/ppermute | solution.py:19
  (14 other events, 168.5 us)
